TPU v7x, 128 devices: a whole 4x4x4 slice. The times are simulated.
128 devices in a mesh: sp: 32 (over z, y, core), tp: 4 (over x).
Axes of the slice: x: 4, y: 4, z: 4, core: 2. Of those that a mesh axis runs over, the one named last changes fastest.
Arguments:
- mixer_output_stream: bfloat16 [4096, 2048], P('sp', 'tp'), may hold values from -6 to 6
- layer_output_gradient: bfloat16 [4096, 2048], P('sp', 'tp'), may hold values from -3.5 to 3.5
- routes: int32 [4096, 2], P('sp'), may hold values from 0 to 31, all different within a row; in each aligned block of 128 rows (0 to 127, 128 to 255, ...) at most 12 rows name the same one
- expert_combine_weight: float32 [4096, 2], P('sp'), may hold values from 0.2 to 1
- expert_gate_weight: bfloat16 [32, 2048, 3584], P('sp', None, 'tp'), may hold values from -0.125 to 0.125
- expert_up_weight: bfloat16 [32, 2048, 3584], P('sp', None, 'tp'), may hold values from -0.125 to 0.125
- expert_down_weight: bfloat16 [32, 3584, 2048], P('sp', 'tp'), may hold values from -0.09375 to 0.09375
- head_mixer_input: bfloat16 [4096, 4096], P('sp', 'tp'), may hold values from -6 to 6
- head_step_size: float32 [4096, 64], P('sp', 'tp'), may hold values from 0.25 to 4
- head_decay_rate: float32 [64], P('tp'), may hold values from 0 to 1
- extra_log_decay: float32 [4096, 64], P('sp', 'tp'), may hold values from -3 to 0
- state_entering_span: float32 [64, 64, 128], P('tp'), may hold values from -48 to 48
- state_input_vectors: bfloat16 [4096, 1024], P('sp', 'tp'), may hold values from -1.75 to 1.75
- state_readout_vectors: bfloat16 [4096, 1024], P('sp', 'tp'), may hold values from -1.75 to 1.75
- gate_preactivation: bfloat16 [4096, 4096], P('sp', 'tp'), may hold values from -6 to 6
- group_norm_scale: float32 [4096], P('tp'), may hold values from 0.1 to 1.9
- mixer_output_weight: bfloat16 [4096, 2048], P('tp', 'sp'), may hold values from -0.09375 to 0.09375
Outputs:
- grad_gate: bfloat16 [32, 2048, 3584], P('sp', None, 'tp')
- grad_up: bfloat16 [32, 2048, 3584], P('sp', None, 'tp')
- grad_down: bfloat16 [32, 3584, 2048], P('sp', 'tp')
- grad_out_proj: float32 [4096, 2048], P('tp', 'sp')
- grad_input: bfloat16 [4096, 4096], P('sp', 'tp')
- grad_step: float32 [4096, 64], P('sp', 'tp')
- grad_state_in: bfloat16 [4096, 1024], P('sp', 'tp')
- grad_read_out: bfloat16 [4096, 1024], P('sp', 'tp')
- grad_gate_in: bfloat16 [4096, 4096], P('sp', 'tp')
Inputs may be any that keep to these rules, and one draw needn't show every extreme that they name: `routes`: the two experts of a token differ. In each aligned block of 128 rows no expert is named more than 12 times, and in every draw some expert is named exactly 12 times in some block.
All inputs are finite; a program needn't handle non-finite values.
Results may differ from a plain program's by a relative error of at most 0.02.
Values may be sent and summed in bfloat16 or wider, within the bound.
A program may use at most 128 MiB of HBM per device.

v0:
```python
import jax
import jax.numpy as jnp
from jax import lax
from jax.sharding import Mesh
from jax.sharding import PartitionSpec as P

HDIM = 64
STATE = 128
BLK = 128
SP = ("sp_0", "sp_1", "sp_2")


norm_eps = 1e-05
exact_mode = lax.Precision.HIGHEST


def split_up(x, dim, length):
    lengths = x.shape
    blocks = x.reshape(*lengths[:dim], length, lengths[dim] // length, *lengths[dim + 1 :])
    return jnp.moveaxis(blocks, dim, 0)


def sum_at_owner(x, axis, dim):
    length = lax.axis_size(axis)
    blocks = lax.all_to_all(split_up(x, dim, length), axis, 0, 0, tiled=True)
    return jnp.sum(blocks.astype(jnp.float32), axis=0)


def nothing_yet(x, identity):
    return jax.tree.map(
        lambda part, zero: jnp.zeros_like(part) + jnp.asarray(zero, part.dtype), x, identity
    )


def prefix_by_axis(x, axes, combine, identity):
    before = start = nothing_yet(x, identity)
    subtotal = x
    for axis in reversed(axes):
        length, here = (lax.axis_size(axis), lax.axis_index(axis))
        pieces = jax.tree.map(
            lambda part, kind: lax.all_gather(part.astype(kind), axis),
            subtotal,
            (jnp.bfloat16, jnp.bfloat16),
        )
        inside, subtotal = (start, start)
        for k in range(length):
            passed = k < here
            subtotal = combine(
                subtotal, jax.tree.map(lambda part, own: part[k].astype(own.dtype), pieces, x)
            )
            inside = jax.tree.map(lambda new, old: jnp.where(passed, new, old), subtotal, inside)
        before = combine(inside, before)
    return before


def prefix_by_axis_2(x, axes, combine, identity):
    before = start = nothing_yet(x, identity)
    subtotal = x
    for axis in reversed(axes):
        length, here = (lax.axis_size(axis), lax.axis_index(axis))
        pieces = jax.tree.map(
            lambda part, kind: lax.all_gather(part.astype(kind), axis),
            subtotal,
            jax.tree.map(lambda a: jnp.bfloat16 if a.dtype == jnp.float32 else a.dtype, x),
        )
        inside, subtotal = (start, start)
        for k in reversed(range(length)):
            passed = k > here
            subtotal = combine(
                subtotal, jax.tree.map(lambda part, own: part[k].astype(own.dtype), pieces, x)
            )
            inside = jax.tree.map(lambda new, old: jnp.where(passed, new, old), subtotal, inside)
        before = combine(inside, before)
    return before


def span_local_scan(
    input_heads,
    time_step,
    decay_speed,
    sudden_decay,
    input_vector_groups,
    readout_groups,
    starting_state,
):
    length, head_count, head_size = input_heads.shape
    groups, state_size = (input_vector_groups.shape[1], input_vector_groups.shape[2])
    per_group = head_count // groups
    block_count = length // BLK
    log_decay_total = sudden_decay - time_step * decay_speed[None, :]
    scaled = (input_heads * time_step[:, :, None]).reshape(
        block_count, BLK, groups, per_group, head_size
    )
    log_decay_total = log_decay_total.reshape(block_count, BLK, groups, per_group)
    b_rows = input_vector_groups.reshape(block_count, BLK, groups, state_size)
    c_rows = readout_groups.reshape(block_count, BLK, groups, state_size)
    cumulative = jnp.cumsum(log_decay_total, axis=1)
    causal_mask = jnp.tril(jnp.ones((BLK, BLK), dtype=bool))
    cum_t = jnp.moveaxis(cumulative, 1, -1)
    gaps = cum_t[..., :, None] - cum_t[..., None, :]
    decays = jnp.where(causal_mask, jnp.exp(jnp.where(causal_mask, gaps, 0.0)), 0.0)
    affinity = jnp.einsum("blgn,bsgn->bgls", c_rows, b_rows, precision=exact_mode)
    y_diag = jnp.einsum(
        "bghls,bsghp->blghp", affinity[:, :, None] * decays, scaled, precision=exact_mode
    )
    to_end = jnp.exp(cumulative[:, -1:] - cumulative)
    states = jnp.einsum(
        "blgn,blghp->bghpn", b_rows, scaled * to_end[..., None], precision=exact_mode
    )
    block_decay = jnp.exp(cumulative[:, -1])

    def advance(running, inputs):
        block_state, decay_now = inputs
        return (decay_now[..., None, None] * running + block_state, running)

    first_state = starting_state.reshape(groups, per_group, head_size, state_size)
    closing_state, incoming_state = lax.scan(advance, first_state, (states, block_decay))
    y_off = (
        jnp.einsum("blgn,bghpn->blghp", c_rows, incoming_state, precision=exact_mode)
        * jnp.exp(cumulative)[..., None]
    )
    result_rows = (y_diag + y_off).reshape(length, head_count, head_size)
    return (result_rows, closing_state.reshape(head_count, head_size, state_size))


def span_final_state(input_heads, time_step, decay_speed, sudden_decay, input_vector_groups):
    length, head_count, head_size = input_heads.shape
    groups = input_vector_groups.shape[1]
    log_decay_total = sudden_decay - time_step * decay_speed[None, :]
    sum_total = jnp.sum(log_decay_total, axis=0)
    after = sum_total[None, :] - jnp.cumsum(log_decay_total, axis=0)
    weighted = (input_heads * (time_step * jnp.exp(after))[:, :, None]).reshape(
        length, groups, head_count // groups, head_size
    )
    result = jnp.einsum("tgn,tghp->ghpn", input_vector_groups, weighted, precision=exact_mode)
    return (result.reshape(head_count, head_size, -1), jnp.exp(sum_total))


def carried_weight(scanned_gradient, readout_groups, time_step, decay_speed, sudden_decay):
    length, head_count, head_size = scanned_gradient.shape
    groups = readout_groups.shape[1]
    log_decay_total = sudden_decay - time_step * decay_speed[None, :]
    weighted = (
        scanned_gradient * jnp.exp(jnp.cumsum(log_decay_total, axis=0))[:, :, None]
    ).reshape(length, groups, head_count // groups, head_size)
    result = jnp.einsum("tgn,tghp->ghpn", readout_groups, weighted, precision=exact_mode)
    return result.reshape(head_count, head_size, -1)


def join_spans(earlier, later):
    return (later[1][:, None, None] * earlier[0] + later[0], earlier[1] * later[1])


def gate_norm(scan_out, gate_vals, group_norm_scale, groups):
    length = scan_out.shape[0]
    gated = scan_out.reshape(length, -1) * jax.nn.silu(gate_vals)
    grouped = gated.reshape(length, groups, -1)
    factor = lax.rsqrt(jnp.mean(grouped * grouped, axis=-1, keepdims=True) + norm_eps)
    return (grouped * factor).reshape(length, -1) * group_norm_scale[None, :]


def slot_index(route_rows, expert_count, capacity):
    flat_routes = route_rows.reshape(-1)
    onehot = (flat_routes[:, None] == jnp.arange(expert_count, dtype=jnp.int32)[None, :]).astype(
        jnp.int32
    )
    before = jnp.cumsum(onehot, axis=0) - onehot
    return flat_routes * capacity + jnp.sum(before * onehot, axis=1)


def build_table(destination, slot_count):
    pair_count = destination.shape[0]
    return (
        jnp.full((slot_count,), pair_count, jnp.int32)
        .at[destination]
        .set(jnp.arange(pair_count, dtype=jnp.int32))
    )


def pack_rows(stream, grad_rows, slot_table, weights):
    token_of = slot_table // 2
    routed = jnp.take(stream, token_of, axis=0, mode="fill", fill_value=0)
    weight_of = jnp.take(weights.reshape(-1), slot_table, mode="fill", fill_value=0.0)
    picked = jnp.take(grad_rows, token_of, axis=0, mode="fill", fill_value=0).astype(jnp.float32)
    return (routed, (picked * weight_of[:, None]).astype(jnp.bfloat16))


def expert_hidden(routed_rows, routed_grads, w_gate, w_up, w_down):
    pre_gate = jnp.dot(routed_rows, w_gate, preferred_element_type=jnp.float32)
    pre_up = jnp.dot(routed_rows, w_up, preferred_element_type=jnp.float32)
    activated = jax.nn.silu(pre_gate)
    hidden = (activated * pre_up).astype(jnp.bfloat16)
    hidden_grad = lax.dot_general(
        routed_grads, w_down, (((1,), (1,)), ((), ())), preferred_element_type=jnp.float32
    )
    sigmoid_gate = jax.nn.sigmoid(pre_gate)
    gate_grad = (
        hidden_grad * pre_up * sigmoid_gate * (1.0 + pre_gate * (1.0 - sigmoid_gate))
    ).astype(jnp.bfloat16)
    up_grad = (hidden_grad * activated).astype(jnp.bfloat16)
    return (hidden, gate_grad, up_grad)


def expert_weight_grads(routed_rows, routed_grads, hidden, gate_grad, up_grad):
    contract = (((0,), (0,)), ((), ()))
    grad_g = lax.dot_general(routed_rows, gate_grad, contract, preferred_element_type=jnp.float32)
    grad_u = lax.dot_general(routed_rows, up_grad, contract, preferred_element_type=jnp.float32)
    grad_d = lax.dot_general(hidden, routed_grads, contract, preferred_element_type=jnp.float32)
    return (grad_g.astype(jnp.bfloat16), grad_u.astype(jnp.bfloat16), grad_d.astype(jnp.bfloat16))


def row_partial(gate_grad, up_grad, w_gate, w_up):
    contract = (((1,), (1,)), ((), ()))
    partial_sum = lax.dot_general(gate_grad, w_gate, contract, preferred_element_type=jnp.float32)
    partial_sum = partial_sum + lax.dot_general(
        up_grad, w_up, contract, preferred_element_type=jnp.float32
    )
    return lax.optimization_barrier(partial_sum.astype(jnp.bfloat16)).astype(jnp.float32)


def add_returns(grad_rows, returned, destination):
    token_count = grad_rows.shape[0]
    gathered = (
        jnp.take(returned, destination, axis=0)
        .reshape(token_count, -1, returned.shape[-1])
        .astype(jnp.float32)
    )
    return (grad_rows.astype(jnp.float32) + jnp.sum(gathered, axis=1)).astype(jnp.bfloat16)


def body(
    mixer_output_stream,
    layer_output_gradient,
    routes,
    expert_combine_weight,
    expert_gate_weight,
    expert_up_weight,
    expert_down_weight,
    head_mixer_input,
    head_step_size,
    head_decay_rate,
    extra_log_decay,
    state_entering_span,
    state_input_vectors,
    state_readout_vectors,
    gate_preactivation,
    group_norm_scale,
    mixer_output_weight,
):
    expert_count = lax.axis_size(SP)
    local_tokens = routes.shape[0]
    capacity = 3 * local_tokens // expert_count
    destination = slot_index(routes, expert_count, capacity)
    slot_table = build_table(destination, expert_count * capacity)
    w_gate = expert_gate_weight[0]
    w_up = expert_up_weight[0]
    w_down = expert_down_weight[0]
    sent_rows, sent_grads = pack_rows(
        mixer_output_stream, layer_output_gradient, slot_table, expert_combine_weight
    )
    part_rows, part_grads = (
        lax.all_to_all(
            sent_rows.reshape(expert_count, capacity, -1),
            SP,
            split_axis=0,
            concat_axis=0,
            tiled=True,
        ),
        lax.all_to_all(
            sent_grads.reshape(expert_count, capacity, -1),
            SP,
            split_axis=0,
            concat_axis=0,
            tiled=True,
        ),
    )
    routed_rows, routed_grads = (
        lax.all_gather(part_rows, "tp", axis=2, tiled=True),
        lax.all_gather(part_grads, "tp", axis=2, tiled=True),
    )
    model_width = routed_rows.shape[2]
    routed_rows = routed_rows.reshape(-1, model_width)
    routed_grads = routed_grads.reshape(-1, model_width)
    hidden, gate_grad, up_grad = expert_hidden(routed_rows, routed_grads, w_gate, w_up, w_down)
    grad_g, grad_u, grad_d = expert_weight_grads(
        routed_rows, routed_grads, hidden, gate_grad, up_grad
    )
    partial_rows = row_partial(gate_grad, up_grad, w_gate, w_up)
    summed = sum_at_owner(partial_rows.astype(jnp.bfloat16), "tp", 1)
    returned = lax.all_to_all(
        summed.astype(jnp.bfloat16).reshape(expert_count, capacity, -1),
        SP,
        split_axis=0,
        concat_axis=0,
        tiled=True,
    )
    own_cols = add_returns(
        layer_output_gradient, returned.reshape(expert_count * capacity, -1), destination
    )
    mix_grad = lax.all_gather(own_cols, "tp", axis=1, tiled=True)
    head_local = head_step_size.shape[1]
    group_local = state_input_vectors.shape[1] // STATE
    input_heads = head_mixer_input.astype(jnp.float32).reshape(local_tokens, head_local, HDIM)
    input_vector_groups = state_input_vectors.astype(jnp.float32).reshape(
        local_tokens, group_local, STATE
    )
    readout_groups = state_readout_vectors.astype(jnp.float32).reshape(
        local_tokens, group_local, STATE
    )
    within_span_state, within_span_decay = span_final_state(
        input_heads, head_step_size, head_decay_rate, extra_log_decay, input_vector_groups
    )
    identity_pair = (jnp.zeros_like(within_span_state), jnp.ones_like(within_span_decay))
    carry_in, carry_decay = prefix_by_axis(
        (within_span_state, within_span_decay), SP, join_spans, identity_pair
    )
    incoming_state = carry_in + carry_decay[:, None, None] * state_entering_span

    def forward(input_values, time_step_values, input_vector_entries, readout_entries):
        return span_local_scan(
            input_values,
            time_step_values,
            head_decay_rate,
            extra_log_decay,
            input_vector_entries,
            readout_entries,
            incoming_state,
        )

    (scan_out, closing_state), pull_back = jax.vjp(
        forward, input_heads, head_step_size, input_vector_groups, readout_groups
    )

    def apply_norm(scan_vals, gate_vals):
        return gate_norm(scan_vals, gate_vals, group_norm_scale, group_local)

    normed, pull_norm = jax.vjp(apply_norm, scan_out, gate_preactivation.astype(jnp.float32))
    normed_low = normed.astype(jnp.bfloat16)
    columns = mix_grad
    proj_grad = lax.psum_scatter(
        lax.dot_general(
            columns, normed_low, (((0,), (0,)), ((), ())), preferred_element_type=jnp.float32
        ).astype(jnp.bfloat16),
        SP,
        scatter_dimension=0,
        tiled=True,
    ).astype(jnp.float32)
    columns = mix_grad
    normed_grad = lax.dot_general(
        columns,
        lax.all_gather(mixer_output_weight, SP, axis=1, tiled=True),
        (((1,), (1,)), ((), ())),
        preferred_element_type=jnp.float32,
    )
    scanned_gradient, gate_grad_in = pull_norm(normed_grad)
    reached_gradient = carried_weight(
        scanned_gradient, readout_groups, head_step_size, head_decay_rate, extra_log_decay
    )
    later_grad, later_decay = prefix_by_axis_2(
        (reached_gradient, within_span_decay), SP, join_spans, identity_pair
    )
    input_grad, step_grad, b_grad, c_grad = pull_back((scanned_gradient, later_grad))
    return (
        grad_g[None],
        grad_u[None],
        grad_d[None],
        proj_grad.T,
        input_grad.reshape(local_tokens, -1).astype(jnp.bfloat16),
        step_grad,
        b_grad.reshape(local_tokens, -1).astype(jnp.bfloat16),
        c_grad.reshape(local_tokens, -1).astype(jnp.bfloat16),
        gate_grad_in.astype(jnp.bfloat16),
    )


def solution(mesh):
    finer = Mesh(mesh.devices.reshape(4, 4, 2, mesh.shape["tp"]), ("sp_0", "sp_1", "sp_2", "tp"))
    placed = (
        P(SP, "tp"),
        P(SP, "tp"),
        P(SP, None),
        P(SP, None),
        P(SP, None, "tp"),
        P(SP, None, "tp"),
        P(SP, "tp", None),
        P(SP, "tp"),
        P(SP, "tp"),
        P("tp"),
        P(SP, "tp"),
        P("tp", None, None),
        P(SP, "tp"),
        P(SP, "tp"),
        P(SP, "tp"),
        P("tp"),
        P("tp", SP),
    )
    return jax.shard_map(
        body,
        mesh=finer,
        in_specs=placed,
        out_specs=(
            P(SP, None, "tp"),
            P(SP, None, "tp"),
            P(SP, "tp", None),
            P("tp", SP),
            P(SP, "tp"),
            P(SP, "tp"),
            P(SP, "tp"),
            P(SP, "tp"),
            P(SP, "tp"),
        ),
        check_vma=False,
    )
```

profile of v0, /device:TPU:0, one launch (start us, length us, event | category | flops | bytes accessed | tf_op | source)
XLA Modules:
  0.0 358.2 jit_solution(8336922889193832031)
XLA Ops:
  11.9 2.4 all-reduce.2
  15.0 10.1 %all-gather.1 = bf16[4,1,16]{2,1,0:T(2,128)(2,1)S(1)} all-gather(bf16[1,1,16]{2,1,0:T(2,128)(2,1)S(1)} %convert_bitcast_fusion.10), channel_id=1, replica_groups=mesh['sp_0'=4,'sp_1'=4,'sp_2'=2,'tp'=4] {'sp_1'}, dimensions={0}, use_global_device_ids=true | all-gather | bytes 160 | tf_op jit(solution)/shard_map/all_gather | solution.py:41
  27.0 2.2 all_gather.62
  34.2 2.8 gather_fusion
  39.5 21.6 %all_to_all.20 = bf16[32,12,512]{2,1,0:T(8,128)(2,1)} all-to-all(bf16[32,12,512]{2,1,0:T(8,128)(2,1)S(1)} %reshape.899), channel_id=1, replica_groups=mesh['sp_0'=4,'sp_1'=4,'sp_2'=2,'tp'=4] {'sp_0','sp_1','sp_2'}, dimensions={0} | all-to-all | bytes 786432 | tf_op jit(solution)/shard_map/all_to_all | solution.py:269
  63.4 15.8 %all_to_all.21 = bf16[32,12,512]{2,1,0:T(8,128)(2,1)} all-to-all(bf16[32,12,512]{2,1,0:T(8,128)(2,1)S(1)} %reshape.896), channel_id=1, replica_groups=mesh['sp_0'=4,'sp_1'=4,'sp_2'=2,'tp'=4] {'sp_0','sp_1','sp_2'}, dimensions={0} | all-to-all | bytes 786432 | tf_op jit(solution)/shard_map/all_to_all | solution.py:262
  79.8 2.2 fusion.47
  83.2 7.9 %all-gather.2 = bf16[4,1,16]{2,1,0:T(2,128)(2,1)S(1)} all-gather(bf16[1,1,16]{2,1,0:T(2,128)(2,1)S(1)} %get-tuple-element.154), channel_id=1, replica_groups=mesh['sp_0'=4,'sp_1'=4,'sp_2'=2,'tp'=4] {'sp_0'}, dimensions={0}, use_global_device_ids=true | all-gather | bytes 160 | tf_op jit(solution)/shard_map/all_gather | solution.py:41
  94.2 2.5 reshape.900
  96.7 27.2 %all-gather.12.cloned.1.call-done = bf16[32,12,2048]{2,1,0:T(8,128)(2,1)} async-done(((bf16[32,12,512]{2,1,0:T(8,128)(2,1)}), bf16[32,12,2048]{2,1,0:T(8,128)(2,1)}) %all-gather.12.cloned.1.call-update) | async-done | bytes 1572880 | tf_op jit(solution)/shard_map/all_gather | solution.py:278
  124.0 3.6 %reshape.897 = bf16[384,2048]{1,0:T(8,128)(2,1)} reshape(bf16[32,12,2048]{2,1,0:T(8,128)(2,1)} %all-gather.12.cloned.1.call-done) | data formatting | bytes 3145728 | tf_op jit(solution)/shard_map/reshape | solution.py:282
  127.6 4.4 %fusion.2 = f32[384,896]{1,0:T(8,128)S(1)} fusion(bf16[384,2048]{1,0:T(8,128)(2,1)} %reshape.897, bf16[1,2048,896]{2,1,0:T(8,128)(2,1)} %param.23), kind=kOutput, calls=%fused_computation.8 | convolution fusion | flops 1409286144 | bytes 6619136 | tf_op jit(solution)/shard_map/dot_general | solution.py:189
  142.2 3.6 all-to-all-start.2
  146.6 3.8 %all-gather.18.cloned.1.call-done = bf16[4,16,64,128]{3,2,1,0:T(8,128)(2,1)} async-done(((bf16[1,16,64,128]{3,2,1,0:T(8,128)(2,1)}), bf16[4,16,64,128]{3,2,1,0:T(8,128)(2,1)}) %all-gather.18.cloned.1.call-update) | async-done | bytes 1048592 | tf_op jit(solution)/shard_map/all_gather | solution.py:41
  150.5 2.5 fusion.32
  153.0 13.5 %all-to-all-done.2 = bf16[4,384,512]{2,1,0:T(8,128)(2,1)S(1)} async-done(((bf16[4,384,512]{2,1,0:T(8,128)(2,1)}), bf16[4,384,512]{2,1,0:T(8,128)(2,1)S(1)}, u32[]{:S(2)}, u32[]{:S(2)}) %all-to-all-start.2) | async-done | bytes 1572896 | tf_op jit(solution)/shard_map/all_to_all | solution.py:25
  167.9 7.3 %all-to-all-start.3 = ((bf16[32,12,512]{2,1,0:T(8,128)(2,1)}), bf16[32,12,512]{2,1,0:T(8,128)(2,1)S(1)}, u32[]{:S(2)}, u32[]{:S(2)}) async-start(bf16[32,12,512]{2,1,0:T(8,128)(2,1)} %reshape.902), calls=%async_computation.3 | async-start | bytes 1048576 | tf_op jit(solution)/shard_map/all_to_all | solution.py:290
  175.9 2.2 fusion.14
  178.3 8.5 %all-to-all-done.3 = bf16[32,12,512]{2,1,0:T(8,128)(2,1)S(1)} async-done(((bf16[32,12,512]{2,1,0:T(8,128)(2,1)}), bf16[32,12,512]{2,1,0:T(8,128)(2,1)S(1)}, u32[]{:S(2)}, u32[]{:S(2)}) %all-to-all-start.3) | async-done | bytes 393248 | tf_op jit(solution)/shard_map/all_to_all | solution.py:290
  188.9 12.8 %all_gather.58 = bf16[128,2048]{1,0:T(8,128)(2,1)S(1)} all-gather(bf16[128,512]{1,0:T(8,128)(2,1)S(1)} %add_convert_fusion.3), channel_id=1, replica_groups=mesh['sp_0'=4,'sp_1'=4,'sp_2'=2,'tp'=4] {'tp'}, dimensions={1}, use_global_device_ids=true | all-gather | bytes 655360 | tf_op jit(solution)/shard_map/all_gather | solution.py:300
  201.7 3.0 fusion.153
  211.9 2.2 all_gather.67
  215.1 21.0 %all-gather.22.cloned.1.call-done = bf16[4,16,64,128]{3,2,1,0:T(8,128)(2,1)} async-done(((bf16[1,16,64,128]{3,2,1,0:T(8,128)(2,1)}), bf16[4,16,64,128]{3,2,1,0:T(8,128)(2,1)}) %all-gather.22.cloned.1.call-update) | async-done | bytes 1048592 | tf_op jit(solution)/shard_map/all_gather | solution.py:62
  236.1 2.2 add_convert_fusion.1
  238.4 3.3 convolution_convert_fusion
  242.3 10.3 %all-gather.3 = bf16[4,1,16]{2,1,0:T(2,128)(2,1)S(1)} all-gather(bf16[1,1,16]{2,1,0:T(2,128)(2,1)S(1)} %copy-done.79), channel_id=1, replica_groups=mesh['sp_0'=4,'sp_1'=4,'sp_2'=2,'tp'=4] {'sp_0'}, dimensions={0}, use_global_device_ids=true | all-gather | bytes 160 | tf_op jit(solution)/shard_map/all_gather | solution.py:62
  257.5 5.3 %convert_bitcast_fusion.1 = bf16[1,2048,896]{2,1,0:T(8,128)(2,1)} fusion(bf16[384,2048]{1,0:T(8,128)(2,1)S(1)} %copy-done.19, bf16[384,896]{1,0:T(8,128)(2,1)} %copy-done.100), kind=kOutput, calls=%fused_computation.17 | convolution fusion | flops 1411121152 | bytes 5931008 | tf_op jit(solution)/shard_map/dot_general | solution.py:207
  262.9 4.1 %convert_bitcast_fusion.2 = bf16[1,2048,896]{2,1,0:T(8,128)(2,1)} fusion(bf16[384,2048]{1,0:T(8,128)(2,1)S(1)} %copy-done.19, bf16[384,896]{1,0:T(8,128)(2,1)S(1)} %copy-done.95), kind=kOutput, calls=%fused_computation.18 | convolution fusion | flops 1411121152 | bytes 5931008 | tf_op jit(solution)/shard_map/dot_general | solution.py:206
  267.0 4.0 %convert_bitcast_fusion = bf16[1,896,2048]{2,1,0:T(8,128)(2,1)} fusion(bf16[384,2048]{1,0:T(8,128)(2,1)S(1)} %copy-done.17, f32[384,896]{1,0:T(8,128)S(1)} %copy-done.99, f32[384,896]{1,0:T(8,128)S(1)} %copy-done.97), kind=kOutput, calls=%fused_computation.16 | convolution fusion | flops 1413185536 | bytes 7995392 | tf_op jit(solution)/shard_map/dot_general | solution.py:208
  272.1 3.0 fusion.23
  280.2 2.3 fusion.66
  293.0 56.5 %reduce-scatter.2.cloned.1.call-done = bf16[64,1024]{1,0:T(8,128)(2,1)} async-done(((bf16[2048,1024]{1,0:T(8,128)(2,1)}), bf16[64,1024]{1,0:T(8,128)(2,1)}) %reduce-scatter.2.cloned.1.call-update) | async-done | bytes 131088 | tf_op jit(solution)/shard_map/reduce_scatter | solution.py:340
  (364 shorter events, 67.3 us)
Async XLA Ops:
  7.2 53.9 %copy-start = (bf16[128,512]{1,0:T(8,128)(2,1)S(1)}, bf16[128,512]{1,0:T(8,128)(2,1)}, u32[]{:S(2)}) copy-start(bf16[128,512]{1,0:T(8,128)(2,1)} %param.19) | copy-start | bytes 393220
  7.2 72.6 %all-gather.16.cloned.1.call-start = ((), (), s32[]{:S(2)}) async-start(), calls=%async_computation.7 | async-start | bytes 1310720 | tf_op jit(solution)/shard_map/all_gather | solution.py:41
  15.0 135.4 %copy-start.56 = (f32[16]{0:T(128)}, f32[16]{0:T(128)S(1)}, u32[]{:S(2)}) copy-start(f32[16]{0:T(128)S(1)} %get-tuple-element.169) | copy-start | bytes 196
  25.1 121.2 %copy-start.32 = (bf16[4,1,16]{2,1,0:T(2,128)(2,1)}, bf16[4,1,16]{2,1,0:T(2,128)(2,1)S(1)}, u32[]{:S(2)}) copy-start(bf16[4,1,16]{2,1,0:T(2,128)(2,1)S(1)} %all-gather.1) | copy-start | bytes 388
  26.6 64.6 %copy-start.20 = (bf16[128,2,128]{2,1,0:T(2,128)(2,1)}, bf16[128,2,128]{2,1,0:T(2,128)(2,1)S(1)}, u32[]{:S(2)}) copy-start(bf16[128,2,128]{2,1,0:T(2,128)(2,1)S(1)} %reshape.906) | copy-start | bytes 196612
  30.9 63.4 %all-gather.14.cloned.1.call-start = ((), (), s32[]{:S(2)}) async-start(), calls=%async_computation.6 | async-start | bytes 2621440 | tf_op jit(solution)/shard_map/all_gather | solution.py:279
  61.0 62.9 %all-gather.12.cloned.1.call-start = ((), (), s32[]{:S(2)}) async-start(), calls=%async_computation.5 | async-start | bytes 2621440 | tf_op jit(solution)/shard_map/all_gather | solution.py:278
  63.4 28.1 %copy-start.36 = (bf16[128,256]{1,0:T(8,128)(2,1)S(1)}, bf16[128,256]{1,0:T(8,128)(2,1)}, u32[]{:S(2)}) copy-start(bf16[128,256]{1,0:T(8,128)(2,1)} %param.32) | copy-start | bytes 196612
  79.2 71.2 %all-gather.18.cloned.1.call-start = ((), (), s32[]{:S(2)}) async-start(), calls=%async_computation.8 | async-start | bytes 1310720 | tf_op jit(solution)/shard_map/all_gather | solution.py:41
  79.8 70.7 %copy-start.44 = (f32[16]{0:T(128)}, f32[16]{0:T(128)S(1)}, u32[]{:S(2)}) copy-start(f32[16]{0:T(128)S(1)} %get-tuple-element.156) | copy-start | bytes 196
  79.8 70.7 %copy-start.47 = (f32[16]{0:T(128)}, f32[16]{0:T(128)S(1)}, u32[]{:S(2)}) copy-start(f32[16]{0:T(128)S(1)} %get-tuple-element.157) | copy-start | bytes 196
  82.1 119.7 %all-gather.20.cloned.1.call-start = ((), (), s32[]{:S(2)}) async-start(), calls=%async_computation.10 | async-start | bytes 4325376 | tf_op jit(solution)/shard_map/all_gather | solution.py:351
  91.3 55.0 %copy-start.26 = (bf16[128,2,128]{0,2,1:T(8,128)(2,1)}, bf16[128,2,128]{0,2,1:T(8,128)(2,1)S(1)}, u32[]{:S(2)}) copy-start(bf16[128,2,128]{0,2,1:T(8,128)(2,1)S(1)} %copy.271) | copy-start | bytes 196612
  91.5 83.9 %copy-start.22 = (bf16[128,2,128]{2,1,0:T(2,128)(2,1)}, bf16[128,2,128]{2,1,0:T(2,128)(2,1)S(1)}, u32[]{:S(2)}) copy-start(bf16[128,2,128]{2,1,0:T(2,128)(2,1)S(1)} %reshape.905) | copy-start | bytes 196612
  92.0 54.4 %copy-start.24 = (bf16[128,2,128]{0,2,1:T(8,128)(2,1)}, bf16[128,2,128]{0,2,1:T(8,128)(2,1)S(1)}, u32[]{:S(2)}) copy-start(bf16[128,2,128]{0,2,1:T(8,128)(2,1)S(1)} %copy.270) | copy-start | bytes 196612
  92.1 83.7 %copy-start.51 = (f32[2,8,128]{2,1,0:T(8,128)}, f32[2,8,128]{2,1,0:T(8,128)S(1)}, u32[]{:S(2)}) copy-start(f32[2,8,128]{2,1,0:T(8,128)S(1)} %copy.246) | copy-start | bytes 24580
  93.6 82.2 %copy-start.41 = (pred[128,128]{1,0:T(8,128)(4,1)}, pred[128,128]{1,0:T(8,128)(4,1)S(1)}, u32[]{:S(2)}) copy-start(pred[128,128]{1,0:T(8,128)(4,1)S(1)} %iota_compare_fusion) | copy-start | bytes 49156
  96.7 37.2 %copy-start.16 = (bf16[384,2048]{1,0:T(8,128)(2,1)}, bf16[384,2048]{1,0:T(8,128)(2,1)S(1)}, u32[]{:S(2)}) copy-start(bf16[384,2048]{1,0:T(8,128)(2,1)S(1)} %reshape.900) | copy-start | bytes 4718596
  142.2 24.3 %all-to-all-start.2 = ((bf16[4,384,512]{2,1,0:T(8,128)(2,1)}), bf16[4,384,512]{2,1,0:T(8,128)(2,1)S(1)}, u32[]{:S(2)}, u32[]{:S(2)}) async-start(bf16[4,384,512]{2,1,0:T(8,128)(2,1)} %bitcast.470), calls=%async_computation.2 | async-start | bytes 3145728 | tf_op jit(solution)/shard_map/all_to_all | solution.py:25
  146.4 29.4 %copy-start.38 = (f32[128,2,8]{0,2,1:T(8,128)}, f32[128,2,8]{0,2,1:T(8,128)S(1)}, u32[]{:S(2)}) copy-start(f32[128,2,8]{0,2,1:T(8,128)S(1)} %bitcast_exponential_fusion) | copy-start | bytes 24580
  146.6 29.2 %copy-start.29 = (f32[2,128,128]{2,1,0:T(8,128)}, f32[2,128,128]{2,1,0:T(8,128)S(1)}, u32[]{:S(2)}) copy-start(f32[2,128,128]{2,1,0:T(8,128)S(1)} %fusion.161) | copy-start | bytes 393220
  153.0 22.4 %copy-start.4 = (f32[16,64,128]{2,1,0:T(8,128)}, f32[16,64,128]{2,1,0:T(8,128)S(1)}, u32[]{:S(2)}) copy-start(f32[16,64,128]{2,1,0:T(8,128)S(1)} %fusion.32) | copy-start | bytes 1572868
  167.9 18.9 %all-to-all-start.3 = ((bf16[32,12,512]{2,1,0:T(8,128)(2,1)}), bf16[32,12,512]{2,1,0:T(8,128)(2,1)S(1)}, u32[]{:S(2)}, u32[]{:S(2)}) async-start(bf16[32,12,512]{2,1,0:T(8,128)(2,1)} %reshape.902), calls=%async_computation.3 | async-start | bytes 1048576 | tf_op jit(solution)/shard_map/all_to_all | solution.py:290
  175.1 60.9 %all-gather.22.cloned.1.call-start = ((), (), s32[]{:S(2)}) async-start(), calls=%async_computation.11 | async-start | bytes 1310720 | tf_op jit(solution)/shard_map/all_gather | solution.py:62
  211.4 24.6 %copy-start.45 = (f32[16]{0:T(128)S(1)}, f32[16]{0:T(128)}, u32[]{:S(2)}) copy-start(f32[16]{0:T(128)} %copy-done.44) | copy-start | bytes 196
  211.4 24.6 %copy-start.48 = (f32[16]{0:T(128)S(1)}, f32[16]{0:T(128)}, u32[]{:S(2)}) copy-start(f32[16]{0:T(128)} %copy-done.47) | copy-start | bytes 196
  211.4 24.6 %copy-start.58 = (f32[16]{0:T(128)S(1)}, f32[16]{0:T(128)}, u32[]{:S(2)}) copy-start(f32[16]{0:T(128)} %get-tuple-element.152) | copy-start | bytes 196
  211.4 24.6 %copy-start.60 = (f32[16]{0:T(128)S(1)}, f32[16]{0:T(128)}, u32[]{:S(2)}) copy-start(f32[16]{0:T(128)} %get-tuple-element.155) | copy-start | bytes 196
  211.9 26.5 %copy-start.40 = (f32[1024]{0:T(1024)S(1)}, f32[1024]{0:T(1024)}, u32[]{:S(2)}) copy-start(f32[1024]{0:T(1024)} %param.34) | copy-start | bytes 12292
  215.0 65.1 %all-gather.24.cloned.1.call-start = ((), (), s32[]{:S(2)}) async-start(), calls=%async_computation.12 | async-start | bytes 1310720 | tf_op jit(solution)/shard_map/all_gather | solution.py:62
  238.3 111.2 %reduce-scatter.2.cloned.1.call-start = ((), (), s32[]{:S(2)}) async-start(), calls=%async_computation.9 | async-start | bytes 4325376 | tf_op jit(solution)/shard_map/reduce_scatter | solution.py:340
  289.9 61.2 %copy-start.1 = (bf16[128,512]{1,0:T(8,128)(2,1)S(1)}, bf16[128,512]{1,0:T(8,128)(2,1)}, u32[]{:S(2)}) copy-start(bf16[128,512]{1,0:T(8,128)(2,1)} %param.19) | copy-start | bytes 393220
  (79 other events, 307.6 us)
Sparse Core Ops, SparseCore 0:
  31.0 28.0 all-gather.15
  61.2 30.3 all-gather.13
  93.2 30.7 all-gather.11
  126.1 24.3 all-gather.17
  152.6 46.5 all-gather.19
  215.2 20.8 all-gather.21
  238.4 24.6 all-gather.23
  266.8 82.7 reduce-scatter.1
where the time goes:
time: 365 us; the launch traced here: 358 us
  waiting for transfers between devices  131 us (36%)
  blocking collectives  85.3 us (23%)
  matrix products  42.4 us (12%)
  local copies, waits for them, and re-layouts  38.9 us (11%)
  other arithmetic  32.4 us (9%)
  between operations  16.8 us (5%)
  starting transfers between devices  11.4 us (3%)
    reduce_scatter x1, waiting for transfers between devices, body(): lax.psum_scatter(lax.dot_general(columns, normed_low, (((0,), (0,)), ((),...  56.5 us
    all_gather x1, waiting for transfers between devices, body(): lax.all_gather(part_rows, 'tp', axis=2, tiled=True)  27.2 us
    all_to_all x1, blocking collectives, body(): lax.all_to_all(sent_grads.reshape(expert_count, capacity, -1), SP, split_...  21.6 us
    all_gather x2, waiting for transfers between devices, prefix_by_axis_2(): lax.all_gather(part.astype(kind), axis)  21 us
    all_gather x3, blocking collectives, prefix_by_axis(): lax.all_gather(part.astype(kind), axis)  20.2 us
    all_to_all x1, blocking collectives, body(): lax.all_to_all(sent_rows.reshape(expert_count, capacity, -1), SP, split_a...  15.8 us
    all_to_all x1, waiting for transfers between devices, sum_at_owner(): blocks = lax.all_to_all(split_up(x, dim, length), axis, 0, 0, tiled=True)  13.5 us
    all_gather x1, blocking collectives, body(): mix_grad = lax.all_gather(own_cols, 'tp', axis=1, tiled=True)  12.8 us
  transfers between devices with their start and end apart: 10, of which 6 were waited for; matrix products, arithmetic and copies ran while one was open for 25% of the time, Pallas kernels for 0%

commit v1 on v0

v1 whole, which is shorter than its diff:
```python
import functools

import jax
import jax.numpy as jnp
from jax import lax
from jax.experimental import pallas as pl
from jax.experimental.pallas import tpu as pltpu
from jax.sharding import PartitionSpec as P

HDIM = 64
STATE = 128
BLK = 128
SP = "sp"
CAP = 12
MESH = pl.DeviceIdType.MESH
F32 = jnp.float32
BF16 = jnp.bfloat16

norm_eps = 1e-05
exact_mode = lax.Precision.HIGHEST
VMEM_BYTES = 60 * 1024 * 1024


def vmem_spec():
    return pl.BlockSpec(memory_space=pltpu.VMEM)


def any_spec():
    return pl.BlockSpec(memory_space=pl.ANY)


def dot(a, b, contract=((1,), (0,))):
    return lax.dot_general(a, b, (contract, ((), ())), preferred_element_type=F32)


def iota(shape, dim):
    return lax.broadcasted_iota(jnp.int32, shape, dim)


def divide(x, by):
    return ((x.astype(F32) + 0.5) * (1.0 / by)).astype(jnp.int32)


def slots_in_rows(routes, experts):
    top, tokens = routes.shape
    ids = iota((experts, tokens), 0)
    earlier = (iota((tokens, tokens), 0) < iota((tokens, tokens), 1)).astype(BF16)
    before = jnp.zeros((experts, 1), F32)
    rows = []
    for k in range(top):
        hits = (ids == routes[k : k + 1, :]).astype(F32)
        rank = dot(hits.astype(BF16), earlier) + before
        rows.append(jnp.sum(hits * rank, axis=0, keepdims=True))
        before = before + jnp.sum(hits, axis=1, keepdims=True)
    return [routes[k : k + 1, :] * CAP + rows[k].astype(jnp.int32) for k in range(top)]


def slots_in_columns(routes, experts):
    tokens, top = routes.shape
    ids = iota((tokens, experts), 1)
    earlier = (iota((tokens, tokens), 1) < iota((tokens, tokens), 0)).astype(BF16)
    before = jnp.zeros((1, experts), F32)
    columns = []
    for k in range(top):
        hits = (ids == routes[:, k : k + 1]).astype(F32)
        rank = dot(earlier, hits.astype(BF16)) + before
        columns.append(jnp.sum(hits * rank, axis=1, keepdims=True))
        before = before + jnp.sum(hits, axis=0, keepdims=True)
    return [routes[:, k : k + 1] * CAP + columns[k].astype(jnp.int32) for k in range(top)]


def pack_kernel(experts, routes_ref, weights_ref, stream_ref, grads_ref, out_ref):
    tokens = stream_ref.shape[0]
    half = stream_ref.shape[1] // 2
    slots = slots_in_rows(routes_ref[...], experts)
    row = iota((experts * 4 * CAP, 1), 0)
    expert = divide(row, 4 * CAP)
    inner = row - expert * (4 * CAP)
    part = divide(inner, CAP)
    slot = expert * CAP + inner - part * CAP
    first = (slot == slots[0]).astype(F32)
    second = (slot == slots[1]).astype(F32)
    match = (first + second).astype(BF16)
    weight = jnp.sum(
        first * weights_ref[0:1, :] + second * weights_ref[1:2, :], axis=1, keepdims=True
    )
    x0 = dot(match, stream_ref[:, :half])
    x1 = dot(match, stream_ref[:, half:])
    g0 = dot(match, grads_ref[:, :half])
    g1 = dot(match, grads_ref[:, half:])
    low = jnp.where(part == 0, x0, g0 * weight)
    high = jnp.where(part == 2, x1, g1 * weight)
    out_ref[...] = jnp.where(part < 2, low, high).astype(BF16)


def pack(routes, weights, stream, grads, experts):
    half = stream.shape[1] // 2
    packed = pl.pallas_call(
        functools.partial(pack_kernel, experts),
        out_shape=jax.ShapeDtypeStruct((experts * 4 * CAP, half), BF16),
        in_specs=[vmem_spec()] * 4,
        out_specs=vmem_spec(),
        compiler_params=pltpu.CompilerParams(vmem_limit_bytes=VMEM_BYTES),
        name="pack",
    )(routes.T, weights.T, stream, grads)
    return packed.reshape(experts, 4 * CAP, half)


def greet(me, tp, n_sp, n_tp, step=1, ring=False, partner=None):
    barrier = pltpu.get_barrier_semaphore()

    def hello(d, carry):
        pl.semaphore_signal(
            barrier, inc=1, device_id=(lax.rem(me + d * step, n_sp), tp), device_id_type=MESH
        )
        return carry

    lax.fori_loop(1, n_sp // step, hello, 0)
    count = n_sp // step - 1
    if partner is not None:
        pl.semaphore_signal(barrier, inc=1, device_id=(partner, tp), device_id_type=MESH)
        count += 1
    if ring:
        for other in (lax.rem(tp + 1, n_tp), lax.rem(tp + n_tp - 1, n_tp)):
            pl.semaphore_signal(barrier, inc=1, device_id=(me, other), device_id_type=MESH)
        count += 2
    pl.semaphore_wait(barrier, count)


def dispatch_kernel(
    n_sp, n_tp, in_ref, out_ref, own, a_send, a_recv, s_right, s_left, r_left, r_right, f_send, f_recv
):
    me, tp = lax.axis_index("sp"), lax.axis_index("tp")
    right, left = lax.rem(tp + 1, n_tp), lax.rem(tp + n_tp - 1, n_tp)
    far = lax.rem(tp + 2, n_tp)
    greet(me, tp, n_sp, n_tp, ring=True)

    def origin(d):
        return lax.rem(me + n_sp - d, n_sp)

    def exchange(d):
        to = lax.rem(me + d, n_sp)
        return pltpu.make_async_remote_copy(
            in_ref.at[to], out_ref.at[tp, me], a_send.at[d], a_recv.at[d], (to, tp), MESH
        )

    def arrived(d):
        return pltpu.make_async_remote_copy(
            in_ref.at[me], out_ref.at[tp, origin(d)], a_send.at[d], a_recv.at[d], (me, tp), MESH
        )

    def to_right(d, block):
        piece = out_ref.at[block, origin(d)]
        return pltpu.make_async_remote_copy(
            piece, piece, s_right.at[d], r_left.at[d], (me, right), MESH
        )

    def to_left(d, block):
        piece = out_ref.at[block, origin(d)]
        return pltpu.make_async_remote_copy(
            piece, piece, s_left.at[d], r_right.at[d], (me, left), MESH
        )

    def onward(d, block, to):
        piece = out_ref.at[block, origin(d)]
        return pltpu.make_async_remote_copy(
            piece, piece, f_send.at[d], f_recv.at[d], (me, to), MESH
        )

    def start_exchange(d, carry):
        exchange(d).start()
        return carry

    lax.fori_loop(1, n_sp, start_exchange, 0)
    mine = pltpu.make_async_copy(in_ref.at[me], out_ref.at[tp, me], own)
    mine.start()
    mine.wait()
    to_right(0, tp).start()
    to_left(0, tp).start()

    def spread(d, carry):
        arrived(d).wait_recv()
        to_right(d, tp).start()
        to_left(d, tp).start()
        return carry

    lax.fori_loop(1, n_sp, spread, 0)

    def relay(q, carry):
        d = 2 * q
        to_right(d, left).wait_recv()
        onward(d, left, right).start()
        to_left(d + 1, right).wait_recv()
        onward(d + 1, right, left).start()
        return carry

    lax.fori_loop(0, n_sp // 2, relay, 0)

    def finish(q, carry):
        d = 2 * q
        to_left(d, right).wait_recv()
        to_right(d + 1, left).wait_recv()
        onward(d, far, right).wait()
        onward(d + 1, far, left).wait()
        to_right(d, tp).wait_send()
        to_left(d, tp).wait_send()
        to_right(d + 1, tp).wait_send()
        to_left(d + 1, tp).wait_send()
        return carry

    lax.fori_loop(0, n_sp // 2, finish, 0)

    def drain(d, carry):
        exchange(d).wait_send()
        return carry

    lax.fori_loop(1, n_sp, drain, 0)


def dispatch(packed, n_sp, n_tp):
    dma = pltpu.SemaphoreType.DMA
    return pl.pallas_call(
        functools.partial(dispatch_kernel, n_sp, n_tp),
        out_shape=jax.ShapeDtypeStruct((n_tp,) + packed.shape, BF16),
        in_specs=[vmem_spec()],
        out_specs=vmem_spec(),
        scratch_shapes=[dma] + [dma((n_sp,))] * 8,
        compiler_params=pltpu.CompilerParams(
            collective_id=0, has_side_effects=True, vmem_limit_bytes=VMEM_BYTES
        ),
        name="dispatch",
    )(packed)


def return_kernel(
    n_sp,
    n_tp,
    part_ref,
    routes_ref,
    grads_ref,
    mix_ref,
    from_left,
    from_right,
    sum_right,
    sum_left,
    out_blocks,
    back,
    own_cols,
    s_r,
    s_l,
    r_l,
    r_r,
    a_send,
    a_recv,
    g_send,
    g_recv,
    local,
):
    me, tp = lax.axis_index("sp"), lax.axis_index("tp")
    right, left = lax.rem(tp + 1, n_tp), lax.rem(tp + n_tp - 1, n_tp)
    far = lax.rem(tp + 2, n_tp)
    tokens, width = grads_ref.shape
    half, quarter = width // 2, width // 4
    greet(me, tp, n_sp, n_tp, ring=True)

    def block(b, which):
        return part_ref.at[:, pl.ds(pl.multiple_of(b * width + which * half, half), half)]

    def right_copy(k, src):
        return pltpu.make_async_remote_copy(
            src, from_left.at[k], s_r.at[k], r_l.at[k], (me, right), MESH
        )

    def left_copy(k, src):
        return pltpu.make_async_remote_copy(
            src, from_right.at[k], s_l.at[k], r_r.at[k], (me, left), MESH
        )

    right_copy(0, block(far, 0)).start()
    left_copy(0, block(far, 1)).start()
    right_copy(1, block(right, 1)).start()
    left_copy(1, block(left, 0)).start()

    slots = slots_in_columns(routes_ref[...], n_sp)
    column = iota((1, n_sp * 4 * CAP), 1)
    expert = divide(column, 4 * CAP)
    inner = column - expert * (4 * CAP)
    piece = divide(inner, CAP)
    slot = expert * CAP + inner - piece * CAP
    match = (slots[0] == slot) | (slots[1] == slot)

    right_copy(0, block(far, 0)).wait()
    sum_right[...] = (
        block(right, 0)[...].astype(F32) + from_left[0].astype(F32)
    ).astype(BF16)
    right_copy(2, sum_right).start()
    left_copy(0, block(far, 1)).wait()
    sum_left[...] = (
        block(left, 1)[...].astype(F32) + from_right[0].astype(F32)
    ).astype(BF16)
    left_copy(2, sum_left).start()
    right_copy(1, block(right, 1)).wait()
    left_copy(1, block(left, 0)).wait()
    right_copy(2, sum_right).wait()
    left_copy(2, sum_left).wait()

    rows = part_ref.shape[0]
    group_of = 8
    span = group_of * CAP
    wide = iota((group_of * 4 * CAP, 1), 0)
    wide_src = divide(wide, 4 * CAP)
    wide_in = wide - wide_src * (4 * CAP)
    wide_piece = divide(wide_in, CAP)
    wide_row = wide_src * CAP + wide_in - wide_piece * CAP
    spots = iota((1, span), 1)
    place = [((wide_row == spots) & (wide_piece == c)).astype(BF16) for c in range(4)]
    for g in range(rows // span):
        at = slice(g * span, (g + 1) * span)
        low = (
            block(tp, 0)[at, :].astype(F32)
            + from_left[2, at, :].astype(F32)
            + from_right[1, at, :].astype(F32)
        ).astype(BF16)
        high = (
            block(tp, 1)[at, :].astype(F32)
            + from_right[2, at, :].astype(F32)
            + from_left[1, at, :].astype(F32)
        ).astype(BF16)
        laid = (
            dot(place[0], low[:, :quarter])
            + dot(place[1], low[:, quarter:])
            + dot(place[2], high[:, :quarter])
            + dot(place[3], high[:, quarter:])
        )
        out_blocks[g * group_of : (g + 1) * group_of] = laid.astype(BF16).reshape(
            group_of, 4 * CAP, quarter
        )

    def exchange(d):
        to = lax.rem(me + d, n_sp)
        return pltpu.make_async_remote_copy(
            out_blocks.at[to], back.at[me], a_send.at[d], a_recv.at[d], (to, tp), MESH
        )

    def start_exchange(d, carry):
        exchange(d).start()
        return carry

    lax.fori_loop(1, n_sp, start_exchange, 0)
    mine = pltpu.make_async_copy(out_blocks.at[me], back.at[me], local)
    mine.start()
    mine.wait()

    def finish_exchange(d, carry):
        exchange(d).wait()
        return carry

    lax.fori_loop(1, n_sp, finish_exchange, 0)
    returned = back[...].reshape(n_sp * 4 * CAP, quarter)
    for c in range(4):
        chosen = jnp.where(match & (piece == c), 1.0, 0.0).astype(BF16)
        cols = slice(c * quarter, (c + 1) * quarter)
        own_cols[:, cols] = (grads_ref[:, cols].astype(F32) + dot(chosen, returned)).astype(BF16)

    def spot(b):
        return mix_ref.at[:, pl.ds(pl.multiple_of(b * width, width), width)]

    def spot_half(b, which):
        return mix_ref.at[:, pl.ds(pl.multiple_of(b * width + which * half, half), half)]

    def gather(k, src, dst, to):
        return pltpu.make_async_remote_copy(
            src, dst, g_send.at[k], g_recv.at[k], (me, to), MESH
        )

    gather(0, own_cols, spot(tp), right).start()
    gather(1, own_cols, spot(tp), left).start()
    spot(tp)[...] = own_cols[...]
    gather(0, own_cols, spot(left), right).wait_recv()
    gather(2, spot_half(left, 0), spot_half(left, 0), right).start()
    gather(1, own_cols, spot(right), left).wait_recv()
    gather(3, spot_half(right, 1), spot_half(right, 1), left).start()
    gather(2, spot_half(far, 0), spot_half(far, 0), right).wait()
    gather(3, spot_half(far, 1), spot_half(far, 1), left).wait()
    gather(0, own_cols, spot(tp), right).wait_send()
    gather(1, own_cols, spot(tp), left).wait_send()


def give_back(partial_rows, routes, grads, n_sp, n_tp):
    rows = partial_rows.shape[0]
    tokens, width = grads.shape
    half, quarter = width // 2, width // 4
    dma = pltpu.SemaphoreType.DMA
    return pl.pallas_call(
        functools.partial(return_kernel, n_sp, n_tp),
        out_shape=jax.ShapeDtypeStruct((tokens, width * n_tp), BF16),
        in_specs=[vmem_spec()] * 3,
        out_specs=vmem_spec(),
        scratch_shapes=[
            pltpu.VMEM((3, rows, half), BF16),
            pltpu.VMEM((3, rows, half), BF16),
            pltpu.VMEM((rows, half), BF16),
            pltpu.VMEM((rows, half), BF16),
            pltpu.VMEM((n_sp, 4 * CAP, quarter), BF16),
            pltpu.VMEM((n_sp, 4 * CAP, quarter), BF16),
            pltpu.VMEM((tokens, width), BF16),
            dma((3,)),
            dma((3,)),
            dma((3,)),
            dma((3,)),
            dma((n_sp,)),
            dma((n_sp,)),
            dma((4,)),
            dma((4,)),
            dma,
        ],
        compiler_params=pltpu.CompilerParams(
            collective_id=1, has_side_effects=True, vmem_limit_bytes=VMEM_BYTES
        ),
        name="give_back",
    )(partial_rows, routes, grads)


def carry_kernel(
    n_sp, n_tp, reverse, state_ref, decay_ref, first_ref, out_ref, states, decays, carries, one, two, sends, recvs, d_sends, d_recvs, b_sends, b_recvs
):
    me, tp = lax.axis_index("sp"), lax.axis_index("tp")
    greet(me, tp, n_sp, n_tp)

    def state_copy(d):
        to = lax.rem(me + d, n_sp)
        return pltpu.make_async_remote_copy(
            state_ref.at[to], states.at[me], sends.at[d], recvs.at[d], (to, tp), MESH
        )

    def decay_copy(d):
        to = lax.rem(me + d, n_sp)
        return pltpu.make_async_remote_copy(
            decay_ref.at[to], decays.at[me], d_sends.at[d], d_recvs.at[d], (to, tp), MESH
        )

    def back_copy(d):
        to = lax.rem(me + d, n_sp)
        return pltpu.make_async_remote_copy(
            carries.at[to], out_ref.at[me], b_sends.at[d], b_recvs.at[d], (to, tp), MESH
        )

    def start(d, carry):
        decay_copy(d).start()
        state_copy(d).start()
        return carry

    def finish(d, carry):
        decay_copy(d).wait()
        state_copy(d).wait()
        return carry

    lax.fori_loop(1, n_sp, start, 0)
    mine = pltpu.make_async_copy(state_ref.at[me], states.at[me], one)
    mine_too = pltpu.make_async_copy(decay_ref.at[me], decays.at[me], two)
    mine.start()
    mine_too.start()
    mine.wait()
    mine_too.wait()
    lax.fori_loop(1, n_sp, finish, 0)
    running = first_ref[...]
    for step in range(n_sp):
        i = n_sp - 1 - step if reverse else step
        carries[i] = running.astype(BF16)
        running = decays[i] * running + states[i].astype(F32)

    def start_back(d, carry):
        back_copy(d).start()
        return carry

    def finish_back(d, carry):
        back_copy(d).wait()
        return carry

    lax.fori_loop(1, n_sp, start_back, 0)
    mine = pltpu.make_async_copy(carries.at[me], out_ref.at[me], one)
    mine.start()
    mine.wait()
    lax.fori_loop(1, n_sp, finish_back, 0)


def carried(state, decay, first, n_sp, n_tp, reverse, identity):
    heads, channels, entries = state.shape
    rows = heads * channels // n_sp
    state = state.reshape(n_sp, rows, entries).astype(BF16)
    decay = jnp.broadcast_to(
        jnp.repeat(decay, channels // rows)[:, None, None], (n_sp, 1, entries)
    ) + jnp.zeros((n_sp, 1, entries), F32)
    dma = pltpu.SemaphoreType.DMA
    out = pl.pallas_call(
        functools.partial(carry_kernel, n_sp, n_tp, reverse),
        out_shape=jax.ShapeDtypeStruct((n_sp, rows, entries), BF16),
        in_specs=[vmem_spec()] * 3,
        out_specs=vmem_spec(),
        scratch_shapes=[
            pltpu.VMEM((n_sp, rows, entries), BF16),
            pltpu.VMEM((n_sp, 1, entries), F32),
            pltpu.VMEM((n_sp, rows, entries), BF16),
            dma,
            dma,
        ]
        + [dma((n_sp,))] * 6,
        compiler_params=pltpu.CompilerParams(
            collective_id=identity, has_side_effects=True, vmem_limit_bytes=VMEM_BYTES
        ),
        name="carry_back" if reverse else "carry",
    )(state, decay, first)
    return out.reshape(heads, channels, entries).astype(F32)


def proj_kernel(
    n_sp, n_tp, normed_ref, mix_ref, out_ref, normed2, mix2, parts, landed, total, other, p_send, p_recv, a_send, a_recv
):
    me, tp = lax.axis_index("sp"), lax.axis_index("tp")
    core = lax.rem(me, 2)
    partner = me + 1 - 2 * core
    chip = lax.div(me, 2)
    chips = n_sp // 2
    half = normed_ref.shape[1] // 2
    cols = out_ref.shape[1]
    greet(me, tp, n_sp, n_tp, step=2, partner=partner)

    def pair(k, src, dst):
        return pltpu.make_async_remote_copy(
            src, dst, p_send.at[k], p_recv.at[k], (partner, tp), MESH
        )

    def mine(c):
        return pl.ds(pl.multiple_of(c * half, half), half)

    pair(0, normed_ref.at[:, mine(1 - core)], normed2).start()
    pair(1, mix_ref, mix2).start()
    pair(0, normed_ref.at[:, mine(1 - core)], normed2).wait()
    pair(1, mix_ref, mix2).wait()
    for c in range(chips):
        at = slice(c * 2 * cols, (c + 1) * 2 * cols)
        parts[c] = (
            dot(normed_ref[:, mine(core)], mix_ref[:, at], ((0,), (0,)))
            + dot(normed2[...], mix2[:, at], ((0,), (0,)))
        ).astype(BF16)

    def exchange(d):
        to = lax.rem(chip + d, chips)
        return pltpu.make_async_remote_copy(
            parts.at[to], landed.at[chip], a_send.at[d], a_recv.at[d], (2 * to + core, tp), MESH
        )

    def start(d, carry):
        exchange(d).start()
        return carry

    lax.fori_loop(1, chips, start, 0)
    total[...] = parts[chip].astype(F32)

    def finish(d, carry):
        exchange(d).wait()
        total[...] += landed[lax.rem(chip + chips - d, chips)].astype(F32)
        return carry

    lax.fori_loop(1, chips, finish, 0)
    pair(2, total, other).start()
    out_ref[mine(core), :] = jnp.where(core == 0, total[:, :cols], total[:, cols:])
    pair(2, total, other).wait()
    out_ref[mine(1 - core), :] = jnp.where(core == 0, other[:, :cols], other[:, cols:])


def project(normed_low, mix, n_sp, n_tp):
    tokens, channels = normed_low.shape
    width = mix.shape[1]
    half = channels // 2
    chips = n_sp // 2
    cols = width // n_sp
    dma = pltpu.SemaphoreType.DMA
    return pl.pallas_call(
        functools.partial(proj_kernel, n_sp, n_tp),
        out_shape=jax.ShapeDtypeStruct((channels, cols), F32),
        in_specs=[vmem_spec()] * 2,
        out_specs=vmem_spec(),
        scratch_shapes=[
            pltpu.VMEM((tokens, half), BF16),
            pltpu.VMEM((tokens, width), BF16),
            pltpu.VMEM((chips, half, 2 * cols), BF16),
            pltpu.VMEM((chips, half, 2 * cols), BF16),
            pltpu.VMEM((half, 2 * cols), F32),
            pltpu.VMEM((half, 2 * cols), F32),
            dma((3,)),
            dma((3,)),
            dma((chips,)),
            dma((chips,)),
        ],
        compiler_params=pltpu.CompilerParams(
            collective_id=4, has_side_effects=True, vmem_limit_bytes=VMEM_BYTES
        ),
        name="project",
    )(normed_low, mix)


def expert_kernel(steps, in_ref, gate_ref, up_ref, down_ref, dgate_ref, dup_ref, ddown_ref, rows_ref, x, g, acc):
    step = pl.program_id(0)
    n_tp, n_sp, tall, half = in_ref.shape
    rows = n_sp * CAP

    @pl.when(step == 0)
    def _():
        group_of = 8
        span = group_of * CAP
        spots = iota((1, group_of * tall), 1)
        src = divide(spots, tall)
        inner = spots - src * tall
        part = divide(inner, CAP)
        row = src * CAP + inner - part * CAP
        mine = iota((span, 1), 0)
        pick = [((row == mine) & (part == p)).astype(BF16) for p in range(4)]
        for t in range(n_tp):
            for k in range(n_sp // group_of):
                block = in_ref[t, k * group_of : (k + 1) * group_of].reshape(
                    group_of * tall, half
                )
                at = slice(k * span, (k + 1) * span)
                for c in range(2):
                    cols = slice((2 * t + c) * half, (2 * t + c + 1) * half)
                    x[at, cols] = dot(pick[2 * c], block).astype(BF16)
                    g[at, cols] = dot(pick[2 * c + 1], block).astype(BF16)
        acc[...] = jnp.zeros_like(acc)

    w_gate, w_up, w_down = gate_ref[0], up_ref[0], down_ref[0]
    pre_gate = dot(x[...], w_gate)
    pre_up = dot(x[...], w_up)
    hidden_grad = dot(g[...], w_down, ((1,), (1,)))
    sigmoid_gate = jax.nn.sigmoid(pre_gate)
    activated = pre_gate * sigmoid_gate
    hidden = (activated * pre_up).astype(BF16)
    gate_grad = (
        hidden_grad * pre_up * sigmoid_gate * (1.0 + pre_gate * (1.0 - sigmoid_gate))
    ).astype(BF16)
    up_grad = (hidden_grad * activated).astype(BF16)
    over_rows = ((0,), (0,))
    dgate_ref[0] = dot(x[...], gate_grad, over_rows).astype(BF16)
    dup_ref[0] = dot(x[...], up_grad, over_rows).astype(BF16)
    ddown_ref[0] = dot(hidden, g[...], over_rows).astype(BF16)
    acc[...] += dot(gate_grad, w_gate, ((1,), (1,))) + dot(up_grad, w_up, ((1,), (1,)))

    @pl.when(step == steps - 1)
    def _():
        rows_ref[...] = acc[...].astype(BF16)


def experts_backward(arrived, w_gate, w_up, w_down):
    n_tp, n_sp, tall, half = arrived.shape
    _, width, hidden = w_gate.shape
    rows = n_sp * CAP
    tile = 128
    steps = hidden // tile
    by_col = pl.BlockSpec((1, width, tile), lambda j: (0, 0, j))
    by_row = pl.BlockSpec((1, tile, width), lambda j: (0, j, 0))
    return pl.pallas_call(
        functools.partial(expert_kernel, steps),
        grid=(steps,),
        out_shape=(
            jax.ShapeDtypeStruct(w_gate.shape, BF16),
            jax.ShapeDtypeStruct(w_up.shape, BF16),
            jax.ShapeDtypeStruct(w_down.shape, BF16),
            jax.ShapeDtypeStruct((rows, width), BF16),
        ),
        in_specs=[
            pl.BlockSpec(arrived.shape, lambda j: (0, 0, 0, 0)),
            by_col,
            by_col,
            by_row,
        ],
        out_specs=(by_col, by_col, by_row, pl.BlockSpec((rows, width), lambda j: (0, 0))),
        scratch_shapes=[
            pltpu.VMEM((rows, width), BF16),
            pltpu.VMEM((rows, width), BF16),
            pltpu.VMEM((rows, width), F32),
        ],
        compiler_params=pltpu.CompilerParams(vmem_limit_bytes=VMEM_BYTES),
        name="experts",
    )(arrived, w_gate, w_up, w_down)


def span_local_scan(
    input_heads,
    time_step,
    decay_speed,
    sudden_decay,
    input_vector_groups,
    readout_groups,
    starting_state,
):
    length, head_count, head_size = input_heads.shape
    groups, state_size = (input_vector_groups.shape[1], input_vector_groups.shape[2])
    per_group = head_count // groups
    block_count = length // BLK
    log_decay_total = sudden_decay - time_step * decay_speed[None, :]
    scaled = (input_heads * time_step[:, :, None]).reshape(
        block_count, BLK, groups, per_group, head_size
    )
    log_decay_total = log_decay_total.reshape(block_count, BLK, groups, per_group)
    b_rows = input_vector_groups.reshape(block_count, BLK, groups, state_size)
    c_rows = readout_groups.reshape(block_count, BLK, groups, state_size)
    cumulative = jnp.cumsum(log_decay_total, axis=1)
    causal_mask = jnp.tril(jnp.ones((BLK, BLK), dtype=bool))
    cum_t = jnp.moveaxis(cumulative, 1, -1)
    gaps = cum_t[..., :, None] - cum_t[..., None, :]
    decays = jnp.where(causal_mask, jnp.exp(jnp.where(causal_mask, gaps, 0.0)), 0.0)
    affinity = jnp.einsum("blgn,bsgn->bgls", c_rows, b_rows, precision=exact_mode)
    y_diag = jnp.einsum(
        "bghls,bsghp->blghp", affinity[:, :, None] * decays, scaled, precision=exact_mode
    )
    to_end = jnp.exp(cumulative[:, -1:] - cumulative)
    states = jnp.einsum(
        "blgn,blghp->bghpn", b_rows, scaled * to_end[..., None], precision=exact_mode
    )
    block_decay = jnp.exp(cumulative[:, -1])

    def advance(running, inputs):
        block_state, decay_now = inputs
        return (decay_now[..., None, None] * running + block_state, running)

    first_state = starting_state.reshape(groups, per_group, head_size, state_size)
    closing_state, incoming_state = lax.scan(advance, first_state, (states, block_decay))
    y_off = (
        jnp.einsum("blgn,bghpn->blghp", c_rows, incoming_state, precision=exact_mode)
        * jnp.exp(cumulative)[..., None]
    )
    result_rows = (y_diag + y_off).reshape(length, head_count, head_size)
    return (result_rows, closing_state.reshape(head_count, head_size, state_size))


def span_final_state(input_heads, time_step, decay_speed, sudden_decay, input_vector_groups):
    length, head_count, head_size = input_heads.shape
    groups = input_vector_groups.shape[1]
    log_decay_total = sudden_decay - time_step * decay_speed[None, :]
    sum_total = jnp.sum(log_decay_total, axis=0)
    after = sum_total[None, :] - jnp.cumsum(log_decay_total, axis=0)
    weighted = (input_heads * (time_step * jnp.exp(after))[:, :, None]).reshape(
        length, groups, head_count // groups, head_size
    )
    result = jnp.einsum("tgn,tghp->ghpn", input_vector_groups, weighted, precision=exact_mode)
    return (result.reshape(head_count, head_size, -1), jnp.exp(sum_total))


def carried_weight(scanned_gradient, readout_groups, time_step, decay_speed, sudden_decay):
    length, head_count, head_size = scanned_gradient.shape
    groups = readout_groups.shape[1]
    log_decay_total = sudden_decay - time_step * decay_speed[None, :]
    weighted = (
        scanned_gradient * jnp.exp(jnp.cumsum(log_decay_total, axis=0))[:, :, None]
    ).reshape(length, groups, head_count // groups, head_size)
    result = jnp.einsum("tgn,tghp->ghpn", readout_groups, weighted, precision=exact_mode)
    return result.reshape(head_count, head_size, -1)


def gate_norm(scan_out, gate_vals, group_norm_scale, groups):
    length = scan_out.shape[0]
    gated = scan_out.reshape(length, -1) * jax.nn.silu(gate_vals)
    grouped = gated.reshape(length, groups, -1)
    factor = lax.rsqrt(jnp.mean(grouped * grouped, axis=-1, keepdims=True) + norm_eps)
    return (grouped * factor).reshape(length, -1) * group_norm_scale[None, :]


def body(
    n_sp,
    n_tp,
    mixer_output_stream,
    layer_output_gradient,
    routes,
    expert_combine_weight,
    expert_gate_weight,
    expert_up_weight,
    expert_down_weight,
    head_mixer_input,
    head_step_size,
    head_decay_rate,
    extra_log_decay,
    state_entering_span,
    state_input_vectors,
    state_readout_vectors,
    gate_preactivation,
    group_norm_scale,
    mixer_output_weight,
):
    local_tokens = routes.shape[0]
    packed = pack(routes, expert_combine_weight, mixer_output_stream, layer_output_gradient, n_sp)
    arrived = dispatch(packed, n_sp, n_tp)
    grad_g, grad_u, grad_d, partial_rows = experts_backward(
        arrived, expert_gate_weight, expert_up_weight, expert_down_weight
    )
    mix_grad = give_back(partial_rows, routes, layer_output_gradient, n_sp, n_tp)

    head_local = head_step_size.shape[1]
    group_local = state_input_vectors.shape[1] // STATE
    input_heads = head_mixer_input.astype(F32).reshape(local_tokens, head_local, HDIM)
    input_vector_groups = state_input_vectors.astype(F32).reshape(local_tokens, group_local, STATE)
    readout_groups = state_readout_vectors.astype(F32).reshape(local_tokens, group_local, STATE)
    within_span_state, within_span_decay = span_final_state(
        input_heads, head_step_size, head_decay_rate, extra_log_decay, input_vector_groups
    )
    part_rows = head_local * HDIM // n_sp
    entering = lax.dynamic_index_in_dim(
        state_entering_span.reshape(n_sp, part_rows, STATE), lax.axis_index(SP), 0, keepdims=False
    )
    incoming_state = carried(
        within_span_state, within_span_decay, entering, n_sp, n_tp, False, 2
    )

    def forward(input_values, time_step_values, input_vector_entries, readout_entries):
        return span_local_scan(
            input_values,
            time_step_values,
            head_decay_rate,
            extra_log_decay,
            input_vector_entries,
            readout_entries,
            incoming_state,
        )

    (scan_out, closing_state), pull_back = jax.vjp(
        forward, input_heads, head_step_size, input_vector_groups, readout_groups
    )

    def apply_norm(scan_vals, gate_vals):
        return gate_norm(scan_vals, gate_vals, group_norm_scale, group_local)

    normed, pull_norm = jax.vjp(apply_norm, scan_out, gate_preactivation.astype(F32))
    normed_low = normed.astype(BF16)
    normed_grad = lax.dot_general(
        mix_grad,
        lax.all_gather(mixer_output_weight, SP, axis=1, tiled=True),
        (((1,), (1,)), ((), ())),
        preferred_element_type=F32,
    )
    scanned_gradient, gate_grad_in = pull_norm(normed_grad)
    reached_gradient = carried_weight(
        scanned_gradient, readout_groups, head_step_size, head_decay_rate, extra_log_decay
    )
    later_grad = carried(
        reached_gradient, within_span_decay, jnp.zeros_like(entering), n_sp, n_tp, True, 3
    )
    input_grad, step_grad, b_grad, c_grad = pull_back((scanned_gradient, later_grad))
    proj_grad = project(normed_low, mix_grad, n_sp, n_tp)
    return (
        grad_g,
        grad_u,
        grad_d,
        proj_grad,
        input_grad.reshape(local_tokens, -1).astype(BF16),
        step_grad,
        b_grad.reshape(local_tokens, -1).astype(BF16),
        c_grad.reshape(local_tokens, -1).astype(BF16),
        gate_grad_in.astype(BF16),
    )


def solution(mesh):
    placed = (
        P(SP, "tp"),
        P(SP, "tp"),
        P(SP, None),
        P(SP, None),
        P(SP, None, "tp"),
        P(SP, None, "tp"),
        P(SP, "tp", None),
        P(SP, "tp"),
        P(SP, "tp"),
        P("tp"),
        P(SP, "tp"),
        P("tp", None, None),
        P(SP, "tp"),
        P(SP, "tp"),
        P(SP, "tp"),
        P("tp"),
        P("tp", SP),
    )
    return jax.shard_map(
        functools.partial(body, mesh.shape["sp"], mesh.shape["tp"]),
        mesh=mesh,
        in_specs=placed,
        out_specs=(
            P(SP, None, "tp"),
            P(SP, None, "tp"),
            P(SP, "tp", None),
            P("tp", SP),
            P(SP, "tp"),
            P(SP, "tp"),
            P(SP, "tp"),
            P(SP, "tp"),
            P(SP, "tp"),
        ),
        check_vma=False,
    )
```

time: 365 us -> 265 us (0.73); the launches traced: 358 us -> 263 us
  Pallas kernels: 0 us -> 206 us
  waiting for transfers between devices: 131 us -> 0.7 us
  blocking collectives: 85.3 us -> 0 us
  matrix products: 42.4 us -> 16.7 us
  other arithmetic: 32.4 us -> 8.04 us
  local copies, waits for them, and re-layouts: 38.9 us -> 17.3 us
  starting transfers between devices: 11.4 us -> 0.04 us
    pallas_call x0 -> x7, Pallas kernels: none -> 206 us  [the longest x1 45.2 us: dispatch(): pl.pallas_call(functools.partial(dispatch_kernel, n_sp, n_tp), out_shape=...]
    reduce_scatter x1 -> x0, waiting for transfers between devices: 56.5 us -> none  [body(): lax.psum_scatter(lax.dot_general(columns, normed_low, (((0,), (0,)), ((),...]
    all_gather x6 -> x0, waiting for transfers between devices: 52 us -> none  [the longest x1 27.2 us: body(): lax.all_gather(part_rows, 'tp', axis=2, tiled=True)]
    all_gather x6 -> x0, blocking collectives: 45.5 us -> none  [the longest x3 20.2 us: prefix_by_axis(): lax.all_gather(part.astype(kind), axis)]
    all_to_all x2 -> x0, blocking collectives: 37.3 us -> none  [the longest x1 21.6 us: body(): lax.all_to_all(sent_grads.reshape(expert_count, capacity, -1), SP, split_...]
    dot_general x10 -> x1, matrix products: 31.7 us -> 3.97 us  [body(): lax.dot_general(mix_grad, lax.all_gather(mixer_output_weight, SP, axis=1,...]
    all_to_all x2 -> x0, waiting for transfers between devices: 21.9 us -> none  [the longest x1 13.5 us: sum_at_owner(): blocks = lax.all_to_all(split_up(x, dim, length), axis, 0, 0, tiled=True)]
    convert_element_type x20 -> x3, other arithmetic: 14.9 us -> 2.02 us  [the longest x1 1.95 us: body(): gate_grad_in.astype(BF16)]
  transfers between devices with their start and end apart: 10 -> 1, of which waited for: 6 -> 0; matrix products, arithmetic and copies ran while one was open for 25% -> 4% of each run, Pallas kernels for 0% -> 54%
where the time goes in v1:
time: 265 us; the launch traced here: 263 us
  Pallas kernels  206 us (78%)
  local copies, waits for them, and re-layouts  17.3 us (7%)
  matrix products  16.7 us (6%)
  between operations  14.6 us (6%)
  other arithmetic  8.04 us (3%)
    pallas_call x1, Pallas kernels, dispatch(): pl.pallas_call(functools.partial(dispatch_kernel, n_sp, n_tp), out_shape=...  45.2 us
    pallas_call x1, Pallas kernels, project(): pl.pallas_call(functools.partial(proj_kernel, n_sp, n_tp), out_shape=jax....  43.4 us
    pallas_call x2, Pallas kernels, carried(): pl.pallas_call(functools.partial(carry_kernel, n_sp, n_tp, reverse), out_...  39.6 us
    pallas_call x1, Pallas kernels, give_back(): pl.pallas_call(functools.partial(return_kernel, n_sp, n_tp), out_shape=ja...  37.3 us
    pallas_call x1, Pallas kernels, experts_backward(): pl.pallas_call(functools.partial(expert_kernel, steps), grid=(steps,), ou...  36.9 us
    unnamed x65, local copies, waits for them, and re-layouts  7.06 us
    dot_general x3, matrix products, span_local_scan(): jnp.einsum('bghls,bsghp->blghp', affinity[:, :, None] * decays, scaled, p...  5.86 us
  transfers between devices with their start and end apart: 1, of which 0 were waited for; matrix products, arithmetic and copies ran while one was open for 4% of the time, Pallas kernels for 54%

profile of v1, /device:TPU:0, one launch (start us, length us, event | category | flops | bytes accessed | tf_op | source)
XLA Modules:
  0.0 263.2 jit_solution(5419652985130483677)
XLA Ops:
  7.3 0.7 all-gather.2.cloned.1.call-update
  8.0 1.4 copy.271.routes_ref
  9.4 3.5 %pack.1 = bf16[1536,256]{1,0:T(8,128)(2,1)} custom-call(s32[2,128]{1,0:T(2,128)} %bitcast.180, f32[2,128]{1,0:T(2,128)} %bitcast.181, bf16[128,512]{1,0:T(8,128)(2,1)} %stream_ref.1, bf16[128,512]{1,0:T(8,128)(2,1)} %grads_ref.3), custom_call_target="tpu_custom_call" | custom-call | tf_op jit(solution)/shard_map/pack/pallas_call | solution.py:98
  12.9 45.2 %dispatch.1.in_ref = bf16[4,32,48,256]{3,2,1,0:T(8,128)(2,1)} custom-call(bf16[32,48,256]{2,1,0:T(8,128)(2,1)} %bitcast.156), custom_call_target="tpu_custom_call" | custom-call | tf_op jit(solution)/shard_map/dispatch/pallas_call | solution.py:222
  60.7 1.1 convolution_convert_fusion.1
  61.8 0.7 broadcast_in_dim.83.decay_ref
  62.5 20.1 %carry.1 = bf16[32,32,128]{2,1,0:T(8,128)(2,1)} custom-call(bf16[32,32,128]{2,1,0:T(8,128)(2,1)} %bitcast.162, f32[32,1,128]{2,1,0:T(1,128)} %broadcast_in_dim.83.decay_ref, f32[32,128]{1,0:T(8,128)} %dynamic-slice_bitcast_fusion.first_ref), custom_call_target="tpu_custom_call" | custom-call | tf_op jit(solution)/shard_map/carry/pallas_call | solution.py:495
  82.7 1.2 convolution_bitcast_fusion.2
  84.1 2.2 fusion.1
  87.2 36.9 %experts.1 = (bf16[1,2048,896]{2,1,0:T(8,128)(2,1)}, bf16[1,2048,896]{2,1,0:T(8,128)(2,1)}, bf16[1,896,2048]{2,1,0:T(8,128)(2,1)}, bf16[384,2048]{1,0:T(8,128)(2,1)}) custom-call(bf16[4,32,48,256]{3,2,1,0:T(8,128)(2,1)} %dispatch.1.in_ref, bf16[1,2048,896]{2,1,0:T(8,128)(2,1)} %gate_ref.1, bf16[1,2048,896]{2,1,0:T(8,128)(2,1)} %up_ref.1, ...), custom_call_target="tpu_custom_call" | custom-call | tf_op jit(solution)/shard_map/experts/pallas_call | solution.py:661
  124.2 37.3 %give_back.1.mix_ref = bf16[128,2048]{1,0:T(8,128)(2,1)} custom-call(bf16[384,2048]{1,0:T(8,128)(2,1)} %get-tuple-element.55.part_ref, s32[128,2]{1,0:T(8,128)} %copy.271.routes_ref, bf16[128,512]{1,0:T(8,128)(2,1)} %grads_ref.3), custom_call_target="tpu_custom_call" | custom-call | tf_op jit(solution)/shard_map/give_back/pallas_call | solution.py:394
  161.5 4.0 %fusion.60 = (f32[128,1024]{1,0:T(8,128)S(1)}, f32[128,1024]{1,0:T(8,128)S(1)}, f32[128,1024]{1,0:T(8,128)}) fusion(f32[128,1024]{1,0:T(8,128)S(1)} %copy.268, bf16[128,1024]{1,0:T(8,128)(2,1)S(1)} %copy-done.6, f32[1024]{0:T(1024)S(1)} %copy-done.19, bf16[128,2048]{1,0:T(8,128)(2,1)} %give_back.1.mix_ref, bf16[1024,2048]{0,1:T(8,128)(2,1)} %all-gather.2.cloned.1.call-done), kind=kOutput, calls=%fused_computation.98 | convolution fusion | flops 538050560 | bytes 7081984 | tf_op jit(solution)/shard_map/dot_general | solution.py:833
  165.5 1.2 mul.331
  166.7 1.3 reduce_sum.123
  168.1 1.3 mul.322
  169.4 1.3 reduce_sum.122
  171.2 0.7 copy.270
  171.9 1.1 mul.323
  173.1 2.0 fusion.16
  175.1 1.3 copy.274
  176.3 1.8 convolution_convert_fusion
  178.7 19.4 %carry_back.1 = bf16[32,32,128]{2,1,0:T(8,128)(2,1)} custom-call(bf16[32,32,128]{2,1,0:T(8,128)(2,1)} %bitcast.163, f32[32,1,128]{2,1,0:T(1,128)} %broadcast_in_dim.83.decay_ref, f32[32,128]{1,0:T(8,128)} %broadcast_in_dim.86.first_ref), custom_call_target="tpu_custom_call" | custom-call | tf_op jit(solution)/shard_map/carry_back/pallas_call | solution.py:495
  198.2 1.2 multiply_reduce_fusion.2
  199.7 1.2 multiply_reduce_fusion.1
  201.1 1.3 fusion
  202.6 2.4 fusion.10
  205.5 43.4 %project.1 = f32[1024,64]{1,0:T(8,128)} custom-call(bf16[128,1024]{1,0:T(8,128)(2,1)} %get-tuple-element.128.normed_ref, bf16[128,2048]{1,0:T(8,128)(2,1)} %give_back.1.mix_ref), custom_call_target="tpu_custom_call" | custom-call | tf_op jit(solution)/shard_map/project/pallas_call | solution.py:579
  248.9 1.9 copy.289
  250.9 0.8 copy.290
  252.1 1.1 reduce_window_sum.42
  254.6 0.7 copy.292
  255.6 0.7 copy.293
  (110 shorter events, 8.2 us)
Async XLA Ops:
  7.2 52.9 %copy-start = (f32[16,64,128]{2,1,0:T(8,128)S(1)}, f32[16,64,128]{2,1,0:T(8,128)}, u32[]{:S(2)}) copy-start(f32[16,64,128]{2,1,0:T(8,128)} %param.28) | copy-start | bytes 1572868
  7.2 50.9 %copy-start.11 = (bf16[128,1024]{1,0:T(8,128)(2,1)S(1)}, bf16[128,1024]{1,0:T(8,128)(2,1)}, u32[]{:S(2)}) copy-start(bf16[128,1024]{1,0:T(8,128)(2,1)} %param.24) | copy-start | bytes 786436
  7.2 51.1 %copy-start.22 = (f32[128,16]{0,1:T(8,128)S(1)}, f32[128,16]{0,1:T(8,128)}, u32[]{:S(2)}) copy-start(f32[128,16]{0,1:T(8,128)} %param.27) | copy-start | bytes 24580
  7.2 51.2 %copy-start.12 = (f32[128,16]{0,1:T(8,128)S(1)}, f32[128,16]{0,1:T(8,128)}, u32[]{:S(2)}) copy-start(f32[128,16]{0,1:T(8,128)} %param.25) | copy-start | bytes 24580
  7.2 51.3 %copy-start.25 = (f32[16]{0:T(128)S(1)}, f32[16]{0:T(128)}, u32[]{:S(2)}) copy-start(f32[16]{0:T(128)} %param.26) | copy-start | bytes 196
  7.2 154.2 %all-gather.2.cloned.1.call-start = ((), (), s32[]{:S(2)}) async-start(), calls=%async_computation | async-start | bytes 4325376 | tf_op jit(solution)/shard_map/all_gather | solution.py:835
  8.0 51.1 %copy-start.15 = (bf16[128,256]{1,0:T(8,128)(2,1)S(1)}, bf16[128,256]{1,0:T(8,128)(2,1)}, u32[]{:S(2)}) copy-start(bf16[128,256]{1,0:T(8,128)(2,1)} %param.29) | copy-start | bytes 196612
  9.4 49.9 %copy-start.16 = (bf16[128,256]{1,0:T(8,128)(2,1)S(1)}, bf16[128,256]{1,0:T(8,128)(2,1)}, u32[]{:S(2)}) copy-start(bf16[128,256]{1,0:T(8,128)(2,1)} %param.30) | copy-start | bytes 196612
  59.8 64.4 %copy-start.23 = (f32[2,8,128]{2,1,0:T(8,128)}, f32[2,8,128]{2,1,0:T(8,128)S(1)}, u32[]{:S(2)}) copy-start(f32[2,8,128]{2,1,0:T(8,128)S(1)} %copy.261) | copy-start | bytes 24580
  59.9 26.6 %copy-start.7 = (bf16[128,2,128]{0,2,1:T(8,128)(2,1)}, bf16[128,2,128]{0,2,1:T(8,128)(2,1)S(1)}, u32[]{:S(2)}) copy-start(bf16[128,2,128]{0,2,1:T(8,128)(2,1)S(1)} %copy.286) | copy-start | bytes 196612
  60.0 26.5 %copy-start.9 = (bf16[128,2,128]{0,2,1:T(8,128)(2,1)}, bf16[128,2,128]{0,2,1:T(8,128)(2,1)S(1)}, u32[]{:S(2)}) copy-start(bf16[128,2,128]{0,2,1:T(8,128)(2,1)S(1)} %copy.287) | copy-start | bytes 196612
  82.6 41.5 %copy-start.20 = (pred[128,128]{1,0:T(8,128)(4,1)}, pred[128,128]{1,0:T(8,128)(4,1)S(1)}, u32[]{:S(2)}) copy-start(pred[128,128]{1,0:T(8,128)(4,1)S(1)} %iota_compare_fusion) | copy-start | bytes 49156
  83.8 2.5 copy-start.3
  83.9 40.3 %copy-start.17 = (f32[128,2,8]{0,2,1:T(8,128)}, f32[128,2,8]{0,2,1:T(8,128)S(1)}, u32[]{:S(2)}) copy-start(f32[128,2,8]{0,2,1:T(8,128)S(1)} %bitcast_exponential_fusion) | copy-start | bytes 24580
  84.1 2.4 copy-start.13
  87.2 74.3 %copy-start.6 = (bf16[128,1024]{1,0:T(8,128)(2,1)S(1)}, bf16[128,1024]{1,0:T(8,128)(2,1)}, u32[]{:S(2)}) copy-start(bf16[128,1024]{1,0:T(8,128)(2,1)} %param.31) | copy-start | bytes 786436
  87.2 74.3 %copy-start.19 = (f32[1024]{0:T(1024)S(1)}, f32[1024]{0:T(1024)}, u32[]{:S(2)}) copy-start(f32[1024]{0:T(1024)} %param.32) | copy-start | bytes 12292
  166.7 6.4 %copy-start.5 = (f32[128,1024]{1,0:T(8,128)S(1)}, f32[128,1024]{1,0:T(8,128)}, u32[]{:S(2)}) copy-start(f32[128,1024]{1,0:T(8,128)} %get-tuple-element.137) | copy-start | bytes 1572868
  171.9 26.3 %copy-start.1 = (bf16[32,32,128]{2,1,0:T(8,128)(2,1)S(1)}, bf16[32,32,128]{2,1,0:T(8,128)(2,1)}, u32[]{:S(2)}) copy-start(bf16[32,32,128]{2,1,0:T(8,128)(2,1)} %carry.1) | copy-start | bytes 786436
  175.1 26.1 %copy-start.14 = (f32[2,128,128]{2,1,0:T(8,128)S(1)}, f32[2,128,128]{2,1,0:T(8,128)}, u32[]{:S(2)}) copy-start(f32[2,128,128]{2,1,0:T(8,128)} %copy-done.13) | copy-start | bytes 393220
  175.1 26.1 %copy-start.21 = (pred[128,128]{1,0:T(8,128)(4,1)S(1)}, pred[128,128]{1,0:T(8,128)(4,1)}, u32[]{:S(2)}) copy-start(pred[128,128]{1,0:T(8,128)(4,1)} %copy-done.20) | copy-start | bytes 49156
  175.1 26.1 %copy-start.24 = (f32[2,8,128]{2,1,0:T(8,128)S(1)}, f32[2,8,128]{2,1,0:T(8,128)}, u32[]{:S(2)}) copy-start(f32[2,8,128]{2,1,0:T(8,128)} %copy-done.23) | copy-start | bytes 24580
  201.1 3.9 %copy-start.4 = (f32[1,128,2,8,64]{1,4,3,2,0:T(8,128)S(1)}, f32[1,128,2,8,64]{1,4,3,2,0:T(8,128)}, u32[]{:S(2)}) copy-start(f32[1,128,2,8,64]{1,4,3,2,0:T(8,128)} %copy-done.3) | copy-start | bytes 1572868
  202.4 2.7 %copy-start.18 = (f32[128,2,8]{0,2,1:T(8,128)S(1)}, f32[128,2,8]{0,2,1:T(8,128)}, u32[]{:S(2)}) copy-start(f32[128,2,8]{0,2,1:T(8,128)} %copy-done.17) | copy-start | bytes 24580
  202.6 50.7 %copy-start.26 = (f32[16]{0:T(128)S(1)}, f32[16]{0:T(128)}, u32[]{:S(2)}) copy-start(f32[16]{0:T(128)} %param.26) | copy-start | bytes 196
  205.0 49.0 %copy-start.8 = (bf16[128,2,128]{0,2,1:T(8,128)(2,1)S(1)}, bf16[128,2,128]{0,2,1:T(8,128)(2,1)}, u32[]{:S(2)}) copy-start(bf16[128,2,128]{0,2,1:T(8,128)(2,1)} %copy-done.7) | copy-start | bytes 196612
  205.0 49.2 %copy-start.2 = (bf16[32,32,128]{2,1,0:T(8,128)(2,1)S(1)}, bf16[32,32,128]{2,1,0:T(8,128)(2,1)}, u32[]{:S(2)}) copy-start(bf16[32,32,128]{2,1,0:T(8,128)(2,1)} %carry_back.1) | copy-start | bytes 786436
  205.0 50.4 %copy-start.10 = (bf16[128,2,128]{0,2,1:T(8,128)(2,1)S(1)}, bf16[128,2,128]{0,2,1:T(8,128)(2,1)}, u32[]{:S(2)}) copy-start(bf16[128,2,128]{0,2,1:T(8,128)(2,1)} %copy-done.9) | copy-start | bytes 196612
Sparse Core Ops, SparseCore 0:
  10.3 53.1 all-gather.1

commit v2 on v1

v2 whole, which is shorter than its diff:
```python
import functools

import jax
import jax.numpy as jnp
from jax import lax
from jax.experimental import pallas as pl
from jax.experimental.pallas import tpu as pltpu
from jax.sharding import PartitionSpec as P

HDIM = 64
STATE = 128
SP = "sp"
CAP = 12
MESH = pl.DeviceIdType.MESH
F32 = jnp.float32
BF16 = jnp.bfloat16

norm_eps = 1e-05
VMEM_BYTES = 60 * 1024 * 1024


def vmem_spec():
    return pl.BlockSpec(memory_space=pltpu.VMEM)


def any_spec():
    return pl.BlockSpec(memory_space=pl.ANY)


def dot(a, b, contract=((1,), (0,))):
    return lax.dot_general(a, b, (contract, ((), ())), preferred_element_type=F32)


def iota(shape, dim):
    return lax.broadcasted_iota(jnp.int32, shape, dim)


def divide(x, by):
    return ((x.astype(F32) + 0.5) * (1.0 / by)).astype(jnp.int32)


def slots_in_rows(routes, experts):
    top, tokens = routes.shape
    ids = iota((experts, tokens), 0)
    earlier = (iota((tokens, tokens), 0) < iota((tokens, tokens), 1)).astype(BF16)
    before = jnp.zeros((experts, 1), F32)
    rows = []
    for k in range(top):
        hits = (ids == routes[k : k + 1, :]).astype(F32)
        rank = dot(hits.astype(BF16), earlier) + before
        rows.append(jnp.sum(hits * rank, axis=0, keepdims=True))
        before = before + jnp.sum(hits, axis=1, keepdims=True)
    return [routes[k : k + 1, :] * CAP + rows[k].astype(jnp.int32) for k in range(top)]


def slots_in_columns(routes, experts):
    tokens, top = routes.shape
    ids = iota((tokens, experts), 1)
    earlier = (iota((tokens, tokens), 1) < iota((tokens, tokens), 0)).astype(BF16)
    before = jnp.zeros((1, experts), F32)
    columns = []
    for k in range(top):
        hits = (ids == routes[:, k : k + 1]).astype(F32)
        rank = dot(earlier, hits.astype(BF16)) + before
        columns.append(jnp.sum(hits * rank, axis=1, keepdims=True))
        before = before + jnp.sum(hits, axis=0, keepdims=True)
    return [routes[:, k : k + 1] * CAP + columns[k].astype(jnp.int32) for k in range(top)]


def pack_kernel(experts, routes_ref, weights_ref, stream_ref, grads_ref, out_ref):
    tokens = stream_ref.shape[0]
    half = stream_ref.shape[1] // 2
    slots = slots_in_rows(routes_ref[...], experts)
    row = iota((experts * 4 * CAP, 1), 0)
    expert = divide(row, 4 * CAP)
    inner = row - expert * (4 * CAP)
    part = divide(inner, CAP)
    slot = expert * CAP + inner - part * CAP
    first = (slot == slots[0]).astype(F32)
    second = (slot == slots[1]).astype(F32)
    match = (first + second).astype(BF16)
    weight = jnp.sum(
        first * weights_ref[0:1, :] + second * weights_ref[1:2, :], axis=1, keepdims=True
    )
    x0 = dot(match, stream_ref[:, :half])
    x1 = dot(match, stream_ref[:, half:])
    g0 = dot(match, grads_ref[:, :half])
    g1 = dot(match, grads_ref[:, half:])
    low = jnp.where(part == 0, x0, g0 * weight)
    high = jnp.where(part == 2, x1, g1 * weight)
    out_ref[...] = jnp.where(part < 2, low, high).astype(BF16)


def pack(routes, weights, stream, grads, experts):
    half = stream.shape[1] // 2
    packed = pl.pallas_call(
        functools.partial(pack_kernel, experts),
        out_shape=jax.ShapeDtypeStruct((experts * 4 * CAP, half), BF16),
        in_specs=[vmem_spec()] * 4,
        out_specs=vmem_spec(),
        compiler_params=pltpu.CompilerParams(vmem_limit_bytes=VMEM_BYTES),
        name="pack",
    )(routes.T, weights.T, stream, grads)
    return packed.reshape(experts, 4 * CAP, half)


def greet(me, tp, n_sp, n_tp, step=1, ring=False, partner=None):
    barrier = pltpu.get_barrier_semaphore()

    def hello(d, carry):
        pl.semaphore_signal(
            barrier, inc=1, device_id=(lax.rem(me + d * step, n_sp), tp), device_id_type=MESH
        )
        return carry

    lax.fori_loop(1, n_sp // step, hello, 0)
    count = n_sp // step - 1
    if partner is not None:
        pl.semaphore_signal(barrier, inc=1, device_id=(partner, tp), device_id_type=MESH)
        count += 1
    if ring:
        for other in (lax.rem(tp + 1, n_tp), lax.rem(tp + n_tp - 1, n_tp)):
            pl.semaphore_signal(barrier, inc=1, device_id=(me, other), device_id_type=MESH)
        count += 2
    pl.semaphore_wait(barrier, count)


def split(x, pieces):
    terms = []
    for _ in range(pieces):
        term = x.astype(BF16)
        terms.append(term)
        x = x - term.astype(F32)
    return terms


def dot_split(x, exact, pieces, contract, left=True):
    total = None
    for term in split(x, pieces):
        part = dot(term, exact, contract) if left else dot(exact, term, contract)
        total = part if total is None else total + part
    return total


def triangle(n, keep):
    return keep(iota((n, n), 0), iota((n, n), 1)).astype(BF16)


def head_spread(heads, size):
    channel, head = iota((heads, heads * size), 1), iota((heads, heads * size), 0)
    return ((channel >= head * size) & (channel < (head + 1) * size)).astype(BF16)


def spread(x, owner):
    return dot_split(x, owner, 2, ((1,), (0,)))


def by_head(x, owner):
    return dot_split(x, owner, 2, ((1,), (1,)))


def cumulative_decay(time_step, rate, extra):
    log_decay = extra - time_step * rate
    upto = triangle(log_decay.shape[0], lambda t, s: s <= t)
    return dot_split(log_decay, upto, 3, ((1,), (0,)), left=False)


def in_rows(x):
    n = x.shape[1]
    return dot_split(x, triangle(n, lambda a, b: a == b), 3, ((1,), (1,)), left=False)


def decay_between(cum, cum_rows, h):
    gap = cum[:, h : h + 1] - cum_rows[h : h + 1, :]
    n = gap.shape[0]
    return jnp.exp(jnp.where(iota((n, n), 1) <= iota((n, n), 0), gap, -1e30))


def halves(pair):
    lane = iota(pair.shape, 1)
    zero = jnp.zeros_like(pair)
    size = pair.shape[1] // 2
    return jnp.concatenate([jnp.where(lane < size, pair, zero), jnp.where(lane < size, zero, pair)], axis=0)


def front_kernel(
    n_sp,
    n_tp,
    in_ref,
    x_ref,
    dt_ref,
    rate_ref,
    extra_ref,
    first_ref,
    b_ref,
    c_ref,
    gate_ref,
    scale_ref,
    out_ref,
    y_ref,
    normed_ref,
    coming,
    state_mine,
    decay_mine,
    states,
    decays,
    carries,
    diag,
    own,
    one,
    two,
    a_send,
    a_recv,
    s_right,
    s_left,
    r_left,
    r_right,
    f_send,
    f_recv,
    sends,
    recvs,
    d_sends,
    d_recvs,
    b_sends,
    b_recvs,
):
    me, tp = lax.axis_index("sp"), lax.axis_index("tp")
    right, left = lax.rem(tp + 1, n_tp), lax.rem(tp + n_tp - 1, n_tp)
    far = lax.rem(tp + 2, n_tp)
    greet(me, tp, n_sp, n_tp, ring=True)

    def origin(d):
        return lax.rem(me + n_sp - d, n_sp)

    def exchange(d):
        to = lax.rem(me + d, n_sp)
        return pltpu.make_async_remote_copy(
            in_ref.at[to], out_ref.at[tp, me], a_send.at[d], a_recv.at[d], (to, tp), MESH
        )

    def arrived(d):
        return pltpu.make_async_remote_copy(
            in_ref.at[me], out_ref.at[tp, origin(d)], a_send.at[d], a_recv.at[d], (me, tp), MESH
        )

    def to_right(d, block):
        piece = out_ref.at[block, origin(d)]
        return pltpu.make_async_remote_copy(
            piece, piece, s_right.at[d], r_left.at[d], (me, right), MESH
        )

    def to_left(d, block):
        piece = out_ref.at[block, origin(d)]
        return pltpu.make_async_remote_copy(
            piece, piece, s_left.at[d], r_right.at[d], (me, left), MESH
        )

    def onward(d, block, to):
        piece = out_ref.at[block, origin(d)]
        return pltpu.make_async_remote_copy(
            piece, piece, f_send.at[d], f_recv.at[d], (me, to), MESH
        )

    def start_exchange(d, carry):
        exchange(d).start()
        return carry

    lax.fori_loop(1, n_sp, start_exchange, 0)
    mine = pltpu.make_async_copy(in_ref.at[me], out_ref.at[tp, me], own)
    mine.start()

    tokens, heads = dt_ref.shape
    channels = x_ref.shape[1]
    groups = b_ref.shape[1] // STATE
    wide = channels // groups
    owner = head_spread(heads, HDIM)
    dt = dt_ref[...]
    cum = cumulative_decay(dt, rate_ref[...], extra_ref[...])
    cum_rows = in_rows(cum)
    last = cum[tokens - 1 : tokens, :]
    values = x_ref[...].astype(F32)
    ending = (values * spread(dt * jnp.exp(last - cum), owner)).astype(BF16)
    parts, rows, entries = state_mine.shape
    per_group = parts // groups
    for g in range(groups):
        state = dot(
            ending[:, g * wide : (g + 1) * wide],
            b_ref[:, g * STATE : (g + 1) * STATE],
            ((0,), (0,)),
        )
        state_mine[g * per_group : (g + 1) * per_group] = state.astype(BF16).reshape(
            per_group, rows, entries
        )
    total = jnp.exp(last)
    for p in range(parts):
        h = p * rows // HDIM
        decay_mine[p] = jnp.broadcast_to(total[:, h : h + 1], (1, entries))

    mine.wait()
    to_right(0, tp).start()
    to_left(0, tp).start()

    def state_copy(d):
        to = lax.rem(me + d, n_sp)
        return pltpu.make_async_remote_copy(
            state_mine.at[to], states.at[me], sends.at[d], recvs.at[d], (to, tp), MESH
        )

    def decay_copy(d):
        to = lax.rem(me + d, n_sp)
        return pltpu.make_async_remote_copy(
            decay_mine.at[to], decays.at[me], d_sends.at[d], d_recvs.at[d], (to, tp), MESH
        )

    def back_copy(d):
        to = lax.rem(me + d, n_sp)
        return pltpu.make_async_remote_copy(
            carries.at[to], coming.at[me], b_sends.at[d], b_recvs.at[d], (to, tp), MESH
        )

    def start_states(d, carry):
        decay_copy(d).start()
        state_copy(d).start()
        return carry

    lax.fori_loop(1, n_sp, start_states, 0)
    kept = pltpu.make_async_copy(state_mine.at[me], states.at[me], one)
    kept_too = pltpu.make_async_copy(decay_mine.at[me], decays.at[me], two)
    kept.start()
    kept_too.start()

    def spread_out(d, carry):
        arrived(d).wait_recv()
        to_right(d, tp).start()
        to_left(d, tp).start()
        return carry

    lax.fori_loop(1, n_sp, spread_out, 0)

    scaled = (values * spread(dt, owner)).astype(BF16)
    affinity = [
        dot(
            c_ref[:, g * STATE : (g + 1) * STATE],
            b_ref[:, g * STATE : (g + 1) * STATE],
            ((1,), (1,)),
        )
        for g in range(groups)
    ]
    for q in range(heads // 2):
        g = q // (heads // 2 // groups)
        both = jnp.concatenate(
            [(affinity[g] * decay_between(cum, cum_rows, 2 * q + j)).astype(BF16) for j in range(2)],
            axis=1,
        )
        at = slice(q * 2 * HDIM, (q + 1) * 2 * HDIM)
        diag[:, at] = dot(both, halves(scaled[:, at]))

    kept.wait()
    kept_too.wait()

    def finish_states(d, carry):
        decay_copy(d).wait()
        state_copy(d).wait()
        return carry

    lax.fori_loop(1, n_sp, finish_states, 0)
    running = first_ref[...]
    for i in range(n_sp):
        carries[i] = running.astype(BF16)
        running = decays[i] * running + states[i].astype(F32)

    def start_back(d, carry):
        back_copy(d).start()
        return carry

    lax.fori_loop(1, n_sp, start_back, 0)
    kept_back = pltpu.make_async_copy(carries.at[me], coming.at[me], one)
    kept_back.start()

    def relay(q, carry):
        d = 2 * q
        to_right(d, left).wait_recv()
        onward(d, left, right).start()
        to_left(d + 1, right).wait_recv()
        onward(d + 1, right, left).start()
        return carry

    lax.fori_loop(0, n_sp // 2, relay, 0)
    kept_back.wait()

    def finish_back(d, carry):
        back_copy(d).wait()
        return carry

    lax.fori_loop(1, n_sp, finish_back, 0)
    since = spread(jnp.exp(cum), owner)
    for g in range(groups):
        at = slice(g * wide, (g + 1) * wide)
        incoming = coming[g * per_group : (g + 1) * per_group].reshape(wide, entries)
        y = diag[:, at] + since[:, at] * dot(
            c_ref[:, g * STATE : (g + 1) * STATE], incoming, ((1,), (1,))
        )
        y_ref[:, at] = y
        gate = gate_ref[:, at].astype(F32)
        gated = y * gate * jax.nn.sigmoid(gate)
        factor = lax.rsqrt(jnp.mean(gated * gated, axis=1, keepdims=True) + norm_eps)
        normed_ref[:, at] = (gated * factor * scale_ref[:, at]).astype(BF16)

    def finish(q, carry):
        d = 2 * q
        to_left(d, right).wait_recv()
        to_right(d + 1, left).wait_recv()
        onward(d, far, right).wait()
        onward(d + 1, far, left).wait()
        to_right(d, tp).wait_send()
        to_left(d, tp).wait_send()
        to_right(d + 1, tp).wait_send()
        to_left(d + 1, tp).wait_send()
        return carry

    lax.fori_loop(0, n_sp // 2, finish, 0)

    def drain(d, carry):
        exchange(d).wait_send()
        return carry

    lax.fori_loop(1, n_sp, drain, 0)


def front(packed, x, dt, rate, extra, first, b, c, gate, scale, n_sp, n_tp):
    dma = pltpu.SemaphoreType.DMA
    tokens, channels = x.shape
    rows, entries = first.shape
    return pl.pallas_call(
        functools.partial(front_kernel, n_sp, n_tp),
        out_shape=(
            jax.ShapeDtypeStruct((n_tp,) + packed.shape, BF16),
            jax.ShapeDtypeStruct((tokens, channels), F32),
            jax.ShapeDtypeStruct((tokens, channels), BF16),
            jax.ShapeDtypeStruct((n_sp, rows, entries), BF16),
        ),
        in_specs=[vmem_spec()] * 10,
        out_specs=(vmem_spec(),) * 4,
        scratch_shapes=[
            pltpu.VMEM((n_sp, rows, entries), BF16),
            pltpu.VMEM((n_sp, 1, entries), F32),
            pltpu.VMEM((n_sp, rows, entries), BF16),
            pltpu.VMEM((n_sp, 1, entries), F32),
            pltpu.VMEM((n_sp, rows, entries), BF16),
            pltpu.VMEM((tokens, channels), F32),
            dma,
            dma,
            dma,
        ]
        + [dma((n_sp,))] * 14,
        compiler_params=pltpu.CompilerParams(
            collective_id=0, has_side_effects=True, vmem_limit_bytes=VMEM_BYTES
        ),
        name="front",
    )(packed, x, dt, rate, extra, first, b, c, gate, scale)


def expert_kernel(
    n_sp,
    n_tp,
    in_ref,
    gate_hbm,
    up_hbm,
    down_hbm,
    routes_ref,
    grads_ref,
    mix_ref,
    dgate_hbm,
    dup_hbm,
    ddown_hbm,
    w_gate,
    w_up,
    w_down,
    d_gate,
    d_up,
    d_down,
    x,
    x_t,
    g,
    gate_grad,
    up_grad,
    hidden,
    part_ref,
    from_left,
    from_right,
    sum_right,
    sum_left,
    out_blocks,
    back,
    own_cols,
    loads,
    stores,
    s_r,
    s_l,
    r_l,
    r_r,
    a_send,
    a_recv,
    g_send,
    g_recv,
    local,
):
    me, tp = lax.axis_index("sp"), lax.axis_index("tp")
    right, left = lax.rem(tp + 1, n_tp), lax.rem(tp + n_tp - 1, n_tp)
    far = lax.rem(tp + 2, n_tp)
    tokens, width = grads_ref.shape
    half, quarter = width // 2, width // 4
    model, units = w_gate.shape
    rows = x.shape[0]
    cuts = [(i, min(256, units - i)) for i in range(0, units, 256)]
    fetches = []
    for k, (start, size) in enumerate(cuts):
        at = pl.ds(start, size)
        fetches.append(
            [
                pltpu.make_async_copy(gate_hbm.at[0, :, at], w_gate.at[:, at], loads.at[3 * k]),
                pltpu.make_async_copy(up_hbm.at[0, :, at], w_up.at[:, at], loads.at[3 * k + 1]),
                pltpu.make_async_copy(down_hbm.at[0, at, :], w_down.at[at, :], loads.at[3 * k + 2]),
            ]
        )
        for fetch in fetches[-1]:
            fetch.start()
    greet(me, tp, n_sp, n_tp, ring=True)

    tall = in_ref.shape[2]
    group_of = 8
    span = group_of * CAP
    spots = iota((1, group_of * tall), 1)
    src = divide(spots, tall)
    inner = spots - src * tall
    which = divide(inner, CAP)
    row = src * CAP + inner - which * CAP
    lines = iota((span, 1), 0)
    pick = [((row == lines) & (which == p)).astype(BF16) for p in range(4)]
    for t in range(n_tp):
        for k in range(n_sp // group_of):
            block = in_ref[t, k * group_of : (k + 1) * group_of].reshape(group_of * tall, half)
            at = slice(k * span, (k + 1) * span)
            for c in range(2):
                cols = slice((2 * t + c) * half, (2 * t + c + 1) * half)
                x[at, cols] = dot(pick[2 * c], block).astype(BF16)
                g[at, cols] = dot(pick[2 * c + 1], block).astype(BF16)

    for k, (start, size) in enumerate(cuts):
        for fetch in fetches[k]:
            fetch.wait()
        at = slice(start, start + size)
        pre_gate = dot(x[...], w_gate[:, at])
        pre_up = dot(x[...], w_up[:, at])
        hidden_grad = dot(g[...], w_down[at, :], ((1,), (1,)))
        sigmoid_gate = jax.nn.sigmoid(pre_gate)
        activated = pre_gate * sigmoid_gate
        hidden[:, at] = (activated * pre_up).astype(BF16)
        gate_grad[:, at] = (
            hidden_grad * pre_up * sigmoid_gate * (1.0 + pre_gate * (1.0 - sigmoid_gate))
        ).astype(BF16)
        up_grad[:, at] = (hidden_grad * activated).astype(BF16)

    def row_block(b):
        for c in range(2):
            cols = pl.ds(pl.multiple_of(b * width + c * half, half), half)
            part_ref[2 * b + c] = (
                dot(gate_grad[...], w_gate[cols, :], ((1,), (1,)))
                + dot(up_grad[...], w_up[cols, :], ((1,), (1,)))
            ).astype(BF16)

    def block(b, which):
        return part_ref.at[2 * b + which]

    def right_copy(k, src):
        return pltpu.make_async_remote_copy(
            src, from_left.at[k], s_r.at[k], r_l.at[k], (me, right), MESH
        )

    def left_copy(k, src):
        return pltpu.make_async_remote_copy(
            src, from_right.at[k], s_l.at[k], r_r.at[k], (me, left), MESH
        )

    row_block(far)
    row_block(right)
    right_copy(0, block(far, 0)).start()
    left_copy(0, block(far, 1)).start()
    row_block(left)
    right_copy(1, block(right, 1)).start()
    row_block(tp)
    left_copy(1, block(left, 0)).start()

    saves = []

    def save(k, src, dst):
        copy = pltpu.make_async_copy(src, dst, stores.at[k])
        copy.start()
        saves.append(copy)

    def passed_right():
        right_copy(0, block(far, 0)).wait()
        sum_right[...] = (block(right, 0)[...].astype(F32) + from_left[0].astype(F32)).astype(BF16)
        left_copy(0, block(far, 1)).wait()
        sum_left[...] = (block(left, 1)[...].astype(F32) + from_right[0].astype(F32)).astype(BF16)

    def gate_up_rows(i):
        at = slice(i * 256, (i + 1) * 256)
        x_t[at, :] = jnp.transpose(x[:, at])
        d_gate[at, :] = dot(x_t[at, :], gate_grad[...]).astype(BF16)
        save(2 * i, d_gate.at[at, :], dgate_hbm.at[0, at, :])
        d_up[at, :] = dot(x_t[at, :], up_grad[...]).astype(BF16)
        save(2 * i + 1, d_up.at[at, :], dup_hbm.at[0, at, :])

    for i in range(4):
        gate_up_rows(i)
    passed_right()
    right_copy(2, sum_right).start()
    left_copy(2, sum_left).start()
    for i in range(4, 8):
        gate_up_rows(i)

    for k, (start, size) in enumerate(cuts):
        at = slice(start, start + size)
        d_down[at, :] = dot(hidden[:, at], g[...], ((0,), (0,))).astype(BF16)
        save(16 + k, d_down.at[at, :], ddown_hbm.at[0, at, :])

    slots = slots_in_columns(routes_ref[...], n_sp)
    column = iota((1, n_sp * 4 * CAP), 1)
    expert = divide(column, 4 * CAP)
    place_in = column - expert * (4 * CAP)
    piece = divide(place_in, CAP)
    slot = expert * CAP + place_in - piece * CAP
    match = (slots[0] == slot) | (slots[1] == slot)

    right_copy(1, block(right, 1)).wait()
    left_copy(1, block(left, 0)).wait()
    right_copy(2, sum_right).wait()
    left_copy(2, sum_left).wait()

    tall_out = iota((group_of * 4 * CAP, 1), 0)
    out_src = divide(tall_out, 4 * CAP)
    out_in = tall_out - out_src * (4 * CAP)
    out_piece = divide(out_in, CAP)
    out_row = out_src * CAP + out_in - out_piece * CAP
    pair_at = iota((1, span), 1)
    place = [((out_row == pair_at) & (out_piece == c)).astype(BF16) for c in range(4)]
    for k in range(rows // span):
        at = slice(k * span, (k + 1) * span)
        low = (
            part_ref[2 * tp, at, :].astype(F32)
            + from_left[2, at, :].astype(F32)
            + from_right[1, at, :].astype(F32)
        ).astype(BF16)
        high = (
            part_ref[2 * tp + 1, at, :].astype(F32)
            + from_right[2, at, :].astype(F32)
            + from_left[1, at, :].astype(F32)
        ).astype(BF16)
        laid = (
            dot(place[0], low[:, :quarter])
            + dot(place[1], low[:, quarter:])
            + dot(place[2], high[:, :quarter])
            + dot(place[3], high[:, quarter:])
        )
        out_blocks[k * group_of : (k + 1) * group_of] = laid.astype(BF16).reshape(
            group_of, 4 * CAP, quarter
        )

    def exchange(d):
        to = lax.rem(me + d, n_sp)
        return pltpu.make_async_remote_copy(
            out_blocks.at[to], back.at[me], a_send.at[d], a_recv.at[d], (to, tp), MESH
        )

    def start_exchange(d, carry):
        exchange(d).start()
        return carry

    lax.fori_loop(1, n_sp, start_exchange, 0)
    mine = pltpu.make_async_copy(out_blocks.at[me], back.at[me], local)
    mine.start()
    mine.wait()

    def finish_exchange(d, carry):
        exchange(d).wait()
        return carry

    lax.fori_loop(1, n_sp, finish_exchange, 0)
    returned = back[...].reshape(n_sp * 4 * CAP, quarter)
    for c in range(4):
        chosen = jnp.where(match & (piece == c), 1.0, 0.0).astype(BF16)
        cols = slice(c * quarter, (c + 1) * quarter)
        own_cols[:, cols] = (grads_ref[:, cols].astype(F32) + dot(chosen, returned)).astype(BF16)

    def spot(b):
        return mix_ref.at[:, pl.ds(pl.multiple_of(b * width, width), width)]

    def spot_half(b, which):
        return mix_ref.at[:, pl.ds(pl.multiple_of(b * width + which * half, half), half)]

    def gather(k, src, dst, to):
        return pltpu.make_async_remote_copy(
            src, dst, g_send.at[k], g_recv.at[k], (me, to), MESH
        )

    gather(0, own_cols, spot(tp), right).start()
    gather(1, own_cols, spot(tp), left).start()
    spot(tp)[...] = own_cols[...]
    gather(0, own_cols, spot(left), right).wait_recv()
    gather(2, spot_half(left, 0), spot_half(left, 0), right).start()
    gather(1, own_cols, spot(right), left).wait_recv()
    gather(3, spot_half(right, 1), spot_half(right, 1), left).start()
    gather(2, spot_half(far, 0), spot_half(far, 0), right).wait()
    gather(3, spot_half(far, 1), spot_half(far, 1), left).wait()
    gather(0, own_cols, spot(tp), right).wait_send()
    gather(1, own_cols, spot(tp), left).wait_send()
    for copy in saves:
        copy.wait()


def experts_backward(arrived, w_gate, w_up, w_down, routes, grads, n_sp, n_tp):
    _, model, units = w_gate.shape
    rows = n_sp * CAP
    tokens, width = grads.shape
    half, quarter = width // 2, width // 4
    dma = pltpu.SemaphoreType.DMA
    return pl.pallas_call(
        functools.partial(expert_kernel, n_sp, n_tp),
        out_shape=(
            jax.ShapeDtypeStruct((tokens, width * n_tp), BF16),
            jax.ShapeDtypeStruct(w_gate.shape, BF16),
            jax.ShapeDtypeStruct(w_up.shape, BF16),
            jax.ShapeDtypeStruct(w_down.shape, BF16),
        ),
        in_specs=[vmem_spec()] + [any_spec()] * 3 + [vmem_spec()] * 2,
        out_specs=(vmem_spec(),) + (any_spec(),) * 3,
        scratch_shapes=[
            pltpu.VMEM((model, units), BF16),
            pltpu.VMEM((model, units), BF16),
            pltpu.VMEM((units, model), BF16),
            pltpu.VMEM((model, units), BF16),
            pltpu.VMEM((model, units), BF16),
            pltpu.VMEM((units, model), BF16),
            pltpu.VMEM((rows, model), BF16),
            pltpu.VMEM((model, rows), BF16),
            pltpu.VMEM((rows, model), BF16),
            pltpu.VMEM((rows, units), BF16),
            pltpu.VMEM((rows, units), BF16),
            pltpu.VMEM((rows, units), BF16),
            pltpu.VMEM((2 * n_tp, rows, half), BF16),
            pltpu.VMEM((3, rows, half), BF16),
            pltpu.VMEM((3, rows, half), BF16),
            pltpu.VMEM((rows, half), BF16),
            pltpu.VMEM((rows, half), BF16),
            pltpu.VMEM((n_sp, 4 * CAP, quarter), BF16),
            pltpu.VMEM((n_sp, 4 * CAP, quarter), BF16),
            pltpu.VMEM((tokens, width), BF16),
            dma((12,)),
            dma((20,)),
            dma((3,)),
            dma((3,)),
            dma((3,)),
            dma((3,)),
            dma((n_sp,)),
            dma((n_sp,)),
            dma((4,)),
            dma((4,)),
            dma,
        ],
        compiler_params=pltpu.CompilerParams(
            collective_id=1, has_side_effects=True, vmem_limit_bytes=VMEM_BYTES
        ),
        name="experts",
    )(arrived, w_gate, w_up, w_down, routes, grads)


def tail_kernel(
    n_sp,
    n_tp,
    mix_ref,
    weight_hbm,
    y_ref,
    normed_ref,
    x_ref,
    dt_ref,
    rate_ref,
    extra_ref,
    coming_ref,
    b_ref,
    c_ref,
    gate_ref,
    scale_ref,
    proj_ref,
    dx_ref,
    ddt_ref,
    db_ref,
    dc_ref,
    dgate_ref,
    weight,
    normed2,
    mix2,
    parts,
    landed,
    total,
    other,
    state_mine,
    decay_mine,
    states,
    decays,
    carries,
    later,
    d_scaled,
    one,
    two,
    load,
    p_send,
    p_recv,
    a_send,
    a_recv,
    sends,
    recvs,
    d_sends,
    d_recvs,
    b_sends,
    b_recvs,
):
    me, tp = lax.axis_index("sp"), lax.axis_index("tp")
    core = lax.rem(me, 2)
    partner = me + 1 - 2 * core
    chip = lax.div(me, 2)
    chips = n_sp // 2
    fetch = pltpu.make_async_copy(weight_hbm, weight, load)
    fetch.start()
    greet(me, tp, n_sp, n_tp)
    tokens, heads = dt_ref.shape
    channels = x_ref.shape[1]
    groups = b_ref.shape[1] // STATE
    wide = channels // groups
    half = channels // 2
    cols = proj_ref.shape[1]
    n_parts, rows, entries = state_mine.shape
    per_group = n_parts // groups

    def pair(k, src, dst):
        return pltpu.make_async_remote_copy(
            src, dst, p_send.at[k], p_recv.at[k], (partner, tp), MESH
        )

    def mine(c):
        return pl.ds(pl.multiple_of(c * half, half), half)

    pair(0, normed_ref.at[:, mine(1 - core)], normed2).start()
    pair(1, mix_ref, mix2).start()

    owner = head_spread(heads, HDIM)
    dt = dt_ref[...]
    cum = cumulative_decay(dt, rate_ref[...], extra_ref[...])
    cum_rows = in_rows(cum)
    last = cum[tokens - 1 : tokens, :]
    since = spread(jnp.exp(cum), owner)
    fetch.wait()
    d_y = []
    for g in range(groups):
        at = slice(g * wide, (g + 1) * wide)
        normed_grad = dot(mix_ref[...], weight[at, :], ((1,), (1,)))
        y = y_ref[:, at]
        gate = gate_ref[:, at].astype(F32)
        sigmoid_gate = jax.nn.sigmoid(gate)
        activated = gate * sigmoid_gate
        gated = y * activated
        factor = lax.rsqrt(jnp.mean(gated * gated, axis=1, keepdims=True) + norm_eps)
        scaled_grad = normed_grad * scale_ref[:, at]
        along = jnp.mean(scaled_grad * gated, axis=1, keepdims=True) * factor * factor
        gated_grad = factor * (scaled_grad - gated * along)
        d_y.append(gated_grad * activated)
        dgate_ref[:, at] = (
            gated_grad * y * (sigmoid_gate * (1.0 + gate * (1.0 - sigmoid_gate)))
        ).astype(BF16)
    d_out = jnp.concatenate(d_y, axis=1)
    since_grad = since * d_out
    since_low = since_grad.astype(BF16)
    for g in range(groups):
        state = dot(
            since_low[:, g * wide : (g + 1) * wide],
            c_ref[:, g * STATE : (g + 1) * STATE],
            ((0,), (0,)),
        )
        state_mine[g * per_group : (g + 1) * per_group] = state.astype(BF16).reshape(
            per_group, rows, entries
        )
    whole = jnp.exp(last)
    for p in range(n_parts):
        h = p * rows // HDIM
        decay_mine[p] = jnp.broadcast_to(whole[:, h : h + 1], (1, entries))

    def state_copy(d):
        to = lax.rem(me + d, n_sp)
        return pltpu.make_async_remote_copy(
            state_mine.at[to], states.at[me], sends.at[d], recvs.at[d], (to, tp), MESH
        )

    def decay_copy(d):
        to = lax.rem(me + d, n_sp)
        return pltpu.make_async_remote_copy(
            decay_mine.at[to], decays.at[me], d_sends.at[d], d_recvs.at[d], (to, tp), MESH
        )

    def back_copy(d):
        to = lax.rem(me + d, n_sp)
        return pltpu.make_async_remote_copy(
            carries.at[to], later.at[me], b_sends.at[d], b_recvs.at[d], (to, tp), MESH
        )

    def start_states(d, carry):
        decay_copy(d).start()
        state_copy(d).start()
        return carry

    lax.fori_loop(1, n_sp, start_states, 0)
    kept = pltpu.make_async_copy(state_mine.at[me], states.at[me], one)
    kept_too = pltpu.make_async_copy(decay_mine.at[me], decays.at[me], two)
    kept.start()
    kept_too.start()

    pair(0, normed_ref.at[:, mine(1 - core)], normed2).wait()
    pair(1, mix_ref, mix2).wait()
    own_t = jnp.transpose(normed_ref[:, mine(core)])
    other_t = jnp.transpose(normed2[...])
    for c in range(chips):
        at = slice(c * 2 * cols, (c + 1) * 2 * cols)
        parts[c] = (dot(own_t, mix_ref[:, at]) + dot(other_t, mix2[:, at])).astype(BF16)

    def exchange(d):
        to = lax.rem(chip + d, chips)
        return pltpu.make_async_remote_copy(
            parts.at[to], landed.at[chip], a_send.at[d], a_recv.at[d], (2 * to + core, tp), MESH
        )

    def start_parts(d, carry):
        exchange(d).start()
        return carry

    kept.wait()
    kept_too.wait()

    def finish_states(d, carry):
        decay_copy(d).wait()
        state_copy(d).wait()
        return carry

    lax.fori_loop(1, n_sp, finish_states, 0)
    running = jnp.zeros((rows, entries), F32)
    for step in range(n_sp):
        i = n_sp - 1 - step
        carries[i] = running.astype(BF16)
        running = decays[i] * running + states[i].astype(F32)

    def start_back(d, carry):
        back_copy(d).start()
        return carry

    lax.fori_loop(1, n_sp, start_back, 0)
    lax.fori_loop(1, chips, start_parts, 0)
    kept_back = pltpu.make_async_copy(carries.at[me], later.at[me], one)
    kept_back.start()

    values = x_ref[...].astype(F32)
    steps = spread(dt, owner)
    scaled = values * steps
    scaled_low = scaled.astype(BF16)
    d_low = d_out.astype(BF16)
    not_before = triangle(tokens, lambda t, s: s >= t)
    below = (iota((tokens, tokens), 1) < iota((tokens, tokens), 0)).astype(F32)
    head_lane = iota((1, heads), 1)
    crossing = jnp.zeros((tokens, heads), F32)
    d_affinity = []
    for g in range(groups):
        affinity = dot(
            c_ref[:, g * STATE : (g + 1) * STATE],
            b_ref[:, g * STATE : (g + 1) * STATE],
            ((1,), (1,)),
        )
        sum_affinity = jnp.zeros((tokens, tokens), F32)
        first = g * (heads // 2 // groups)
        for q in range(first, first + heads // 2 // groups):
            at = slice(q * 2 * HDIM, (q + 1) * 2 * HDIM)
            d_halves = halves(d_low[:, at])
            d_weights = dot(d_halves, scaled_low[:, at], ((1,), (1,)))
            weights, moved = [], []
            for j in range(2):
                between = decay_between(cum, cum_rows, 2 * q + j)
                weights.append((affinity * between).astype(BF16))
                d_between = d_weights[j * tokens : (j + 1) * tokens] * between
                sum_affinity = sum_affinity + d_between
                moved.append((d_between * affinity).astype(BF16))
            d_scaled[:, at] = dot(jnp.concatenate(weights, axis=0), d_halves, ((0,), (0,)))
            reach = dot(not_before, jnp.concatenate(moved, axis=1))
            for j in range(2):
                over = jnp.sum(
                    reach[:, j * tokens : (j + 1) * tokens] * below, axis=1, keepdims=True
                )
                crossing = crossing + jnp.where(head_lane == 2 * q + j, over, 0.0)
        d_affinity.append(sum_affinity.astype(BF16))
    read_out = []
    for g in range(groups):
        at = slice(g * wide, (g + 1) * wide)
        by = slice(g * STATE, (g + 1) * STATE)
        incoming = coming_ref[g * per_group : (g + 1) * per_group].reshape(wide, entries)
        read_out.append(dot(c_ref[:, by], incoming, ((1,), (1,))))
        dc_ref[:, by] = (
            dot(d_affinity[g], b_ref[:, by]) + dot(since_low[:, at], incoming)
        ).astype(BF16)
    reading = by_head(since_grad * jnp.concatenate(read_out, axis=1), owner)

    kept_back.wait()

    def finish_back(d, carry):
        back_copy(d).wait()
        return carry

    lax.fori_loop(1, n_sp, finish_back, 0)
    until = spread(jnp.exp(last - cum), owner)
    ending = scaled * until
    ending_low = ending.astype(BF16)
    from_later = []
    for g in range(groups):
        at = slice(g * wide, (g + 1) * wide)
        by = slice(g * STATE, (g + 1) * STATE)
        after = later[g * per_group : (g + 1) * per_group].reshape(wide, entries)
        from_later.append(dot(b_ref[:, by], after, ((1,), (1,))))
        db_ref[:, by] = (
            dot(d_affinity[g], c_ref[:, by], ((0,), (0,))) + dot(ending_low[:, at], after)
        ).astype(BF16)
    closing = jnp.concatenate(from_later, axis=1)
    gradient = d_scaled[...] + until * closing
    dx_ref[...] = (gradient * steps).astype(BF16)
    direct = by_head(gradient * values, owner)
    stored = by_head(ending * closing, owner)
    kept_state = jnp.sum(
        (
            coming_ref[...].astype(F32).reshape(heads, HDIM, entries)
            * later[...].astype(F32).reshape(heads, HDIM, entries)
        ),
        axis=1,
    )
    passing = dot_split(
        kept_state, jnp.ones((8, entries), BF16), 3, ((1,), (1,)), left=False
    )[0:1, :]
    earlier = triangle(tokens, lambda t, s: s < t)
    d_decay = (
        crossing
        + dot_split(reading, not_before, 3, ((1,), (0,)), left=False)
        + dot_split(stored, earlier, 3, ((1,), (0,)), left=False)
        + passing * whole
    )
    ddt_ref[...] = direct - d_decay * rate_ref[...]

    total[...] = parts[chip].astype(F32)

    def finish_parts(d, carry):
        exchange(d).wait()
        total[...] += landed[lax.rem(chip + chips - d, chips)].astype(F32)
        return carry

    lax.fori_loop(1, chips, finish_parts, 0)
    pair(2, total, other).start()
    proj_ref[mine(core), :] = jnp.where(core == 0, total[:, :cols], total[:, cols:])
    pair(2, total, other).wait()
    proj_ref[mine(1 - core), :] = jnp.where(core == 0, other[:, :cols], other[:, cols:])


def tail(mix, weight, y, normed, x, dt, rate, extra, coming, b, c, gate, scale, n_sp, n_tp):
    dma = pltpu.SemaphoreType.DMA
    tokens, channels = x.shape
    heads = dt.shape[1]
    _, rows, entries = coming.shape
    width = mix.shape[1]
    half = channels // 2
    chips = n_sp // 2
    cols = width // n_sp
    return pl.pallas_call(
        functools.partial(tail_kernel, n_sp, n_tp),
        out_shape=(
            jax.ShapeDtypeStruct((channels, cols), F32),
            jax.ShapeDtypeStruct((tokens, channels), BF16),
            jax.ShapeDtypeStruct((tokens, heads), F32),
            jax.ShapeDtypeStruct(b.shape, BF16),
            jax.ShapeDtypeStruct(c.shape, BF16),
            jax.ShapeDtypeStruct((tokens, channels), BF16),
        ),
        in_specs=[vmem_spec(), any_spec()] + [vmem_spec()] * 11,
        out_specs=(vmem_spec(),) * 6,
        scratch_shapes=[
            pltpu.VMEM((channels, width), BF16),
            pltpu.VMEM((tokens, half), BF16),
            pltpu.VMEM((tokens, width), BF16),
            pltpu.VMEM((chips, half, 2 * cols), BF16),
            pltpu.VMEM((chips, half, 2 * cols), BF16),
            pltpu.VMEM((half, 2 * cols), F32),
            pltpu.VMEM((half, 2 * cols), F32),
            pltpu.VMEM((n_sp, rows, entries), BF16),
            pltpu.VMEM((n_sp, 1, entries), F32),
            pltpu.VMEM((n_sp, rows, entries), BF16),
            pltpu.VMEM((n_sp, 1, entries), F32),
            pltpu.VMEM((n_sp, rows, entries), BF16),
            pltpu.VMEM((n_sp, rows, entries), BF16),
            pltpu.VMEM((tokens, channels), F32),
            dma,
            dma,
            dma,
            dma((3,)),
            dma((3,)),
            dma((chips,)),
            dma((chips,)),
        ]
        + [dma((n_sp,))] * 6,
        compiler_params=pltpu.CompilerParams(
            collective_id=2, has_side_effects=True, vmem_limit_bytes=VMEM_BYTES
        ),
        name="tail",
    )(mix, weight, y, normed, x, dt, rate, extra, coming, b, c, gate, scale)


def body(
    n_sp,
    n_tp,
    mixer_output_stream,
    layer_output_gradient,
    routes,
    expert_combine_weight,
    expert_gate_weight,
    expert_up_weight,
    expert_down_weight,
    head_mixer_input,
    head_step_size,
    head_decay_rate,
    extra_log_decay,
    state_entering_span,
    state_input_vectors,
    state_readout_vectors,
    gate_preactivation,
    group_norm_scale,
    mixer_output_weight,
):
    packed = pack(routes, expert_combine_weight, mixer_output_stream, layer_output_gradient, n_sp)
    heads = head_step_size.shape[1]
    part_rows = heads * HDIM // n_sp
    entering = lax.dynamic_index_in_dim(
        state_entering_span.reshape(n_sp, part_rows, STATE), lax.axis_index(SP), 0, keepdims=False
    )
    rate = head_decay_rate[None, :]
    scale = group_norm_scale[None, :]
    arrived, scan_out, normed_low, coming = front(
        packed,
        head_mixer_input,
        head_step_size,
        rate,
        extra_log_decay,
        entering,
        state_input_vectors,
        state_readout_vectors,
        gate_preactivation,
        scale,
        n_sp,
        n_tp,
    )
    mix_grad, grad_g, grad_u, grad_d = experts_backward(
        arrived,
        expert_gate_weight,
        expert_up_weight,
        expert_down_weight,
        routes,
        layer_output_gradient,
        n_sp,
        n_tp,
    )
    weight = lax.all_gather(mixer_output_weight, SP, axis=1, tiled=True)
    proj_grad, input_grad, step_grad, b_grad, c_grad, gate_grad_in = tail(
        mix_grad,
        weight,
        scan_out,
        normed_low,
        head_mixer_input,
        head_step_size,
        rate,
        extra_log_decay,
        coming,
        state_input_vectors,
        state_readout_vectors,
        gate_preactivation,
        scale,
        n_sp,
        n_tp,
    )
    return (
        grad_g,
        grad_u,
        grad_d,
        proj_grad,
        input_grad,
        step_grad,
        b_grad,
        c_grad,
        gate_grad_in,
    )


def solution(mesh):
    placed = (
        P(SP, "tp"),
        P(SP, "tp"),
        P(SP, None),
        P(SP, None),
        P(SP, None, "tp"),
        P(SP, None, "tp"),
        P(SP, "tp", None),
        P(SP, "tp"),
        P(SP, "tp"),
        P("tp"),
        P(SP, "tp"),
        P("tp", None, None),
        P(SP, "tp"),
        P(SP, "tp"),
        P(SP, "tp"),
        P("tp"),
        P("tp", SP),
    )
    return jax.shard_map(
        functools.partial(body, mesh.shape["sp"], mesh.shape["tp"]),
        mesh=mesh,
        in_specs=placed,
        out_specs=(
            P(SP, None, "tp"),
            P(SP, None, "tp"),
            P(SP, "tp", None),
            P("tp", SP),
            P(SP, "tp"),
            P(SP, "tp"),
            P(SP, "tp"),
            P(SP, "tp"),
            P(SP, "tp"),
        ),
        check_vma=False,
    )
```

time: 265 us -> 198 us (0.75)
  Pallas kernels: 206 us -> 154 us
  matrix products: 16.7 us -> 0 us
  local copies, waits for them, and re-layouts: 17.3 us -> 27.1 us
  other arithmetic: 8.04 us -> 0 us
    pallas_call x6 -> x3, Pallas kernels: 202 us -> 151 us  [the longest x1 53.3 us: tail(): pl.pallas_call(functools.partial(tail_kernel, n_sp, n_tp), out_shape=(jax...]
    dot_general x13 -> x0, matrix products: 16.7 us -> none  [the longest x3 5.86 us: span_local_scan(): jnp.einsum('bghls,bsghp->blghp', affinity[:, :, None] * decays, scaled, p...]
    unnamed x65 -> x26, local copies, waits for them, and re-layouts: 7.06 us -> 19.9 us
    all_gather x0 -> x1, local copies, waits for them, and re-layouts: none -> 6.56 us  [body(): weight = lax.all_gather(mixer_output_weight, SP, axis=1, tiled=True)]
    mul x6 -> x0, local copies, waits for them, and re-layouts: 5.01 us -> none  [the longest x2 2.33 us: gate_norm(): return (grouped * factor).reshape(length, -1) * group_norm_scale[None, :]]
    reduce_sum x8 -> x0, other arithmetic: 4.18 us -> none  [the longest x1 1.32 us: gate_norm(): return (grouped * factor).reshape(length, -1) * group_norm_scale[None, :]]
  transfers between devices with their start and end apart: 1 -> 1, of which waited for: 0 -> 0; matrix products, arithmetic and copies ran while one was open for 4% -> 2% of each run, Pallas kernels for 54% -> 52%
where the time goes in v2:
time: 198 us; the launch traced here: 196 us
  Pallas kernels  154 us (78%)
  local copies, waits for them, and re-layouts  27.1 us (14%)
  between operations  14.1 us (7%)
    pallas_call x1, Pallas kernels, tail(): pl.pallas_call(functools.partial(tail_kernel, n_sp, n_tp), out_shape=(jax...  53.3 us
    pallas_call x1, Pallas kernels, experts_backward(): pl.pallas_call(functools.partial(expert_kernel, n_sp, n_tp), out_shape=(j...  50 us
    pallas_call x1, Pallas kernels, front(): pl.pallas_call(functools.partial(front_kernel, n_sp, n_tp), out_shape=(ja...  47.8 us
    unnamed x26, local copies, waits for them, and re-layouts  19.9 us
    all_gather x1, local copies, waits for them, and re-layouts, body(): weight = lax.all_gather(mixer_output_weight, SP, axis=1, tiled=True)  6.56 us
  transfers between devices with their start and end apart: 1, of which 0 were waited for; matrix products, arithmetic and copies ran while one was open for 2% of the time, Pallas kernels for 52%

profile of v2, /device:TPU:0, one launch (start us, length us, event | category | flops | bytes accessed | tf_op | source)
XLA Modules:
  0.0 196.4 jit_solution(15321402924479090115)
XLA Ops:
  7.2 0.0 copy-start
  7.2 0.0 all-gather.2.cloned.1.call-start
  7.2 0.7 all-gather.2.cloned.1.call-update
  7.9 1.4 copy.34.dt_ref
  9.4 1.4 copy.35.extra_ref
  10.8 1.4 copy.36.routes_ref
  12.2 3.4 %pack.1 = bf16[1536,256]{1,0:T(8,128)(2,1)} custom-call(s32[2,128]{1,0:T(2,128)} %bitcast.12, f32[2,128]{1,0:T(2,128)} %bitcast.15, bf16[128,512]{1,0:T(8,128)(2,1)} %stream_ref.1, bf16[128,512]{1,0:T(8,128)(2,1)} %grads_ref.3), custom_call_target="tpu_custom_call" | custom-call | tf_op jit(solution)/shard_map/pack/pallas_call | solution.py:96
  15.6 0.0 copy-done
  15.6 0.6 dynamic-slice_bitcast_fusion.first_ref
  16.2 47.8 %front.1 = (bf16[4,32,48,256]{3,2,1,0:T(8,128)(2,1)}, f32[128,1024]{1,0:T(8,128)}, bf16[128,1024]{1,0:T(8,128)(2,1)}, bf16[32,32,128]{2,1,0:T(8,128)(2,1)}) custom-call(bf16[32,48,256]{2,1,0:T(8,128)(2,1)} %bitcast.9, bf16[128,1024]{1,0:T(8,128)(2,1)} %x_ref.3, f32[128,16]{1,0:T(8,128)} %copy.34.dt_ref, f32[1,16]{1,0:T(1,128)} %bitcast.13, ...), custom_call_target="tpu_custom_call" | custom-call | tf_op jit(solution)/shard_map/front/pallas_call | solution.py:434
  64.0 50.0 %experts.1 = (bf16[128,2048]{1,0:T(8,128)(2,1)}, bf16[1,2048,896]{2,1,0:T(8,128)(2,1)}, bf16[1,2048,896]{2,1,0:T(8,128)(2,1)}, bf16[1,896,2048]{2,1,0:T(8,128)(2,1)}) custom-call(bf16[4,32,48,256]{3,2,1,0:T(8,128)(2,1)} %get-tuple-element.23.in_ref, bf16[1,2048,896]{2,1,0:T(8,128)(2,1)} %gate_hbm.1, bf16[1,2048,896]{2,1,0:T(8,128)(2,1)} %up_hbm.1, ...), custom_call_target="tpu_custom_call" | custom-call | tf_op jit(solution)/shard_map/experts/pallas_call | solution.py:728
  114.0 0.0 all-gather.2.cloned.1.call-done
  114.0 6.6 %copy.37.weight_hbm = bf16[1024,2048]{1,0:T(8,128)(2,1)} copy(bf16[1024,2048]{0,1:T(8,128)(2,1)} %all-gather.2.cloned.1.call-done) | data formatting | bytes 8388608 | tf_op jit(solution)/shard_map/all_gather | solution.py:1178
  120.6 53.3 %tail.1 = (f32[1024,64]{1,0:T(8,128)}, bf16[128,1024]{1,0:T(8,128)(2,1)}, f32[128,16]{1,0:T(8,128)}, bf16[128,256]{1,0:T(8,128)(2,1)}, bf16[128,256]{1,0:T(8,128)(2,1)}, /*index=5*/bf16[128,1024]{1,0:T(8,128)(2,1)}) custom-call(bf16[128,2048]{1,0:T(8,128)(2,1)} %get-tuple-element.27.mix_ref, bf16[1024,2048]{1,0:T(8,128)(2,1)} %copy.37.weight_hbm, ...), custom_call_target="tpu_custom_call" | custom-call | tf_op jit(solution)/shard_map/tail/pallas_call | solution.py:1082
  173.9 1.9 copy.40
  175.8 1.5 copy.41
  177.3 0.0 copy-start.2
  177.3 4.3 %copy.49 = bf16[1,2048,896]{2,1,0:T(8,128)(2,1)} copy(bf16[1,2048,896]{2,1,0:T(8,128)(2,1)} %get-tuple-element.64) | data formatting | bytes 7340032
  181.6 0.0 copy-done.2
  181.6 0.0 copy-start.1
  181.6 1.9 copy.50
  183.5 1.5 copy-done.1
  185.0 0.0 copy-start.4
  185.0 1.8 copy.51
  186.8 0.0 copy-done.4
  186.8 0.7 copy.52
  187.5 0.0 copy-done.6
  187.6 0.6 copy.53
  188.2 0.0 copy-done.5
  188.2 0.6 copy.54
  188.8 0.0 copy-done.3
  188.8 0.7 copy.55
  (3 shorter events, 0.0 us)
Async XLA Ops:
  7.2 8.4 %copy-start = (f32[16,64,128]{2,1,0:T(8,128)S(1)}, f32[16,64,128]{2,1,0:T(8,128)}, u32[]{:S(2)}) copy-start(f32[16,64,128]{2,1,0:T(8,128)} %param.28) | copy-start | bytes 1572868
  7.2 106.8 %all-gather.2.cloned.1.call-start = ((), (), s32[]{:S(2)}) async-start(), calls=%async_computation | async-start | bytes 4325376 | tf_op jit(solution)/shard_map/all_gather | solution.py:1178
  177.3 4.3 %copy-start.2 = (bf16[1,2048,896]{2,1,0:T(8,128)(2,1)S(1)}, bf16[1,2048,896]{2,1,0:T(8,128)(2,1)}, u32[]{:S(2)}) copy-start(bf16[1,2048,896]{2,1,0:T(8,128)(2,1)} %get-tuple-element.65) | copy-start | bytes 11010052
  181.6 3.4 %copy-start.1 = (bf16[1,896,2048]{2,1,0:T(8,128)(2,1)S(1)}, bf16[1,896,2048]{2,1,0:T(8,128)(2,1)}, u32[]{:S(2)}) copy-start(bf16[1,896,2048]{2,1,0:T(8,128)(2,1)} %get-tuple-element.66) | copy-start | bytes 11010052
  185.0 1.9 copy-start.4
  185.0 2.6 %copy-start.6 = (bf16[128,256]{1,0:T(8,128)(2,1)S(1)}, bf16[128,256]{1,0:T(8,128)(2,1)}, u32[]{:S(2)}) copy-start(bf16[128,256]{1,0:T(8,128)(2,1)} %get-tuple-element.70) | copy-start | bytes 196612
  185.0 3.2 %copy-start.5 = (bf16[128,256]{1,0:T(8,128)(2,1)S(1)}, bf16[128,256]{1,0:T(8,128)(2,1)}, u32[]{:S(2)}) copy-start(bf16[128,256]{1,0:T(8,128)(2,1)} %get-tuple-element.71) | copy-start | bytes 196612
  185.0 3.8 %copy-start.3 = (bf16[128,1024]{1,0:T(8,128)(2,1)S(1)}, bf16[128,1024]{1,0:T(8,128)(2,1)}, u32[]{:S(2)}) copy-start(bf16[128,1024]{1,0:T(8,128)(2,1)} %get-tuple-element.72) | copy-start | bytes 786436
Sparse Core Ops, SparseCore 0:
  10.3 58.4 all-gather.1

commit v3 on v2

--- a/solution.py
+++ b/solution.py
@@ -51,20 +51,6 @@
         rows.append(jnp.sum(hits * rank, axis=0, keepdims=True))
         before = before + jnp.sum(hits, axis=1, keepdims=True)
     return [routes[k : k + 1, :] * CAP + rows[k].astype(jnp.int32) for k in range(top)]
-
-
-def slots_in_columns(routes, experts):
-    tokens, top = routes.shape
-    ids = iota((tokens, experts), 1)
-    earlier = (iota((tokens, tokens), 1) < iota((tokens, tokens), 0)).astype(BF16)
-    before = jnp.zeros((1, experts), F32)
-    columns = []
-    for k in range(top):
-        hits = (ids == routes[:, k : k + 1]).astype(F32)
-        rank = dot(earlier, hits.astype(BF16)) + before
-        columns.append(jnp.sum(hits * rank, axis=1, keepdims=True))
-        before = before + jnp.sum(hits, axis=0, keepdims=True)
-    return [routes[:, k : k + 1] * CAP + columns[k].astype(jnp.int32) for k in range(top)]
 
 
 def pack_kernel(experts, routes_ref, weights_ref, stream_ref, grads_ref, out_ref):
@@ -104,6 +90,55 @@
     return packed.reshape(experts, 4 * CAP, half)
 
 
+def hop(i, n_sp):
+    return lax.rem(i * 11, n_sp)
+
+
+def ring_reduce(piece, place, to_right, to_left, from_left, from_right, sum_right, sum_left, sems):
+    s_r, s_l, r_l, r_r = sems
+    right, left, far = lax.rem(place + 1, 4), lax.rem(place + 3, 4), lax.rem(place + 2, 4)
+
+    def right_copy(k, src):
+        return pltpu.make_async_remote_copy(
+            src, from_left.at[k], s_r.at[k], r_l.at[k], to_right, MESH
+        )
+
+    def left_copy(k, src):
+        return pltpu.make_async_remote_copy(
+            src, from_right.at[k], s_l.at[k], r_r.at[k], to_left, MESH
+        )
+
+    def start():
+        right_copy(0, piece(far, 0)).start()
+        left_copy(0, piece(far, 1)).start()
+        right_copy(1, piece(right, 1)).start()
+        left_copy(1, piece(left, 0)).start()
+
+    def middle():
+        right_copy(0, piece(far, 0)).wait()
+        sum_right[...] = (piece(right, 0)[...].astype(F32) + from_left[0].astype(F32)).astype(BF16)
+        left_copy(0, piece(far, 1)).wait()
+        sum_left[...] = (piece(left, 1)[...].astype(F32) + from_right[0].astype(F32)).astype(BF16)
+        right_copy(2, sum_right).start()
+        left_copy(2, sum_left).start()
+
+    def finish():
+        right_copy(1, piece(right, 1)).wait()
+        left_copy(1, piece(left, 0)).wait()
+        right_copy(2, sum_right).wait()
+        left_copy(2, sum_left).wait()
+
+    def total(w, at=()):
+        near, across = (from_left, from_right) if w == 0 else (from_right, from_left)
+        return (
+            piece(place, w)[at or Ellipsis].astype(F32)
+            + near[(2,) + at].astype(F32)
+            + across[(1,) + at].astype(F32)
+        )
+
+    return start, middle, finish, total
+
+
 def greet(me, tp, n_sp, n_tp, step=1, ring=False, partner=None):
     barrier = pltpu.get_barrier_semaphore()
 
@@ -165,7 +200,7 @@
     return dot_split(log_decay, upto, 3, ((1,), (0,)), left=False)
 
 
-def in_rows(x):
+def turned(x):
     n = x.shape[1]
     return dot_split(x, triangle(n, lambda a, b: a == b), 3, ((1,), (1,)), left=False)
 
@@ -191,7 +226,7 @@
     dt_ref,
     rate_ref,
     extra_ref,
-    first_ref,
+    first_hbm,
     b_ref,
     c_ref,
     gate_ref,
@@ -223,8 +258,12 @@
     d_recvs,
     b_sends,
     b_recvs,
+    first_ref,
+    first_sem,
 ):
     me, tp = lax.axis_index("sp"), lax.axis_index("tp")
+    entering = pltpu.make_async_copy(first_hbm.at[me], first_ref, first_sem)
+    entering.start()
     right, left = lax.rem(tp + 1, n_tp), lax.rem(tp + n_tp - 1, n_tp)
     far = lax.rem(tp + 2, n_tp)
     greet(me, tp, n_sp, n_tp, ring=True)
@@ -262,21 +301,21 @@
         )
 
     def start_exchange(d, carry):
-        exchange(d).start()
+        exchange(hop(d, n_sp)).start()
         return carry
 
     lax.fori_loop(1, n_sp, start_exchange, 0)
     mine = pltpu.make_async_copy(in_ref.at[me], out_ref.at[tp, me], own)
     mine.start()
 
-    tokens, heads = dt_ref.shape
+    heads, tokens = dt_ref.shape
     channels = x_ref.shape[1]
     groups = b_ref.shape[1] // STATE
     wide = channels // groups
     owner = head_spread(heads, HDIM)
-    dt = dt_ref[...]
-    cum = cumulative_decay(dt, rate_ref[...], extra_ref[...])
-    cum_rows = in_rows(cum)
+    dt = turned(dt_ref[...])
+    cum = cumulative_decay(dt, rate_ref[...], turned(extra_ref[...]))
+    cum_rows = turned(cum)
     last = cum[tokens - 1 : tokens, :]
     values = x_ref[...].astype(F32)
     ending = (values * spread(dt * jnp.exp(last - cum), owner)).astype(BF16)
@@ -319,8 +358,8 @@
         )
 
     def start_states(d, carry):
-        decay_copy(d).start()
-        state_copy(d).start()
+        decay_copy(hop(d, n_sp)).start()
+        state_copy(hop(d, n_sp)).start()
         return carry
 
     lax.fori_loop(1, n_sp, start_states, 0)
@@ -329,7 +368,8 @@
     kept.start()
     kept_too.start()
 
-    def spread_out(d, carry):
+    def spread_out(i, carry):
+        d = hop(i, n_sp)
         arrived(d).wait_recv()
         to_right(d, tp).start()
         to_left(d, tp).start()
@@ -364,13 +404,14 @@
         return carry
 
     lax.fori_loop(1, n_sp, finish_states, 0)
+    entering.wait()
     running = first_ref[...]
     for i in range(n_sp):
         carries[i] = running.astype(BF16)
         running = decays[i] * running + states[i].astype(F32)
 
     def start_back(d, carry):
-        back_copy(d).start()
+        back_copy(hop(d, n_sp)).start()
         return carry
 
     lax.fori_loop(1, n_sp, start_back, 0)
@@ -378,11 +419,11 @@
     kept_back.start()
 
     def relay(q, carry):
-        d = 2 * q
+        d, e = hop(2 * q, n_sp), hop(2 * q + 1, n_sp)
         to_right(d, left).wait_recv()
         onward(d, left, right).start()
-        to_left(d + 1, right).wait_recv()
-        onward(d + 1, right, left).start()
+        to_left(e, right).wait_recv()
+        onward(e, right, left).start()
         return carry
 
     lax.fori_loop(0, n_sp // 2, relay, 0)
@@ -407,15 +448,15 @@
         normed_ref[:, at] = (gated * factor * scale_ref[:, at]).astype(BF16)
 
     def finish(q, carry):
-        d = 2 * q
+        d, e = hop(2 * q, n_sp), hop(2 * q + 1, n_sp)
         to_left(d, right).wait_recv()
-        to_right(d + 1, left).wait_recv()
+        to_right(e, left).wait_recv()
         onward(d, far, right).wait()
-        onward(d + 1, far, left).wait()
+        onward(e, far, left).wait()
         to_right(d, tp).wait_send()
         to_left(d, tp).wait_send()
-        to_right(d + 1, tp).wait_send()
-        to_left(d + 1, tp).wait_send()
+        to_right(e, tp).wait_send()
+        to_left(e, tp).wait_send()
         return carry
 
     lax.fori_loop(0, n_sp // 2, finish, 0)
@@ -430,7 +471,7 @@
 def front(packed, x, dt, rate, extra, first, b, c, gate, scale, n_sp, n_tp):
     dma = pltpu.SemaphoreType.DMA
     tokens, channels = x.shape
-    rows, entries = first.shape
+    _, rows, entries = first.shape
     return pl.pallas_call(
         functools.partial(front_kernel, n_sp, n_tp),
         out_shape=(
@@ -439,7 +480,7 @@
             jax.ShapeDtypeStruct((tokens, channels), BF16),
             jax.ShapeDtypeStruct((n_sp, rows, entries), BF16),
         ),
-        in_specs=[vmem_spec()] * 10,
+        in_specs=[vmem_spec()] * 5 + [any_spec()] + [vmem_spec()] * 4,
         out_specs=(vmem_spec(),) * 4,
         scratch_shapes=[
             pltpu.VMEM((n_sp, rows, entries), BF16),
@@ -452,7 +493,8 @@
             dma,
             dma,
         ]
-        + [dma((n_sp,))] * 14,
+        + [dma((n_sp,))] * 14
+        + [pltpu.VMEM((rows, entries), F32), dma],
         compiler_params=pltpu.CompilerParams(
             collective_id=0, has_side_effects=True, vmem_limit_bytes=VMEM_BYTES
         ),
@@ -469,7 +511,9 @@
     down_hbm,
     routes_ref,
     grads_ref,
+    own_hbm,
     mix_ref,
+    all_hbm,
     dgate_hbm,
     dup_hbm,
     ddown_hbm,
@@ -504,6 +548,9 @@
     g_send,
     g_recv,
     local,
+    w_own,
+    w_sends,
+    w_recvs,
 ):
     me, tp = lax.axis_index("sp"), lax.axis_index("tp")
     right, left = lax.rem(tp + 1, n_tp), lax.rem(tp + n_tp - 1, n_tp)
@@ -527,6 +574,49 @@
             fetch.start()
     greet(me, tp, n_sp, n_tp, ring=True)
 
+    core = lax.rem(me, 2)
+    lane_y, lane_z = lax.rem(lax.div(me, 2), 4), lax.div(me, 8)
+
+    def at_y(y):
+        return lane_z * 8 + y * 2 + core
+
+    def at_z(z):
+        return z * 8 + lane_y * 2 + core
+
+    def weight_copy(k, src, dst, to):
+        return pltpu.make_async_remote_copy(
+            src, dst, w_sends.at[k], w_recvs.at[k], (to, tp), MESH
+        )
+
+    own_weight = pltpu.make_async_copy(own_hbm, all_hbm.at[core, lane_z, lane_y], w_own)
+    own_weight.start()
+
+    def first_stage(j, sending):
+        y, z = (lane_y, lane_z) if sending else (lax.rem(lane_y + 4 - j, 4), lax.rem(lane_z + 4 - j, 4))
+        return [
+            weight_copy(
+                j - 1, own_hbm.at[0], all_hbm.at[core, lane_z, y, 0], at_y(lax.rem(lane_y + j, 4))
+            ),
+            weight_copy(
+                j + 2, own_hbm.at[1], all_hbm.at[core, z, lane_y, 1], at_z(lax.rem(lane_z + j, 4))
+            ),
+        ]
+
+    def second_stage(j, sending):
+        y, z = (lane_y, lane_z) if sending else (lax.rem(lane_y + 4 - j, 4), lax.rem(lane_z + 4 - j, 4))
+        by_z, by_y = all_hbm.at[core, z, :, 0], all_hbm.at[core, :, y, 1]
+        return [
+            weight_copy(j + 5, by_z, by_z, at_z(lax.rem(lane_z + j, 4))),
+            weight_copy(j + 8, by_y, by_y, at_y(lax.rem(lane_y + j, 4))),
+        ]
+
+    def third_stage(c):
+        return weight_copy(12, all_hbm.at[c], all_hbm.at[c], me + 1 - 2 * core)
+
+    for j in range(1, 4):
+        for copy in first_stage(j, True):
+            copy.start()
+
     tall = in_ref.shape[2]
     group_of = 8
     span = group_of * CAP
@@ -561,6 +651,14 @@
         ).astype(BF16)
         up_grad[:, at] = (hidden_grad * activated).astype(BF16)
 
+    own_weight.wait()
+    for j in range(1, 4):
+        for copy in first_stage(j, False):
+            copy.wait_recv()
+    for j in range(1, 4):
+        for copy in second_stage(j, True):
+            copy.start()
+
     def row_block(b):
         for c in range(2):
             cols = pl.ds(pl.multiple_of(b * width + c * half, half), half)
@@ -625,13 +723,22 @@
         d_down[at, :] = dot(hidden[:, at], g[...], ((0,), (0,))).astype(BF16)
         save(16 + k, d_down.at[at, :], ddown_hbm.at[0, at, :])
 
-    slots = slots_in_columns(routes_ref[...], n_sp)
+    for j in range(1, 4):
+        for copy in second_stage(j, False):
+            copy.wait_recv()
+    third_stage(core).start()
+
+    by_token = slots_in_rows(routes_ref[...], n_sp)
+    line = iota((8, tokens), 0)
+    slots = turned(
+        jnp.where(line == 0, by_token[0], jnp.where(line == 1, by_token[1], 0)).astype(F32)
+    ).astype(jnp.int32)
     column = iota((1, n_sp * 4 * CAP), 1)
     expert = divide(column, 4 * CAP)
     place_in = column - expert * (4 * CAP)
     piece = divide(place_in, CAP)
     slot = expert * CAP + place_in - piece * CAP
-    match = (slots[0] == slot) | (slots[1] == slot)
+    match = (slots[:, 0:1] == slot) | (slots[:, 1:2] == slot)
 
     right_copy(1, block(right, 1)).wait()
     left_copy(1, block(left, 0)).wait()
@@ -674,7 +781,7 @@
         )
 
     def start_exchange(d, carry):
-        exchange(d).start()
+        exchange(hop(d, n_sp)).start()
         return carry
 
     lax.fori_loop(1, n_sp, start_exchange, 0)
@@ -717,9 +824,14 @@
     gather(1, own_cols, spot(tp), left).wait_send()
     for copy in saves:
         copy.wait()
-
-
-def experts_backward(arrived, w_gate, w_up, w_down, routes, grads, n_sp, n_tp):
+    for j in range(1, 4):
+        for copy in first_stage(j, True) + second_stage(j, True):
+            copy.wait_send()
+    third_stage(core).wait_send()
+    third_stage(1 - core).wait_recv()
+
+
+def experts_backward(arrived, w_gate, w_up, w_down, routes, grads, own, n_sp, n_tp):
     _, model, units = w_gate.shape
     rows = n_sp * CAP
     tokens, width = grads.shape
@@ -729,12 +841,13 @@
         functools.partial(expert_kernel, n_sp, n_tp),
         out_shape=(
             jax.ShapeDtypeStruct((tokens, width * n_tp), BF16),
+            jax.ShapeDtypeStruct((2, 4, 4) + own.shape, BF16),
             jax.ShapeDtypeStruct(w_gate.shape, BF16),
             jax.ShapeDtypeStruct(w_up.shape, BF16),
             jax.ShapeDtypeStruct(w_down.shape, BF16),
         ),
-        in_specs=[vmem_spec()] + [any_spec()] * 3 + [vmem_spec()] * 2,
-        out_specs=(vmem_spec(),) + (any_spec(),) * 3,
+        in_specs=[vmem_spec()] + [any_spec()] * 3 + [vmem_spec()] * 2 + [any_spec()],
+        out_specs=(vmem_spec(),) + (any_spec(),) * 4,
         scratch_shapes=[
             pltpu.VMEM((model, units), BF16),
             pltpu.VMEM((model, units), BF16),
@@ -767,12 +880,15 @@
             dma((4,)),
             dma((4,)),
             dma,
+            dma,
+            dma((13,)),
+            dma((13,)),
         ],
         compiler_params=pltpu.CompilerParams(
             collective_id=1, has_side_effects=True, vmem_limit_bytes=VMEM_BYTES
         ),
         name="experts",
-    )(arrived, w_gate, w_up, w_down, routes, grads)
+    )(arrived, w_gate, w_up, w_down, routes, grads, own)
 
 
 def tail_kernel(
@@ -801,9 +917,12 @@
     normed2,
     mix2,
     parts,
-    landed,
+    big_in,
+    big_sum,
+    small_in,
+    small_sum,
+    reduced,
     total,
-    other,
     state_mine,
     decay_mine,
     states,
@@ -816,8 +935,7 @@
     load,
     p_send,
     p_recv,
-    a_send,
-    a_recv,
+    ring_sems,
     sends,
     recvs,
     d_sends,
@@ -830,15 +948,18 @@
     partner = me + 1 - 2 * core
     chip = lax.div(me, 2)
     chips = n_sp // 2
-    fetch = pltpu.make_async_copy(weight_hbm, weight, load)
-    fetch.start()
+    fetches = [
+        pltpu.make_async_copy(weight_hbm.at[c], weight.at[:, c], load.at[c]) for c in range(2)
+    ]
+    for fetch in fetches:
+        fetch.start()
     greet(me, tp, n_sp, n_tp)
-    tokens, heads = dt_ref.shape
+    heads, tokens = dt_ref.shape
     channels = x_ref.shape[1]
     groups = b_ref.shape[1] // STATE
     wide = channels // groups
     half = channels // 2
-    cols = proj_ref.shape[1]
+    cols = proj_ref.shape[0]
     n_parts, rows, entries = state_mine.shape
     per_group = n_parts // groups
 
@@ -854,16 +975,57 @@
     pair(1, mix_ref, mix2).start()
 
     owner = head_spread(heads, HDIM)
-    dt = dt_ref[...]
-    cum = cumulative_decay(dt, rate_ref[...], extra_ref[...])
-    cum_rows = in_rows(cum)
+    dt = turned(dt_ref[...])
+    cum = cumulative_decay(dt, rate_ref[...], turned(extra_ref[...]))
+    cum_rows = turned(cum)
     last = cum[tokens - 1 : tokens, :]
     since = spread(jnp.exp(cum), owner)
-    fetch.wait()
+
+    mix_t = jnp.transpose(mix_ref[...])
+    pair(0, normed_ref.at[:, mine(1 - core)], normed2).wait()
+    pair(1, mix_ref, mix2).wait()
+    both_mix = jnp.concatenate([mix_t, jnp.transpose(mix2[...])], axis=1)
+    both_normed = jnp.concatenate([normed_ref[:, mine(core)], normed2[...]], axis=0)
+    piece_rows = cols // 2
+    for z in range(4):
+        at = slice(z * 8 * cols, (z + 1) * 8 * cols)
+        parts[z] = (
+            dot(both_mix[at, :], both_normed).astype(BF16).reshape(4, 2, 2, piece_rows, half)
+        )
+
+    lane_y, lane_z = lax.rem(chip, 4), lax.div(chip, 4)
+
+    def at_y(y):
+        return (lane_z * 8 + lax.rem(y, 4) * 2 + core, tp)
+
+    def at_z(z):
+        return (lax.rem(z, 4) * 8 + lane_y * 2 + core, tp)
+
+    y_ring = (lane_y, at_y(lane_y + 1), at_y(lane_y + 3))
+    z_ring = (lane_z, at_z(lane_z + 1), at_z(lane_z + 3))
+
+    def four(ref, k):
+        return [ref.at[k, i] for i in range(4)]
+
+    def bufs(landing, sums, k):
+        return [landing.at[k, 0], landing.at[k, 1], sums.at[k, 0], sums.at[k, 1]]
+
+    stages = [
+        ring_reduce(lambda b, w: parts.at[:, b, 0, w], *y_ring, *bufs(big_in, big_sum, 0), four(ring_sems, 0)),
+        ring_reduce(lambda b, w: parts.at[b, :, 1, w], *z_ring, *bufs(big_in, big_sum, 1), four(ring_sems, 1)),
+        ring_reduce(lambda b, w: reduced.at[0, w, b], *z_ring, *bufs(small_in, small_sum, 0), four(ring_sems, 2)),
+        ring_reduce(lambda b, w: reduced.at[1, w, b], *y_ring, *bufs(small_in, small_sum, 1), four(ring_sems, 3)),
+    ]
+    stages[0][0]()
+    stages[1][0]()
+
+    for fetch in fetches:
+        fetch.wait()
+    whole_weight = weight[...].reshape(mix_ref.shape[1], channels)
     d_y = []
     for g in range(groups):
         at = slice(g * wide, (g + 1) * wide)
-        normed_grad = dot(mix_ref[...], weight[at, :], ((1,), (1,)))
+        normed_grad = dot(mix_ref[...], whole_weight[:, at])
         y = y_ref[:, at]
         gate = gate_ref[:, at].astype(F32)
         sigmoid_gate = jax.nn.sigmoid(gate)
@@ -913,8 +1075,8 @@
         )
 
     def start_states(d, carry):
-        decay_copy(d).start()
-        state_copy(d).start()
+        decay_copy(hop(d, n_sp)).start()
+        state_copy(hop(d, n_sp)).start()
         return carry
 
     lax.fori_loop(1, n_sp, start_states, 0)
@@ -922,48 +1084,6 @@
     kept_too = pltpu.make_async_copy(decay_mine.at[me], decays.at[me], two)
     kept.start()
     kept_too.start()
-
-    pair(0, normed_ref.at[:, mine(1 - core)], normed2).wait()
-    pair(1, mix_ref, mix2).wait()
-    own_t = jnp.transpose(normed_ref[:, mine(core)])
-    other_t = jnp.transpose(normed2[...])
-    for c in range(chips):
-        at = slice(c * 2 * cols, (c + 1) * 2 * cols)
-        parts[c] = (dot(own_t, mix_ref[:, at]) + dot(other_t, mix2[:, at])).astype(BF16)
-
-    def exchange(d):
-        to = lax.rem(chip + d, chips)
-        return pltpu.make_async_remote_copy(
-            parts.at[to], landed.at[chip], a_send.at[d], a_recv.at[d], (2 * to + core, tp), MESH
-        )
-
-    def start_parts(d, carry):
-        exchange(d).start()
-        return carry
-
-    kept.wait()
-    kept_too.wait()
-
-    def finish_states(d, carry):
-        decay_copy(d).wait()
-        state_copy(d).wait()
-        return carry
-
-    lax.fori_loop(1, n_sp, finish_states, 0)
-    running = jnp.zeros((rows, entries), F32)
-    for step in range(n_sp):
-        i = n_sp - 1 - step
-        carries[i] = running.astype(BF16)
-        running = decays[i] * running + states[i].astype(F32)
-
-    def start_back(d, carry):
-        back_copy(d).start()
-        return carry
-
-    lax.fori_loop(1, n_sp, start_back, 0)
-    lax.fori_loop(1, chips, start_parts, 0)
-    kept_back = pltpu.make_async_copy(carries.at[me], later.at[me], one)
-    kept_back.start()
 
     values = x_ref[...].astype(F32)
     steps = spread(dt, owner)
@@ -973,9 +1093,10 @@
     not_before = triangle(tokens, lambda t, s: s >= t)
     below = (iota((tokens, tokens), 1) < iota((tokens, tokens), 0)).astype(F32)
     head_lane = iota((1, heads), 1)
-    crossing = jnp.zeros((tokens, heads), F32)
+    crossing = [jnp.zeros((tokens, heads), F32)]
     d_affinity = []
-    for g in range(groups):
+
+    def inside(g):
         affinity = dot(
             c_ref[:, g * STATE : (g + 1) * STATE],
             b_ref[:, g * STATE : (g + 1) * STATE],
@@ -1000,8 +1121,43 @@
                 over = jnp.sum(
                     reach[:, j * tokens : (j + 1) * tokens] * below, axis=1, keepdims=True
                 )
-                crossing = crossing + jnp.where(head_lane == 2 * q + j, over, 0.0)
+                crossing[0] = crossing[0] + jnp.where(head_lane == 2 * q + j, over, 0.0)
         d_affinity.append(sum_affinity.astype(BF16))
+
+    inside(0)
+    stages[0][1]()
+    stages[1][1]()
+    kept.wait()
+    kept_too.wait()
+
+    def finish_states(d, carry):
+        decay_copy(d).wait()
+        state_copy(d).wait()
+        return carry
+
+    lax.fori_loop(1, n_sp, finish_states, 0)
+    running = jnp.zeros((rows, entries), F32)
+    for step in range(n_sp):
+        i = n_sp - 1 - step
+        carries[i] = running.astype(BF16)
+        running = decays[i] * running + states[i].astype(F32)
+
+    def start_back(d, carry):
+        back_copy(hop(d, n_sp)).start()
+        return carry
+
+    lax.fori_loop(1, n_sp, start_back, 0)
+    kept_back = pltpu.make_async_copy(carries.at[me], later.at[me], one)
+    kept_back.start()
+
+    for g in range(1, groups):
+        inside(g)
+    for k in range(2):
+        stages[k][2]()
+        for w in range(2):
+            reduced[k, w] = stages[k][3](w).astype(BF16)
+    stages[2][0]()
+    stages[3][0]()
     read_out = []
     for g in range(groups):
         at = slice(g * wide, (g + 1) * wide)
@@ -1012,6 +1168,9 @@
             dot(d_affinity[g], b_ref[:, by]) + dot(since_low[:, at], incoming)
         ).astype(BF16)
     reading = by_head(since_grad * jnp.concatenate(read_out, axis=1), owner)
+
+    stages[2][1]()
+    stages[3][1]()
 
     kept_back.wait()
 
@@ -1049,31 +1208,33 @@
     )[0:1, :]
     earlier = triangle(tokens, lambda t, s: s < t)
     d_decay = (
-        crossing
+        crossing[0]
         + dot_split(reading, not_before, 3, ((1,), (0,)), left=False)
         + dot_split(stored, earlier, 3, ((1,), (0,)), left=False)
         + passing * whole
     )
-    ddt_ref[...] = direct - d_decay * rate_ref[...]
-
-    total[...] = parts[chip].astype(F32)
-
-    def finish_parts(d, carry):
-        exchange(d).wait()
-        total[...] += landed[lax.rem(chip + chips - d, chips)].astype(F32)
-        return carry
-
-    lax.fori_loop(1, chips, finish_parts, 0)
-    pair(2, total, other).start()
-    proj_ref[mine(core), :] = jnp.where(core == 0, total[:, :cols], total[:, cols:])
-    pair(2, total, other).wait()
-    proj_ref[mine(1 - core), :] = jnp.where(core == 0, other[:, :cols], other[:, cols:])
+    ddt_ref[...] = turned(direct - d_decay * rate_ref[...])
+
+    for k in range(2):
+        stages[2 + k][2]()
+        for w in range(2):
+            first = (2 * k + w) * piece_rows
+            total[first : first + piece_rows, :] = stages[2 + k][3](w)
+
+    def lines(c):
+        return pl.ds(pl.multiple_of(c * cols, cols), cols)
+
+    given = pair(2, total.at[lines(1 - core), :], proj_ref.at[:, mine(core)])
+    given.start()
+    proj_ref[:, mine(core)] = total[lines(core), :]
+    given.wait_send()
+    pair(2, total.at[lines(core), :], proj_ref.at[:, mine(1 - core)]).wait_recv()
 
 
 def tail(mix, weight, y, normed, x, dt, rate, extra, coming, b, c, gate, scale, n_sp, n_tp):
     dma = pltpu.SemaphoreType.DMA
     tokens, channels = x.shape
-    heads = dt.shape[1]
+    heads = dt.shape[0]
     _, rows, entries = coming.shape
     width = mix.shape[1]
     half = channels // 2
@@ -1082,9 +1243,9 @@
     return pl.pallas_call(
         functools.partial(tail_kernel, n_sp, n_tp),
         out_shape=(
-            jax.ShapeDtypeStruct((channels, cols), F32),
+            jax.ShapeDtypeStruct((cols, channels), F32),
             jax.ShapeDtypeStruct((tokens, channels), BF16),
-            jax.ShapeDtypeStruct((tokens, heads), F32),
+            jax.ShapeDtypeStruct((heads, tokens), F32),
             jax.ShapeDtypeStruct(b.shape, BF16),
             jax.ShapeDtypeStruct(c.shape, BF16),
             jax.ShapeDtypeStruct((tokens, channels), BF16),
@@ -1092,13 +1253,16 @@
         in_specs=[vmem_spec(), any_spec()] + [vmem_spec()] * 11,
         out_specs=(vmem_spec(),) * 6,
         scratch_shapes=[
-            pltpu.VMEM((channels, width), BF16),
+            pltpu.VMEM((chips, 2, cols, channels), BF16),
             pltpu.VMEM((tokens, half), BF16),
             pltpu.VMEM((tokens, width), BF16),
-            pltpu.VMEM((chips, half, 2 * cols), BF16),
-            pltpu.VMEM((chips, half, 2 * cols), BF16),
-            pltpu.VMEM((half, 2 * cols), F32),
-            pltpu.VMEM((half, 2 * cols), F32),
+            pltpu.VMEM((4, 4, 2, 2, cols // 2, half), BF16),
+            pltpu.VMEM((2, 2, 3, 4, cols // 2, half), BF16),
+            pltpu.VMEM((2, 2, 4, cols // 2, half), BF16),
+            pltpu.VMEM((2, 2, 3, cols // 2, half), BF16),
+            pltpu.VMEM((2, 2, cols // 2, half), BF16),
+            pltpu.VMEM((2, 2, 4, cols // 2, half), BF16),
+            pltpu.VMEM((2 * cols, half), F32),
             pltpu.VMEM((n_sp, rows, entries), BF16),
             pltpu.VMEM((n_sp, 1, entries), F32),
             pltpu.VMEM((n_sp, rows, entries), BF16),
@@ -1108,11 +1272,10 @@
             pltpu.VMEM((tokens, channels), F32),
             dma,
             dma,
-            dma,
+            dma((2,)),
             dma((3,)),
             dma((3,)),
-            dma((chips,)),
-            dma((chips,)),
+            dma((4, 4, 3)),
         ]
         + [dma((n_sp,))] * 6,
         compiler_params=pltpu.CompilerParams(
@@ -1120,6 +1283,50 @@
         ),
         name="tail",
     )(mix, weight, y, normed, x, dt, rate, extra, coming, b, c, gate, scale)
+
+
+def finish_kernel(count, *refs):
+    sources, results, held = refs[:count], refs[count : 2 * count], refs[2 * count : 3 * count]
+    loads, stores = refs[3 * count :]
+    copies = []
+    for i in range(count):
+        lines = sources[i].shape[-2]
+        pieces = 4 if lines > 512 else 1
+        for p in range(pieces):
+            at = pl.ds(p * (lines // pieces), lines // pieces)
+            views = [
+                ref.at[0, at, :] if len(ref.shape) == 3 else ref.at[at, :]
+                for ref in (sources[i], held[i], results[i])
+            ]
+            k = len(copies)
+            copies.append(
+                (
+                    pltpu.make_async_copy(views[0], views[1], loads.at[k]),
+                    pltpu.make_async_copy(views[1], views[2], stores.at[k]),
+                )
+            )
+    for load, _ in copies:
+        load.start()
+    for load, store in copies:
+        load.wait()
+        store.start()
+    for _, store in copies:
+        store.wait()
+
+
+def finish(*arrays):
+    count = len(arrays)
+    dma = pltpu.SemaphoreType.DMA
+    return pl.pallas_call(
+        functools.partial(finish_kernel, count),
+        out_shape=tuple(jax.ShapeDtypeStruct(a.shape, a.dtype) for a in arrays),
+        in_specs=[any_spec()] * count,
+        out_specs=(any_spec(),) * count,
+        scratch_shapes=[pltpu.VMEM(a.shape, a.dtype) for a in arrays]
+        + [dma((4 * count,)), dma((4 * count,))],
+        compiler_params=pltpu.CompilerParams(vmem_limit_bytes=VMEM_BYTES),
+        name="finish",
+    )(*arrays)
 
 
 def body(
@@ -1146,17 +1353,15 @@
     packed = pack(routes, expert_combine_weight, mixer_output_stream, layer_output_gradient, n_sp)
     heads = head_step_size.shape[1]
     part_rows = heads * HDIM // n_sp
-    entering = lax.dynamic_index_in_dim(
-        state_entering_span.reshape(n_sp, part_rows, STATE), lax.axis_index(SP), 0, keepdims=False
-    )
+    entering = state_entering_span.reshape(n_sp, part_rows, STATE)
     rate = head_decay_rate[None, :]
     scale = group_norm_scale[None, :]
     arrived, scan_out, normed_low, coming = front(
         packed,
         head_mixer_input,
-        head_step_size,
+        head_step_size.T,
         rate,
-        extra_log_decay,
+        extra_log_decay.T,
         entering,
         state_input_vectors,
         state_readout_vectors,
@@ -1165,26 +1370,27 @@
         n_sp,
         n_tp,
     )
-    mix_grad, grad_g, grad_u, grad_d = experts_backward(
+    mix_grad, weight, grad_g, grad_u, grad_d = experts_backward(
         arrived,
         expert_gate_weight,
         expert_up_weight,
         expert_down_weight,
-        routes,
+        routes.T,
         layer_output_gradient,
+        mixer_output_weight.T.reshape(2, -1, mixer_output_weight.shape[0]),
         n_sp,
         n_tp,
     )
-    weight = lax.all_gather(mixer_output_weight, SP, axis=1, tiled=True)
+    weight = weight.reshape(2, n_sp // 2, -1, mixer_output_weight.shape[0])
     proj_grad, input_grad, step_grad, b_grad, c_grad, gate_grad_in = tail(
         mix_grad,
         weight,
         scan_out,
         normed_low,
         head_mixer_input,
-        head_step_size,
+        head_step_size.T,
         rate,
-        extra_log_decay,
+        extra_log_decay.T,
         coming,
         state_input_vectors,
         state_readout_vectors,
@@ -1193,13 +1399,24 @@
         n_sp,
         n_tp,
     )
+    proj_grad, input_grad, step_grad, b_grad, c_grad, gate_grad_in, grad_g, grad_u, grad_d = finish(
+        proj_grad,
+        input_grad,
+        step_grad,
+        b_grad,
+        c_grad,
+        gate_grad_in,
+        grad_g,
+        grad_u,
+        grad_d,
+    )
     return (
         grad_g,
         grad_u,
         grad_d,
-        proj_grad,
+        proj_grad.T,
         input_grad,
-        step_grad,
+        step_grad.T,
         b_grad,
         c_grad,
         gate_grad_in,

time: 198 us -> 147 us (0.74)
  local copies, waits for them, and re-layouts: 27.1 us -> 0 us
  between operations: 14.1 us -> 0.85 us
  Pallas kernels: 154 us -> 145 us
    unnamed x26 -> x0, local copies, waits for them, and re-layouts: 19.9 us -> none
    pallas_call x1, Pallas kernels: 53.3 us -> 34.8 us  [tail(): pl.pallas_call(functools.partial(tail_kernel, n_sp, n_tp), out_shape=(jax...]
    pallas_call x0 -> x1, Pallas kernels: none -> 9.21 us  [finish(): pl.pallas_call(functools.partial(finish_kernel, count), out_shape=tuple((...]
    all_gather x1 -> x0, local copies, waits for them, and re-layouts: 6.56 us -> none  [body(): weight = lax.all_gather(mixer_output_weight, SP, axis=1, tiled=True)]
  transfers between devices with their start and end apart: 1 -> 0, of which waited for: 0 -> 0; matrix products, arithmetic and copies ran while one was open for 2% -> 0% of each run, Pallas kernels for 52% -> 0%
where the time goes in v3:
time: 147 us; the launch traced here: 146 us
  Pallas kernels  145 us (99%)
    pallas_call x1, Pallas kernels, experts_backward(): pl.pallas_call(functools.partial(expert_kernel, n_sp, n_tp), out_shape=(j...  50.1 us
    pallas_call x1, Pallas kernels, front(): pl.pallas_call(functools.partial(front_kernel, n_sp, n_tp), out_shape=(ja...  47.2 us
    pallas_call x1, Pallas kernels, tail(): pl.pallas_call(functools.partial(tail_kernel, n_sp, n_tp), out_shape=(jax...  34.8 us
    pallas_call x1, Pallas kernels, finish(): pl.pallas_call(functools.partial(finish_kernel, count), out_shape=tuple((...  9.21 us
    pallas_call x1, Pallas kernels, pack(): pl.pallas_call(functools.partial(pack_kernel, experts), out_shape=jax.Sha...  3.42 us

profile of v3, /device:TPU:0, one launch (start us, length us, event | category | flops | bytes accessed | tf_op | source)
XLA Modules:
  0.0 145.6 jit_solution(11901339095657704883)
XLA Ops:
  0.6 3.4 %pack.1 = bf16[1536,256]{1,0:T(8,128)(2,1)} custom-call(s32[2,128]{1,0:T(2,128)} %bitcast.24, f32[2,128]{1,0:T(2,128)} %bitcast.28, bf16[128,512]{1,0:T(8,128)(2,1)} %stream_ref.1, bf16[128,512]{1,0:T(8,128)(2,1)} %grads_ref.3), custom_call_target="tpu_custom_call" | custom-call | tf_op jit(solution)/shard_map/pack/pallas_call | solution.py:82
  4.1 47.2 %front.1 = (bf16[4,32,48,256]{3,2,1,0:T(8,128)(2,1)}, f32[128,1024]{1,0:T(8,128)}, bf16[128,1024]{1,0:T(8,128)(2,1)}, bf16[32,32,128]{2,1,0:T(8,128)(2,1)}) custom-call(bf16[32,48,256]{2,1,0:T(8,128)(2,1)} %bitcast.15, bf16[128,1024]{1,0:T(8,128)(2,1)} %x_ref.3, f32[16,128]{1,0:T(8,128)} %bitcast.18, f32[1,16]{1,0:T(1,128)} %bitcast.26, f32[16,128]{1,0:T(8,128)} %bitcast.20, ...), custom_call_target="tpu_custom_call" | custom-call | tf_op jit(solution)/shard_map/front/pallas_call | solution.py:475
  51.3 50.1 %experts.1 = (bf16[128,2048]{1,0:T(8,128)(2,1)}, bf16[2,4,4,2,32,1024]{5,4,3,2,1,0:T(8,128)(2,1)}, bf16[1,2048,896]{2,1,0:T(8,128)(2,1)}, bf16[1,2048,896]{2,1,0:T(8,128)(2,1)}, bf16[1,896,2048]{2,1,0:T(8,128)(2,1)}) custom-call(bf16[4,32,48,256]{3,2,1,0:T(8,128)(2,1)} %get-tuple-element.33.in_ref, bf16[1,2048,896]{2,1,0:T(8,128)(2,1)} %gate_hbm.1, ...), custom_call_target="tpu_custom_call" | custom-call | tf_op jit(solution)/shard_map/experts/pallas_call | solution.py:840
  101.4 34.8 %tail.1 = (f32[64,1024]{1,0:T(8,128)}, bf16[128,1024]{1,0:T(8,128)(2,1)}, f32[16,128]{1,0:T(8,128)}, bf16[128,256]{1,0:T(8,128)(2,1)}, bf16[128,256]{1,0:T(8,128)(2,1)}, /*index=5*/bf16[128,1024]{1,0:T(8,128)(2,1)}) custom-call(bf16[128,2048]{1,0:T(8,128)(2,1)} %get-tuple-element.34.mix_ref, bf16[2,16,64,1024]{3,2,1,0:T(8,128)(2,1)} %bitcast.14, ...), custom_call_target="tpu_custom_call" | custom-call | tf_op jit(solution)/shard_map/tail/pallas_call | solution.py:1243
  136.2 9.2 %finish.1 = (f32[64,1024]{1,0:T(8,128)}, bf16[128,1024]{1,0:T(8,128)(2,1)}, f32[16,128]{1,0:T(8,128)}, bf16[128,256]{1,0:T(8,128)(2,1)}, bf16[128,256]{1,0:T(8,1...) custom-call(f32[64,1024]{1,0:T(8,128)} %get-tuple-element.39.refs_0_, ...), custom_call_target="tpu_custom_call" | custom-call | tf_op jit(solution)/shard_map/finish/pallas_call | solution.py:1320

commit v4 on v3

--- a/solution.py
+++ b/solution.py
@@ -53,7 +53,7 @@
     return [routes[k : k + 1, :] * CAP + rows[k].astype(jnp.int32) for k in range(top)]
 
 
-def pack_kernel(experts, routes_ref, weights_ref, stream_ref, grads_ref, out_ref):
+def pack(experts, routes_ref, weights_ref, stream_ref, grads_ref, out_ref):
     tokens = stream_ref.shape[0]
     half = stream_ref.shape[1] // 2
     slots = slots_in_rows(routes_ref[...], experts)
@@ -74,20 +74,7 @@
     g1 = dot(match, grads_ref[:, half:])
     low = jnp.where(part == 0, x0, g0 * weight)
     high = jnp.where(part == 2, x1, g1 * weight)
-    out_ref[...] = jnp.where(part < 2, low, high).astype(BF16)
-
-
-def pack(routes, weights, stream, grads, experts):
-    half = stream.shape[1] // 2
-    packed = pl.pallas_call(
-        functools.partial(pack_kernel, experts),
-        out_shape=jax.ShapeDtypeStruct((experts * 4 * CAP, half), BF16),
-        in_specs=[vmem_spec()] * 4,
-        out_specs=vmem_spec(),
-        compiler_params=pltpu.CompilerParams(vmem_limit_bytes=VMEM_BYTES),
-        name="pack",
-    )(routes.T, weights.T, stream, grads)
-    return packed.reshape(experts, 4 * CAP, half)
+    out_ref[...] = jnp.where(part < 2, low, high).astype(BF16).reshape(out_ref.shape)
 
 
 def hop(i, n_sp):
@@ -139,25 +126,22 @@
     return start, middle, finish, total
 
 
-def greet(me, tp, n_sp, n_tp, step=1, ring=False, partner=None):
+def greet(me, tp, n_sp, n_tp, ring=False):
     barrier = pltpu.get_barrier_semaphore()
 
     def hello(d, carry):
         pl.semaphore_signal(
-            barrier, inc=1, device_id=(lax.rem(me + d * step, n_sp), tp), device_id_type=MESH
+            barrier, inc=1, device_id=(lax.rem(me + d, n_sp), tp), device_id_type=MESH
         )
         return carry
 
-    lax.fori_loop(1, n_sp // step, hello, 0)
-    count = n_sp // step - 1
-    if partner is not None:
-        pl.semaphore_signal(barrier, inc=1, device_id=(partner, tp), device_id_type=MESH)
-        count += 1
+    lax.fori_loop(1, n_sp, hello, 0)
+    count = n_sp - 1
     if ring:
         for other in (lax.rem(tp + 1, n_tp), lax.rem(tp + n_tp - 1, n_tp)):
             pl.semaphore_signal(barrier, inc=1, device_id=(me, other), device_id_type=MESH)
         count += 2
-    pl.semaphore_wait(barrier, count)
+    return lambda: pl.semaphore_wait(barrier, count)
 
 
 def split(x, pieces):
@@ -218,9 +202,12 @@
     return jnp.concatenate([jnp.where(lane < size, pair, zero), jnp.where(lane < size, zero, pair)], axis=0)
 
 
-def front_kernel(
+def front_part(
     n_sp,
     n_tp,
+    begin,
+    prepare,
+    between,
     in_ref,
     x_ref,
     dt_ref,
@@ -235,10 +222,10 @@
     y_ref,
     normed_ref,
     coming,
+    decays,
     state_mine,
     decay_mine,
     states,
-    decays,
     carries,
     diag,
     own,
@@ -264,49 +251,83 @@
     me, tp = lax.axis_index("sp"), lax.axis_index("tp")
     entering = pltpu.make_async_copy(first_hbm.at[me], first_ref, first_sem)
     entering.start()
+    begin()
     right, left = lax.rem(tp + 1, n_tp), lax.rem(tp + n_tp - 1, n_tp)
     far = lax.rem(tp + 2, n_tp)
-    greet(me, tp, n_sp, n_tp, ring=True)
-
-    def origin(d):
-        return lax.rem(me + n_sp - d, n_sp)
-
-    def exchange(d):
-        to = lax.rem(me + d, n_sp)
-        return pltpu.make_async_remote_copy(
-            in_ref.at[to], out_ref.at[tp, me], a_send.at[d], a_recv.at[d], (to, tp), MESH
-        )
-
-    def arrived(d):
-        return pltpu.make_async_remote_copy(
-            in_ref.at[me], out_ref.at[tp, origin(d)], a_send.at[d], a_recv.at[d], (me, tp), MESH
-        )
-
-    def to_right(d, block):
-        piece = out_ref.at[block, origin(d)]
-        return pltpu.make_async_remote_copy(
-            piece, piece, s_right.at[d], r_left.at[d], (me, right), MESH
-        )
-
-    def to_left(d, block):
-        piece = out_ref.at[block, origin(d)]
-        return pltpu.make_async_remote_copy(
-            piece, piece, s_left.at[d], r_right.at[d], (me, left), MESH
-        )
-
-    def onward(d, block, to):
-        piece = out_ref.at[block, origin(d)]
-        return pltpu.make_async_remote_copy(
-            piece, piece, f_send.at[d], f_recv.at[d], (me, to), MESH
-        )
-
-    def start_exchange(d, carry):
-        exchange(hop(d, n_sp)).start()
-        return carry
-
-    lax.fori_loop(1, n_sp, start_exchange, 0)
+    met = greet(me, tp, n_sp, n_tp, ring=True)
+    prepare()
+    met()
+
+    low, plane = lax.rem(me, 8), lax.div(me, 8)
+    away = (0, 1, 3, 2)
+
+    def planes_off(j):
+        return lax.rem(plane + 4 - away[j], 4)
+
+    def exchange(j, k):
+        to = lax.rem(plane + away[j], 4) * 8 + lax.rem(low + k, 8)
+        return pltpu.make_async_remote_copy(
+            in_ref.at[to],
+            out_ref.at[tp, me],
+            a_send.at[8 * j + k],
+            a_recv.at[8 * j + k],
+            (to, tp),
+            MESH,
+        )
+
+    def arrived(j, k):
+        source = planes_off(j) * 8 + lax.rem(low + 8 - k, 8)
+        return pltpu.make_async_remote_copy(
+            in_ref.at[me],
+            out_ref.at[tp, source],
+            a_send.at[8 * j + k],
+            a_recv.at[8 * j + k],
+            (me, tp),
+            MESH,
+        )
+
+    def to_right(j, block):
+        piece = out_ref.at[block, pl.ds(pl.multiple_of(planes_off(j) * 8, 8), 8)]
+        return pltpu.make_async_remote_copy(
+            piece, piece, s_right.at[j], r_left.at[j], (me, right), MESH
+        )
+
+    def to_left(j, block):
+        piece = out_ref.at[block, pl.ds(pl.multiple_of(planes_off(j) * 8, 8), 8)]
+        return pltpu.make_async_remote_copy(
+            piece, piece, s_left.at[j], r_right.at[j], (me, left), MESH
+        )
+
+    def onward(j, block, rightward):
+        first = planes_off(j) * 8 + (0 if rightward else 4)
+        piece = out_ref.at[block, pl.ds(pl.multiple_of(first, 4), 4)]
+        at = j if rightward else 4 + j
+        return pltpu.make_async_remote_copy(
+            piece, piece, f_send.at[at], f_recv.at[at], (me, right if rightward else left), MESH
+        )
+
+    for j in range(4):
+
+        def start_exchange(k, carry, j=j):
+            exchange(j, k).start()
+            return carry
+
+        lax.fori_loop(1 if j == 0 else 0, 8, start_exchange, 0)
+
+    def pass_on(j):
+        def await_chunk(k, carry):
+            arrived(j, k).wait_recv()
+            return carry
+
+        lax.fori_loop(1 if j == 0 else 0, 8, await_chunk, 0)
+        to_right(j, tp).start()
+        to_left(j, tp).start()
+
     mine = pltpu.make_async_copy(in_ref.at[me], out_ref.at[tp, me], own)
     mine.start()
+
+    mine.wait()
+    pass_on(0)
 
     heads, tokens = dt_ref.shape
     channels = x_ref.shape[1]
@@ -335,9 +356,6 @@
         h = p * rows // HDIM
         decay_mine[p] = jnp.broadcast_to(total[:, h : h + 1], (1, entries))
 
-    mine.wait()
-    to_right(0, tp).start()
-    to_left(0, tp).start()
 
     def state_copy(d):
         to = lax.rem(me + d, n_sp)
@@ -368,14 +386,7 @@
     kept.start()
     kept_too.start()
 
-    def spread_out(i, carry):
-        d = hop(i, n_sp)
-        arrived(d).wait_recv()
-        to_right(d, tp).start()
-        to_left(d, tp).start()
-        return carry
-
-    lax.fori_loop(1, n_sp, spread_out, 0)
+    pass_on(1)
 
     scaled = (values * spread(dt, owner)).astype(BF16)
     affinity = [
@@ -394,6 +405,9 @@
         )
         at = slice(q * 2 * HDIM, (q + 1) * 2 * HDIM)
         diag[:, at] = dot(both, halves(scaled[:, at]))
+        if q == heads // 4 - 1:
+            pass_on(2)
+    pass_on(3)
 
     kept.wait()
     kept_too.wait()
@@ -418,15 +432,11 @@
     kept_back = pltpu.make_async_copy(carries.at[me], coming.at[me], one)
     kept_back.start()
 
-    def relay(q, carry):
-        d, e = hop(2 * q, n_sp), hop(2 * q + 1, n_sp)
-        to_right(d, left).wait_recv()
-        onward(d, left, right).start()
-        to_left(e, right).wait_recv()
-        onward(e, right, left).start()
-        return carry
-
-    lax.fori_loop(0, n_sp // 2, relay, 0)
+    for j in range(4):
+        to_right(j, left).wait_recv()
+        onward(j, left, True).start()
+        to_left(j, right).wait_recv()
+        onward(j, right, False).start()
     kept_back.wait()
 
     def finish_back(d, carry):
@@ -447,62 +457,21 @@
         factor = lax.rsqrt(jnp.mean(gated * gated, axis=1, keepdims=True) + norm_eps)
         normed_ref[:, at] = (gated * factor * scale_ref[:, at]).astype(BF16)
 
-    def finish(q, carry):
-        d, e = hop(2 * q, n_sp), hop(2 * q + 1, n_sp)
-        to_left(d, right).wait_recv()
-        to_right(e, left).wait_recv()
-        onward(d, far, right).wait()
-        onward(e, far, left).wait()
-        to_right(d, tp).wait_send()
-        to_left(d, tp).wait_send()
-        to_right(e, tp).wait_send()
-        to_left(e, tp).wait_send()
-        return carry
-
-    lax.fori_loop(0, n_sp // 2, finish, 0)
-
-    def drain(d, carry):
-        exchange(d).wait_send()
-        return carry
-
-    lax.fori_loop(1, n_sp, drain, 0)
-
-
-def front(packed, x, dt, rate, extra, first, b, c, gate, scale, n_sp, n_tp):
-    dma = pltpu.SemaphoreType.DMA
-    tokens, channels = x.shape
-    _, rows, entries = first.shape
-    return pl.pallas_call(
-        functools.partial(front_kernel, n_sp, n_tp),
-        out_shape=(
-            jax.ShapeDtypeStruct((n_tp,) + packed.shape, BF16),
-            jax.ShapeDtypeStruct((tokens, channels), F32),
-            jax.ShapeDtypeStruct((tokens, channels), BF16),
-            jax.ShapeDtypeStruct((n_sp, rows, entries), BF16),
-        ),
-        in_specs=[vmem_spec()] * 5 + [any_spec()] + [vmem_spec()] * 4,
-        out_specs=(vmem_spec(),) * 4,
-        scratch_shapes=[
-            pltpu.VMEM((n_sp, rows, entries), BF16),
-            pltpu.VMEM((n_sp, 1, entries), F32),
-            pltpu.VMEM((n_sp, rows, entries), BF16),
-            pltpu.VMEM((n_sp, 1, entries), F32),
-            pltpu.VMEM((n_sp, rows, entries), BF16),
-            pltpu.VMEM((tokens, channels), F32),
-            dma,
-            dma,
-            dma,
-        ]
-        + [dma((n_sp,))] * 14
-        + [pltpu.VMEM((rows, entries), F32), dma],
-        compiler_params=pltpu.CompilerParams(
-            collective_id=0, has_side_effects=True, vmem_limit_bytes=VMEM_BYTES
-        ),
-        name="front",
-    )(packed, x, dt, rate, extra, first, b, c, gate, scale)
-
-
-def expert_kernel(
+    between()
+    for j in range(4):
+        onward(j, far, True).wait()
+        onward(j, far, False).wait()
+        to_right(j, tp).wait_send()
+        to_left(j, tp).wait_send()
+
+        def drain(k, carry, j=j):
+            exchange(j, k).wait_send()
+            return carry
+
+        lax.fori_loop(1 if j == 0 else 0, 8, drain, 0)
+
+
+def expert_part(
     n_sp,
     n_tp,
     in_ref,
@@ -551,6 +520,7 @@
     w_own,
     w_sends,
     w_recvs,
+    so_far,
 ):
     me, tp = lax.axis_index("sp"), lax.axis_index("tp")
     right, left = lax.rem(tp + 1, n_tp), lax.rem(tp + n_tp - 1, n_tp)
@@ -572,7 +542,7 @@
         )
         for fetch in fetches[-1]:
             fetch.start()
-    greet(me, tp, n_sp, n_tp, ring=True)
+    yield
 
     core = lax.rem(me, 2)
     lane_y, lane_z = lax.rem(lax.div(me, 2), 4), lax.div(me, 8)
@@ -627,22 +597,45 @@
     row = src * CAP + inner - which * CAP
     lines = iota((span, 1), 0)
     pick = [((row == lines) & (which == p)).astype(BF16) for p in range(4)]
-    for t in range(n_tp):
+
+    def columns_of(b):
+        return pl.ds(pl.multiple_of(b * width, width), width)
+
+    def select(b):
         for k in range(n_sp // group_of):
-            block = in_ref[t, k * group_of : (k + 1) * group_of].reshape(group_of * tall, half)
+            block = in_ref[b, k * group_of : (k + 1) * group_of].reshape(group_of * tall, half)
             at = slice(k * span, (k + 1) * span)
             for c in range(2):
-                cols = slice((2 * t + c) * half, (2 * t + c + 1) * half)
+                cols = pl.ds(pl.multiple_of(b * width + c * half, half), half)
                 x[at, cols] = dot(pick[2 * c], block).astype(BF16)
                 g[at, cols] = dot(pick[2 * c + 1], block).astype(BF16)
 
+    def products(b, at):
+        cols = columns_of(b)
+        return (
+            dot(x[:, cols], w_gate[cols, at]),
+            dot(x[:, cols], w_up[cols, at]),
+            dot(g[:, cols], w_down[at, cols], ((1,), (1,))),
+        )
+
+    near = (tp, left, right)
+    for b in near:
+        select(b)
     for k, (start, size) in enumerate(cuts):
         for fetch in fetches[k]:
             fetch.wait()
         at = slice(start, start + size)
-        pre_gate = dot(x[...], w_gate[:, at])
-        pre_up = dot(x[...], w_up[:, at])
-        hidden_grad = dot(g[...], w_down[at, :], ((1,), (1,)))
+        sums = [products(b, at) for b in near]
+        for i in range(3):
+            so_far[i, :, at] = sums[0][i] + sums[1][i] + sums[2][i]
+    yield
+    select(far)
+    for start, size in cuts:
+        at = slice(start, start + size)
+        last_gate, last_up, last_grad = products(far, at)
+        pre_gate = so_far[0, :, at] + last_gate
+        pre_up = so_far[1, :, at] + last_up
+        hidden_grad = so_far[2, :, at] + last_grad
         sigmoid_gate = jax.nn.sigmoid(pre_gate)
         activated = pre_gate * sigmoid_gate
         hidden[:, at] = (activated * pre_up).astype(BF16)
@@ -831,64 +824,154 @@
     third_stage(1 - core).wait_recv()
 
 
-def experts_backward(arrived, w_gate, w_up, w_down, routes, grads, own, n_sp, n_tp):
+FRONT_SCRATCH = 24
+
+
+def main_kernel(n_sp, n_tp, *refs):
+    (stream, weights, x, dt, rate, extra, first, b, c, gate, scale) = refs[:11]
+    (w_gate, w_up, w_down, routes, grads, own) = refs[11:17]
+    (y, normed, coming, decays) = refs[17:21]
+    expert_outs = refs[21:26]
+    packed, arrived = refs[26:28]
+    front_scratch = refs[28 : 28 + FRONT_SCRATCH]
+    expert_scratch = refs[28 + FRONT_SCRATCH :]
+    steps = expert_part(
+        n_sp,
+        n_tp,
+        arrived,
+        w_gate,
+        w_up,
+        w_down,
+        routes,
+        grads,
+        own,
+        *expert_outs,
+        *expert_scratch,
+    )
+    front_part(
+        n_sp,
+        n_tp,
+        lambda: next(steps),
+        lambda: pack(n_sp, routes, weights, stream, grads, packed),
+        lambda: next(steps),
+        packed,
+        x,
+        dt,
+        rate,
+        extra,
+        first,
+        b,
+        c,
+        gate,
+        scale,
+        arrived,
+        y,
+        normed,
+        coming,
+        decays,
+        *front_scratch,
+    )
+    for _ in steps:
+        pass
+
+
+def main(
+    stream, weights, x, dt, rate, extra, first, b, c, gate, scale, w_gate, w_up, w_down, routes, grads, own, n_sp, n_tp
+):
+    dma = pltpu.SemaphoreType.DMA
+    tokens, channels = x.shape
+    _, rows, entries = first.shape
     _, model, units = w_gate.shape
-    rows = n_sp * CAP
-    tokens, width = grads.shape
+    pairs = n_sp * CAP
+    width = grads.shape[1]
     half, quarter = width // 2, width // 4
-    dma = pltpu.SemaphoreType.DMA
+    front_scratch = (
+        [
+            pltpu.VMEM((n_sp, rows, entries), BF16),
+            pltpu.VMEM((n_sp, 1, entries), F32),
+            pltpu.VMEM((n_sp, rows, entries), BF16),
+            pltpu.VMEM((n_sp, rows, entries), BF16),
+            pltpu.VMEM((tokens, channels), F32),
+            dma,
+            dma,
+            dma,
+        ]
+        + [dma((n_sp,))] * 2
+        + [dma((4,))] * 4
+        + [dma((8,))] * 2
+        + [dma((n_sp,))] * 6
+        + [pltpu.VMEM((rows, entries), F32), dma]
+    )
+    expert_scratch = [
+        pltpu.VMEM((model, units), BF16),
+        pltpu.VMEM((model, units), BF16),
+        pltpu.VMEM((units, model), BF16),
+        pltpu.VMEM((model, units), BF16),
+        pltpu.VMEM((model, units), BF16),
+        pltpu.VMEM((units, model), BF16),
+        pltpu.VMEM((pairs, model), BF16),
+        pltpu.VMEM((model, pairs), BF16),
+        pltpu.VMEM((pairs, model), BF16),
+        pltpu.VMEM((pairs, units), BF16),
+        pltpu.VMEM((pairs, units), BF16),
+        pltpu.VMEM((pairs, units), BF16),
+        pltpu.VMEM((2 * n_tp, pairs, half), BF16),
+        pltpu.VMEM((3, pairs, half), BF16),
+        pltpu.VMEM((3, pairs, half), BF16),
+        pltpu.VMEM((pairs, half), BF16),
+        pltpu.VMEM((pairs, half), BF16),
+        pltpu.VMEM((n_sp, 4 * CAP, quarter), BF16),
+        pltpu.VMEM((n_sp, 4 * CAP, quarter), BF16),
+        pltpu.VMEM((tokens, width), BF16),
+        dma((12,)),
+        dma((20,)),
+        dma((3,)),
+        dma((3,)),
+        dma((3,)),
+        dma((3,)),
+        dma((n_sp,)),
+        dma((n_sp,)),
+        dma((4,)),
+        dma((4,)),
+        dma,
+        dma,
+        dma((13,)),
+        dma((13,)),
+        pltpu.VMEM((3, pairs, units), F32),
+    ]
     return pl.pallas_call(
-        functools.partial(expert_kernel, n_sp, n_tp),
+        functools.partial(main_kernel, n_sp, n_tp),
         out_shape=(
+            jax.ShapeDtypeStruct((tokens, channels), F32),
+            jax.ShapeDtypeStruct((tokens, channels), BF16),
+            jax.ShapeDtypeStruct((n_sp, rows, entries), BF16),
+            jax.ShapeDtypeStruct((n_sp, 1, entries), F32),
             jax.ShapeDtypeStruct((tokens, width * n_tp), BF16),
             jax.ShapeDtypeStruct((2, 4, 4) + own.shape, BF16),
             jax.ShapeDtypeStruct(w_gate.shape, BF16),
             jax.ShapeDtypeStruct(w_up.shape, BF16),
             jax.ShapeDtypeStruct(w_down.shape, BF16),
         ),
-        in_specs=[vmem_spec()] + [any_spec()] * 3 + [vmem_spec()] * 2 + [any_spec()],
-        out_specs=(vmem_spec(),) + (any_spec(),) * 4,
+        in_specs=[vmem_spec()] * 6
+        + [any_spec()]
+        + [vmem_spec()] * 4
+        + [any_spec()] * 3
+        + [vmem_spec()] * 2
+        + [any_spec()],
+        out_specs=(vmem_spec(),) * 5 + (any_spec(),) * 4,
         scratch_shapes=[
-            pltpu.VMEM((model, units), BF16),
-            pltpu.VMEM((model, units), BF16),
-            pltpu.VMEM((units, model), BF16),
-            pltpu.VMEM((model, units), BF16),
-            pltpu.VMEM((model, units), BF16),
-            pltpu.VMEM((units, model), BF16),
-            pltpu.VMEM((rows, model), BF16),
-            pltpu.VMEM((model, rows), BF16),
-            pltpu.VMEM((rows, model), BF16),
-            pltpu.VMEM((rows, units), BF16),
-            pltpu.VMEM((rows, units), BF16),
-            pltpu.VMEM((rows, units), BF16),
-            pltpu.VMEM((2 * n_tp, rows, half), BF16),
-            pltpu.VMEM((3, rows, half), BF16),
-            pltpu.VMEM((3, rows, half), BF16),
-            pltpu.VMEM((rows, half), BF16),
-            pltpu.VMEM((rows, half), BF16),
-            pltpu.VMEM((n_sp, 4 * CAP, quarter), BF16),
-            pltpu.VMEM((n_sp, 4 * CAP, quarter), BF16),
-            pltpu.VMEM((tokens, width), BF16),
-            dma((12,)),
-            dma((20,)),
-            dma((3,)),
-            dma((3,)),
-            dma((3,)),
-            dma((3,)),
-            dma((n_sp,)),
-            dma((n_sp,)),
-            dma((4,)),
-            dma((4,)),
-            dma,
-            dma,
-            dma((13,)),
-            dma((13,)),
-        ],
+            pltpu.VMEM((n_sp, 4 * CAP, half), BF16),
+            pltpu.VMEM((n_tp, n_sp, 4 * CAP, half), BF16),
+        ]
+        + front_scratch
+        + expert_scratch,
         compiler_params=pltpu.CompilerParams(
-            collective_id=1, has_side_effects=True, vmem_limit_bytes=VMEM_BYTES
+            collective_id=0, has_side_effects=True, vmem_limit_bytes=VMEM_BYTES
         ),
-        name="experts",
-    )(arrived, w_gate, w_up, w_down, routes, grads, own)
+        name="main",
+    )(
+        stream, weights, x, dt, rate, extra, first, b, c, gate, scale, w_gate, w_up, w_down, routes, grads, own
+    )
 
 
 def tail_kernel(
@@ -903,6 +986,7 @@
     rate_ref,
     extra_ref,
     coming_ref,
+    decays,
     b_ref,
     c_ref,
     gate_ref,
@@ -924,22 +1008,17 @@
     reduced,
     total,
     state_mine,
-    decay_mine,
     states,
-    decays,
     carries,
     later,
     d_scaled,
     one,
-    two,
     load,
     p_send,
     p_recv,
     ring_sems,
     sends,
     recvs,
-    d_sends,
-    d_recvs,
     b_sends,
     b_recvs,
 ):
@@ -953,7 +1032,7 @@
     ]
     for fetch in fetches:
         fetch.start()
-    greet(me, tp, n_sp, n_tp)
+    met = greet(me, tp, n_sp, n_tp)
     heads, tokens = dt_ref.shape
     channels = x_ref.shape[1]
     groups = b_ref.shape[1] // STATE
@@ -971,9 +1050,6 @@
     def mine(c):
         return pl.ds(pl.multiple_of(c * half, half), half)
 
-    pair(0, normed_ref.at[:, mine(1 - core)], normed2).start()
-    pair(1, mix_ref, mix2).start()
-
     owner = head_spread(heads, HDIM)
     dt = turned(dt_ref[...])
     cum = cumulative_decay(dt, rate_ref[...], turned(extra_ref[...]))
@@ -981,51 +1057,20 @@
     last = cum[tokens - 1 : tokens, :]
     since = spread(jnp.exp(cum), owner)
 
-    mix_t = jnp.transpose(mix_ref[...])
-    pair(0, normed_ref.at[:, mine(1 - core)], normed2).wait()
-    pair(1, mix_ref, mix2).wait()
-    both_mix = jnp.concatenate([mix_t, jnp.transpose(mix2[...])], axis=1)
-    both_normed = jnp.concatenate([normed_ref[:, mine(core)], normed2[...]], axis=0)
-    piece_rows = cols // 2
-    for z in range(4):
-        at = slice(z * 8 * cols, (z + 1) * 8 * cols)
-        parts[z] = (
-            dot(both_mix[at, :], both_normed).astype(BF16).reshape(4, 2, 2, piece_rows, half)
-        )
-
-    lane_y, lane_z = lax.rem(chip, 4), lax.div(chip, 4)
-
-    def at_y(y):
-        return (lane_z * 8 + lax.rem(y, 4) * 2 + core, tp)
-
-    def at_z(z):
-        return (lax.rem(z, 4) * 8 + lane_y * 2 + core, tp)
-
-    y_ring = (lane_y, at_y(lane_y + 1), at_y(lane_y + 3))
-    z_ring = (lane_z, at_z(lane_z + 1), at_z(lane_z + 3))
-
-    def four(ref, k):
-        return [ref.at[k, i] for i in range(4)]
-
-    def bufs(landing, sums, k):
-        return [landing.at[k, 0], landing.at[k, 1], sums.at[k, 0], sums.at[k, 1]]
-
-    stages = [
-        ring_reduce(lambda b, w: parts.at[:, b, 0, w], *y_ring, *bufs(big_in, big_sum, 0), four(ring_sems, 0)),
-        ring_reduce(lambda b, w: parts.at[b, :, 1, w], *z_ring, *bufs(big_in, big_sum, 1), four(ring_sems, 1)),
-        ring_reduce(lambda b, w: reduced.at[0, w, b], *z_ring, *bufs(small_in, small_sum, 0), four(ring_sems, 2)),
-        ring_reduce(lambda b, w: reduced.at[1, w, b], *y_ring, *bufs(small_in, small_sum, 1), four(ring_sems, 3)),
-    ]
-    stages[0][0]()
-    stages[1][0]()
-
     for fetch in fetches:
         fetch.wait()
     whole_weight = weight[...].reshape(mix_ref.shape[1], channels)
+    normed_grads = [
+        dot(mix_ref[...], whole_weight[:, g * wide : (g + 1) * wide]) for g in range(groups)
+    ]
+    mix_t = jnp.transpose(mix_ref[...])
+    met()
+    pair(0, normed_ref.at[:, mine(1 - core)], normed2).start()
+    pair(1, mix_ref, mix2).start()
     d_y = []
     for g in range(groups):
         at = slice(g * wide, (g + 1) * wide)
-        normed_grad = dot(mix_ref[...], whole_weight[:, at])
+        normed_grad = normed_grads[g]
         y = y_ref[:, at]
         gate = gate_ref[:, at].astype(F32)
         sigmoid_gate = jax.nn.sigmoid(gate)
@@ -1052,9 +1097,6 @@
             per_group, rows, entries
         )
     whole = jnp.exp(last)
-    for p in range(n_parts):
-        h = p * rows // HDIM
-        decay_mine[p] = jnp.broadcast_to(whole[:, h : h + 1], (1, entries))
 
     def state_copy(d):
         to = lax.rem(me + d, n_sp)
@@ -1062,12 +1104,6 @@
             state_mine.at[to], states.at[me], sends.at[d], recvs.at[d], (to, tp), MESH
         )
 
-    def decay_copy(d):
-        to = lax.rem(me + d, n_sp)
-        return pltpu.make_async_remote_copy(
-            decay_mine.at[to], decays.at[me], d_sends.at[d], d_recvs.at[d], (to, tp), MESH
-        )
-
     def back_copy(d):
         to = lax.rem(me + d, n_sp)
         return pltpu.make_async_remote_copy(
@@ -1075,15 +1111,50 @@
         )
 
     def start_states(d, carry):
-        decay_copy(hop(d, n_sp)).start()
         state_copy(hop(d, n_sp)).start()
         return carry
 
     lax.fori_loop(1, n_sp, start_states, 0)
     kept = pltpu.make_async_copy(state_mine.at[me], states.at[me], one)
-    kept_too = pltpu.make_async_copy(decay_mine.at[me], decays.at[me], two)
     kept.start()
-    kept_too.start()
+
+    pair(0, normed_ref.at[:, mine(1 - core)], normed2).wait()
+    pair(1, mix_ref, mix2).wait()
+    both_mix = jnp.concatenate([mix_t, jnp.transpose(mix2[...])], axis=1)
+    both_normed = jnp.concatenate([normed_ref[:, mine(core)], normed2[...]], axis=0)
+    piece_rows = cols // 2
+    for z in range(4):
+        at = slice(z * 8 * cols, (z + 1) * 8 * cols)
+        parts[z] = (
+            dot(both_mix[at, :], both_normed).astype(BF16).reshape(4, 2, 2, piece_rows, half)
+        )
+
+    lane_y, lane_z = lax.rem(chip, 4), lax.div(chip, 4)
+
+    def at_y(y):
+        return (lane_z * 8 + lax.rem(y, 4) * 2 + core, tp)
+
+    def at_z(z):
+        return (lax.rem(z, 4) * 8 + lane_y * 2 + core, tp)
+
+    y_ring = (lane_y, at_y(lane_y + 1), at_y(lane_y + 3))
+    z_ring = (lane_z, at_z(lane_z + 1), at_z(lane_z + 3))
+
+    def four(ref, k):
+        return [ref.at[k, i] for i in range(4)]
+
+    def bufs(landing, sums, k):
+        return [landing.at[k, 0], landing.at[k, 1], sums.at[k, 0], sums.at[k, 1]]
+
+    stages = [
+        ring_reduce(lambda b, w: parts.at[:, b, 0, w], *y_ring, *bufs(big_in, big_sum, 0), four(ring_sems, 0)),
+        ring_reduce(lambda b, w: parts.at[b, :, 1, w], *z_ring, *bufs(big_in, big_sum, 1), four(ring_sems, 1)),
+        ring_reduce(lambda b, w: reduced.at[0, w, b], *z_ring, *bufs(small_in, small_sum, 0), four(ring_sems, 2)),
+        ring_reduce(lambda b, w: reduced.at[1, w, b], *y_ring, *bufs(small_in, small_sum, 1), four(ring_sems, 3)),
+    ]
+    stages[0][0]()
+    stages[1][0]()
+
 
     values = x_ref[...].astype(F32)
     steps = spread(dt, owner)
@@ -1125,13 +1196,9 @@
         d_affinity.append(sum_affinity.astype(BF16))
 
     inside(0)
-    stages[0][1]()
-    stages[1][1]()
     kept.wait()
-    kept_too.wait()
 
     def finish_states(d, carry):
-        decay_copy(d).wait()
         state_copy(d).wait()
         return carry
 
@@ -1152,12 +1219,8 @@
 
     for g in range(1, groups):
         inside(g)
-    for k in range(2):
-        stages[k][2]()
-        for w in range(2):
-            reduced[k, w] = stages[k][3](w).astype(BF16)
-    stages[2][0]()
-    stages[3][0]()
+    stages[0][1]()
+    stages[1][1]()
     read_out = []
     for g in range(groups):
         at = slice(g * wide, (g + 1) * wide)
@@ -1167,10 +1230,13 @@
         dc_ref[:, by] = (
             dot(d_affinity[g], b_ref[:, by]) + dot(since_low[:, at], incoming)
         ).astype(BF16)
+    for k in range(2):
+        stages[k][2]()
+        for w in range(2):
+            reduced[k, w] = stages[k][3](w).astype(BF16)
+    stages[2][0]()
+    stages[3][0]()
     reading = by_head(since_grad * jnp.concatenate(read_out, axis=1), owner)
-
-    stages[2][1]()
-    stages[3][1]()
 
     kept_back.wait()
 
@@ -1191,6 +1257,8 @@
         db_ref[:, by] = (
             dot(d_affinity[g], c_ref[:, by], ((0,), (0,))) + dot(ending_low[:, at], after)
         ).astype(BF16)
+    stages[2][1]()
+    stages[3][1]()
     closing = jnp.concatenate(from_later, axis=1)
     gradient = d_scaled[...] + until * closing
     dx_ref[...] = (gradient * steps).astype(BF16)
@@ -1231,7 +1299,9 @@
     pair(2, total.at[lines(core), :], proj_ref.at[:, mine(1 - core)]).wait_recv()
 
 
-def tail(mix, weight, y, normed, x, dt, rate, extra, coming, b, c, gate, scale, n_sp, n_tp):
+def tail(
+    mix, weight, y, normed, x, dt, rate, extra, coming, decays, b, c, gate, scale, n_sp, n_tp
+):
     dma = pltpu.SemaphoreType.DMA
     tokens, channels = x.shape
     heads = dt.shape[0]
@@ -1250,7 +1320,7 @@
             jax.ShapeDtypeStruct(c.shape, BF16),
             jax.ShapeDtypeStruct((tokens, channels), BF16),
         ),
-        in_specs=[vmem_spec(), any_spec()] + [vmem_spec()] * 11,
+        in_specs=[vmem_spec(), any_spec()] + [vmem_spec()] * 12,
         out_specs=(vmem_spec(),) * 6,
         scratch_shapes=[
             pltpu.VMEM((chips, 2, cols, channels), BF16),
@@ -1264,25 +1334,22 @@
             pltpu.VMEM((2, 2, 4, cols // 2, half), BF16),
             pltpu.VMEM((2 * cols, half), F32),
             pltpu.VMEM((n_sp, rows, entries), BF16),
-            pltpu.VMEM((n_sp, 1, entries), F32),
             pltpu.VMEM((n_sp, rows, entries), BF16),
-            pltpu.VMEM((n_sp, 1, entries), F32),
             pltpu.VMEM((n_sp, rows, entries), BF16),
             pltpu.VMEM((n_sp, rows, entries), BF16),
             pltpu.VMEM((tokens, channels), F32),
-            dma,
             dma,
             dma((2,)),
             dma((3,)),
             dma((3,)),
             dma((4, 4, 3)),
         ]
-        + [dma((n_sp,))] * 6,
+        + [dma((n_sp,))] * 4,
         compiler_params=pltpu.CompilerParams(
             collective_id=2, has_side_effects=True, vmem_limit_bytes=VMEM_BYTES
         ),
         name="tail",
-    )(mix, weight, y, normed, x, dt, rate, extra, coming, b, c, gate, scale)
+    )(mix, weight, y, normed, x, dt, rate, extra, coming, decays, b, c, gate, scale)
 
 
 def finish_kernel(count, *refs):
@@ -1350,14 +1417,14 @@
     group_norm_scale,
     mixer_output_weight,
 ):
-    packed = pack(routes, expert_combine_weight, mixer_output_stream, layer_output_gradient, n_sp)
     heads = head_step_size.shape[1]
     part_rows = heads * HDIM // n_sp
     entering = state_entering_span.reshape(n_sp, part_rows, STATE)
     rate = head_decay_rate[None, :]
     scale = group_norm_scale[None, :]
-    arrived, scan_out, normed_low, coming = front(
-        packed,
+    scan_out, normed_low, coming, decays, mix_grad, weight, grad_g, grad_u, grad_d = main(
+        mixer_output_stream,
+        expert_combine_weight.T,
         head_mixer_input,
         head_step_size.T,
         rate,
@@ -1367,11 +1434,6 @@
         state_readout_vectors,
         gate_preactivation,
         scale,
-        n_sp,
-        n_tp,
-    )
-    mix_grad, weight, grad_g, grad_u, grad_d = experts_backward(
-        arrived,
         expert_gate_weight,
         expert_up_weight,
         expert_down_weight,
@@ -1392,6 +1454,7 @@
         rate,
         extra_log_decay.T,
         coming,
+        decays,
         state_input_vectors,
         state_readout_vectors,
         gate_preactivation,

time: 147 us -> 131 us (0.89)
  Pallas kernels: 145 us -> 129 us
    pallas_call x3 -> x1, Pallas kernels: 101 us -> 85.6 us  [main(): pl.pallas_call(functools.partial(main_kernel, n_sp, n_tp), out_shape=(jax...]
where the time goes in v4:
time: 131 us; the launch traced here: 129 us
  Pallas kernels  129 us (98%)
    pallas_call x1, Pallas kernels, main(): pl.pallas_call(functools.partial(main_kernel, n_sp, n_tp), out_shape=(jax...  85.6 us
    pallas_call x1, Pallas kernels, tail(): pl.pallas_call(functools.partial(tail_kernel, n_sp, n_tp), out_shape=(jax...  33.8 us
    pallas_call x1, Pallas kernels, finish(): pl.pallas_call(functools.partial(finish_kernel, count), out_shape=tuple((...  9.21 us

profile of v4, /device:TPU:0, one launch (start us, length us, event | category | flops | bytes accessed | tf_op | source)
XLA Modules:
  0.0 129.4 jit_solution(11621609553196838449)
XLA Ops:
  0.6 85.6 %main.1 = (f32[128,1024]{1,0:T(8,128)}, bf16[128,1024]{1,0:T(8,128)(2,1)}, bf16[32,32,128]{2,1,0:T(8,128)(2,1)}, f32[32,1,128]{2,1,0:T(1,128)}, bf16[128,2048]{1...) custom-call(bf16[128,512]{1,0:T(8,128)(2,1)} %refs_0_.1, ...), custom_call_target="tpu_custom_call" | custom-call | tf_op jit(solution)/shard_map/main/pallas_call | solution.py:942
  86.3 33.8 %tail.1 = (f32[64,1024]{1,0:T(8,128)}, bf16[128,1024]{1,0:T(8,128)(2,1)}, f32[16,128]{1,0:T(8,128)}, bf16[128,256]{1,0:T(8,128)(2,1)}, bf16[128,256]{1,0:T(8,128)(2,1)}, /*index=5*/bf16[128,1024]{1,0:T(8,128)(2,1)}) custom-call(bf16[128,2048]{1,0:T(8,128)(2,1)} %get-tuple-element.33.mix_ref, bf16[2,16,64,1024]{3,2,1,0:T(8,128)(2,1)} %bitcast.13, ...), custom_call_target="tpu_custom_call" | custom-call | tf_op jit(solution)/shard_map/tail/pallas_call | solution.py:1313
  120.1 9.2 %finish.1 = (f32[64,1024]{1,0:T(8,128)}, bf16[128,1024]{1,0:T(8,128)(2,1)}, f32[16,128]{1,0:T(8,128)}, bf16[128,256]{1,0:T(8,128)(2,1)}, bf16[128,256]{1,0:T(8,1...) custom-call(f32[64,1024]{1,0:T(8,128)} %get-tuple-element.39.refs_0_, ...), custom_call_target="tpu_custom_call" | custom-call | tf_op jit(solution)/shard_map/finish/pallas_call | solution.py:1387

commit v5 on v4

--- a/solution.py
+++ b/solution.py
@@ -16,7 +16,7 @@
 BF16 = jnp.bfloat16
 
 norm_eps = 1e-05
-VMEM_BYTES = 60 * 1024 * 1024
+VMEM_BYTES = 67043328 - 1024 * 1024
 
 
 def vmem_spec():
@@ -482,7 +482,7 @@
     grads_ref,
     own_hbm,
     mix_ref,
-    all_hbm,
+    all_ref,
     dgate_hbm,
     dup_hbm,
     ddown_hbm,
@@ -558,30 +558,30 @@
             src, dst, w_sends.at[k], w_recvs.at[k], (to, tp), MESH
         )
 
-    own_weight = pltpu.make_async_copy(own_hbm, all_hbm.at[core, lane_z, lane_y], w_own)
+    own_weight = pltpu.make_async_copy(own_hbm, all_ref.at[lane_z, lane_y, core], w_own)
     own_weight.start()
 
     def first_stage(j, sending):
         y, z = (lane_y, lane_z) if sending else (lax.rem(lane_y + 4 - j, 4), lax.rem(lane_z + 4 - j, 4))
         return [
             weight_copy(
-                j - 1, own_hbm.at[0], all_hbm.at[core, lane_z, y, 0], at_y(lax.rem(lane_y + j, 4))
+                j - 1, own_hbm.at[0], all_ref.at[lane_z, y, core, 0], at_y(lax.rem(lane_y + j, 4))
             ),
             weight_copy(
-                j + 2, own_hbm.at[1], all_hbm.at[core, z, lane_y, 1], at_z(lax.rem(lane_z + j, 4))
+                j + 2, own_hbm.at[1], all_ref.at[z, lane_y, core, 1], at_z(lax.rem(lane_z + j, 4))
             ),
         ]
 
     def second_stage(j, sending):
         y, z = (lane_y, lane_z) if sending else (lax.rem(lane_y + 4 - j, 4), lax.rem(lane_z + 4 - j, 4))
-        by_z, by_y = all_hbm.at[core, z, :, 0], all_hbm.at[core, :, y, 1]
+        by_z, by_y = all_ref.at[z, :, core, 0], all_ref.at[:, y, core, 1]
         return [
             weight_copy(j + 5, by_z, by_z, at_z(lax.rem(lane_z + j, 4))),
             weight_copy(j + 8, by_y, by_y, at_y(lax.rem(lane_y + j, 4))),
         ]
 
     def third_stage(c):
-        return weight_copy(12, all_hbm.at[c], all_hbm.at[c], me + 1 - 2 * core)
+        return weight_copy(12, all_ref.at[:, :, c], all_ref.at[:, :, c], me + 1 - 2 * core)
 
     for j in range(1, 4):
         for copy in first_stage(j, True):
@@ -824,17 +824,333 @@
     third_stage(1 - core).wait_recv()
 
 
+def tail_part(
+    n_sp,
+    n_tp,
+    mix_ref,
+    weight,
+    y_ref,
+    normed_ref,
+    x_ref,
+    dt_ref,
+    rate_ref,
+    extra_ref,
+    coming_ref,
+    decays,
+    b_ref,
+    c_ref,
+    gate_ref,
+    scale_ref,
+    proj_ref,
+    dx_ref,
+    ddt_ref,
+    db_ref,
+    dc_ref,
+    dgate_ref,
+    normed2,
+    mix2,
+    parts,
+    big_in,
+    big_sum,
+    small_in,
+    small_sum,
+    reduced,
+    total,
+    state_mine,
+    states,
+    carries,
+    later,
+    d_scaled,
+    one,
+    p_send,
+    p_recv,
+    ring_sems,
+    sends,
+    recvs,
+    b_sends,
+    b_recvs,
+):
+    me, tp = lax.axis_index("sp"), lax.axis_index("tp")
+    core = lax.rem(me, 2)
+    partner = me + 1 - 2 * core
+    chip = lax.div(me, 2)
+    chips = n_sp // 2
+    heads, tokens = dt_ref.shape
+    channels = x_ref.shape[1]
+    groups = b_ref.shape[1] // STATE
+    wide = channels // groups
+    half = channels // 2
+    cols = proj_ref.shape[0]
+    n_parts, rows, entries = state_mine.shape
+    per_group = n_parts // groups
+
+    def pair(k, src, dst):
+        return pltpu.make_async_remote_copy(
+            src, dst, p_send.at[k], p_recv.at[k], (partner, tp), MESH
+        )
+
+    def mine(c):
+        return pl.ds(pl.multiple_of(c * half, half), half)
+
+    owner = head_spread(heads, HDIM)
+    dt = turned(dt_ref[...])
+    cum = cumulative_decay(dt, rate_ref[...], turned(extra_ref[...]))
+    cum_rows = turned(cum)
+    last = cum[tokens - 1 : tokens, :]
+    since = spread(jnp.exp(cum), owner)
+
+    whole_weight = weight[...].reshape(mix_ref.shape[1], channels)
+    normed_grads = [
+        dot(mix_ref[...], whole_weight[:, g * wide : (g + 1) * wide]) for g in range(groups)
+    ]
+    mix_t = jnp.transpose(mix_ref[...])
+    pair(0, normed_ref.at[:, mine(1 - core)], normed2).start()
+    pair(1, mix_ref, mix2).start()
+    d_y = []
+    for g in range(groups):
+        at = slice(g * wide, (g + 1) * wide)
+        normed_grad = normed_grads[g]
+        y = y_ref[:, at]
+        gate = gate_ref[:, at].astype(F32)
+        sigmoid_gate = jax.nn.sigmoid(gate)
+        activated = gate * sigmoid_gate
+        gated = y * activated
+        factor = lax.rsqrt(jnp.mean(gated * gated, axis=1, keepdims=True) + norm_eps)
+        scaled_grad = normed_grad * scale_ref[:, at]
+        along = jnp.mean(scaled_grad * gated, axis=1, keepdims=True) * factor * factor
+        gated_grad = factor * (scaled_grad - gated * along)
+        d_y.append(gated_grad * activated)
+        dgate_ref[:, at] = (
+            gated_grad * y * (sigmoid_gate * (1.0 + gate * (1.0 - sigmoid_gate)))
+        ).astype(BF16)
+    d_out = jnp.concatenate(d_y, axis=1)
+    since_grad = since * d_out
+    since_low = since_grad.astype(BF16)
+    for g in range(groups):
+        state = dot(
+            since_low[:, g * wide : (g + 1) * wide],
+            c_ref[:, g * STATE : (g + 1) * STATE],
+            ((0,), (0,)),
+        )
+        state_mine[g * per_group : (g + 1) * per_group] = state.astype(BF16).reshape(
+            per_group, rows, entries
+        )
+    whole = jnp.exp(last)
+
+    def state_copy(d):
+        to = lax.rem(me + d, n_sp)
+        return pltpu.make_async_remote_copy(
+            state_mine.at[to], states.at[me], sends.at[d], recvs.at[d], (to, tp), MESH
+        )
+
+    def back_copy(d):
+        to = lax.rem(me + d, n_sp)
+        return pltpu.make_async_remote_copy(
+            carries.at[to], later.at[me], b_sends.at[d], b_recvs.at[d], (to, tp), MESH
+        )
+
+    def start_states(d, carry):
+        state_copy(hop(d, n_sp)).start()
+        return carry
+
+    lax.fori_loop(1, n_sp, start_states, 0)
+    kept = pltpu.make_async_copy(state_mine.at[me], states.at[me], one)
+    kept.start()
+
+    pair(0, normed_ref.at[:, mine(1 - core)], normed2).wait()
+    pair(1, mix_ref, mix2).wait()
+    both_mix = jnp.concatenate([mix_t, jnp.transpose(mix2[...])], axis=1)
+    both_normed = jnp.concatenate([normed_ref[:, mine(core)], normed2[...]], axis=0)
+    piece_rows = cols // 2
+    for z in range(4):
+        at = slice(z * 8 * cols, (z + 1) * 8 * cols)
+        parts[z] = (
+            dot(both_mix[at, :], both_normed).astype(BF16).reshape(4, 2, 2, piece_rows, half)
+        )
+
+    lane_y, lane_z = lax.rem(chip, 4), lax.div(chip, 4)
+
+    def at_y(y):
+        return (lane_z * 8 + lax.rem(y, 4) * 2 + core, tp)
+
+    def at_z(z):
+        return (lax.rem(z, 4) * 8 + lane_y * 2 + core, tp)
+
+    y_ring = (lane_y, at_y(lane_y + 1), at_y(lane_y + 3))
+    z_ring = (lane_z, at_z(lane_z + 1), at_z(lane_z + 3))
+
+    def four(ref, k):
+        return [ref.at[k, i] for i in range(4)]
+
+    def bufs(landing, sums, k):
+        return [landing.at[k, 0], landing.at[k, 1], sums.at[k, 0], sums.at[k, 1]]
+
+    stages = [
+        ring_reduce(lambda b, w: parts.at[:, b, 0, w], *y_ring, *bufs(big_in, big_sum, 0), four(ring_sems, 0)),
+        ring_reduce(lambda b, w: parts.at[b, :, 1, w], *z_ring, *bufs(big_in, big_sum, 1), four(ring_sems, 1)),
+        ring_reduce(lambda b, w: reduced.at[0, w, b], *z_ring, *bufs(small_in, small_sum, 0), four(ring_sems, 2)),
+        ring_reduce(lambda b, w: reduced.at[1, w, b], *y_ring, *bufs(small_in, small_sum, 1), four(ring_sems, 3)),
+    ]
+    stages[0][0]()
+    stages[1][0]()
+
+
+    values = x_ref[...].astype(F32)
+    steps = spread(dt, owner)
+    scaled = values * steps
+    scaled_low = scaled.astype(BF16)
+    d_low = d_out.astype(BF16)
+    not_before = triangle(tokens, lambda t, s: s >= t)
+    below = (iota((tokens, tokens), 1) < iota((tokens, tokens), 0)).astype(F32)
+    head_lane = iota((1, heads), 1)
+    crossing = [jnp.zeros((tokens, heads), F32)]
+    d_affinity = []
+
+    def inside(g):
+        affinity = dot(
+            c_ref[:, g * STATE : (g + 1) * STATE],
+            b_ref[:, g * STATE : (g + 1) * STATE],
+            ((1,), (1,)),
+        )
+        sum_affinity = jnp.zeros((tokens, tokens), F32)
+        first = g * (heads // 2 // groups)
+        for q in range(first, first + heads // 2 // groups):
+            at = slice(q * 2 * HDIM, (q + 1) * 2 * HDIM)
+            d_halves = halves(d_low[:, at])
+            d_weights = dot(d_halves, scaled_low[:, at], ((1,), (1,)))
+            weights, moved = [], []
+            for j in range(2):
+                between = decay_between(cum, cum_rows, 2 * q + j)
+                weights.append((affinity * between).astype(BF16))
+                d_between = d_weights[j * tokens : (j + 1) * tokens] * between
+                sum_affinity = sum_affinity + d_between
+                moved.append((d_between * affinity).astype(BF16))
+            d_scaled[:, at] = dot(jnp.concatenate(weights, axis=0), d_halves, ((0,), (0,)))
+            reach = dot(not_before, jnp.concatenate(moved, axis=1))
+            for j in range(2):
+                over = jnp.sum(
+                    reach[:, j * tokens : (j + 1) * tokens] * below, axis=1, keepdims=True
+                )
+                crossing[0] = crossing[0] + jnp.where(head_lane == 2 * q + j, over, 0.0)
+        d_affinity.append(sum_affinity.astype(BF16))
+
+    inside(0)
+    kept.wait()
+
+    def finish_states(d, carry):
+        state_copy(d).wait()
+        return carry
+
+    lax.fori_loop(1, n_sp, finish_states, 0)
+    running = jnp.zeros((rows, entries), F32)
+    for step in range(n_sp):
+        i = n_sp - 1 - step
+        carries[i] = running.astype(BF16)
+        running = decays[i] * running + states[i].astype(F32)
+
+    def start_back(d, carry):
+        back_copy(hop(d, n_sp)).start()
+        return carry
+
+    lax.fori_loop(1, n_sp, start_back, 0)
+    kept_back = pltpu.make_async_copy(carries.at[me], later.at[me], one)
+    kept_back.start()
+
+    for g in range(1, groups):
+        inside(g)
+    stages[0][1]()
+    stages[1][1]()
+    read_out = []
+    for g in range(groups):
+        at = slice(g * wide, (g + 1) * wide)
+        by = slice(g * STATE, (g + 1) * STATE)
+        incoming = coming_ref[g * per_group : (g + 1) * per_group].reshape(wide, entries)
+        read_out.append(dot(c_ref[:, by], incoming, ((1,), (1,))))
+        dc_ref[:, by] = (
+            dot(d_affinity[g], b_ref[:, by]) + dot(since_low[:, at], incoming)
+        ).astype(BF16)
+    for k in range(2):
+        stages[k][2]()
+        for w in range(2):
+            reduced[k, w] = stages[k][3](w).astype(BF16)
+    stages[2][0]()
+    stages[3][0]()
+    reading = by_head(since_grad * jnp.concatenate(read_out, axis=1), owner)
+
+    kept_back.wait()
+
+    def finish_back(d, carry):
+        back_copy(d).wait()
+        return carry
+
+    lax.fori_loop(1, n_sp, finish_back, 0)
+    until = spread(jnp.exp(last - cum), owner)
+    ending = scaled * until
+    ending_low = ending.astype(BF16)
+    from_later = []
+    for g in range(groups):
+        at = slice(g * wide, (g + 1) * wide)
+        by = slice(g * STATE, (g + 1) * STATE)
+        after = later[g * per_group : (g + 1) * per_group].reshape(wide, entries)
+        from_later.append(dot(b_ref[:, by], after, ((1,), (1,))))
+        db_ref[:, by] = (
+            dot(d_affinity[g], c_ref[:, by], ((0,), (0,))) + dot(ending_low[:, at], after)
+        ).astype(BF16)
+    stages[2][1]()
+    stages[3][1]()
+    closing = jnp.concatenate(from_later, axis=1)
+    gradient = d_scaled[...] + until * closing
+    dx_ref[...] = (gradient * steps).astype(BF16)
+    direct = by_head(gradient * values, owner)
+    stored = by_head(ending * closing, owner)
+    kept_state = jnp.sum(
+        (
+            coming_ref[...].astype(F32).reshape(heads, HDIM, entries)
+            * later[...].astype(F32).reshape(heads, HDIM, entries)
+        ),
+        axis=1,
+    )
+    passing = dot_split(
+        kept_state, jnp.ones((8, entries), BF16), 3, ((1,), (1,)), left=False
+    )[0:1, :]
+    earlier = triangle(tokens, lambda t, s: s < t)
+    d_decay = (
+        crossing[0]
+        + dot_split(reading, not_before, 3, ((1,), (0,)), left=False)
+        + dot_split(stored, earlier, 3, ((1,), (0,)), left=False)
+        + passing * whole
+    )
+    ddt_ref[...] = turned(direct - d_decay * rate_ref[...])
+
+    for k in range(2):
+        stages[2 + k][2]()
+        for w in range(2):
+            first = (2 * k + w) * piece_rows
+            total[first : first + piece_rows, :] = stages[2 + k][3](w)
+
+    def lines(c):
+        return pl.ds(pl.multiple_of(c * cols, cols), cols)
+
+    given = pair(2, total.at[lines(1 - core), :], proj_ref.at[:, mine(core)])
+    given.start()
+    proj_ref[:, mine(core)] = total[lines(core), :]
+    given.wait_send()
+    pair(2, total.at[lines(core), :], proj_ref.at[:, mine(1 - core)]).wait_recv()
+
+
 FRONT_SCRATCH = 24
+EXPERT_SCRATCH = 35
 
 
 def main_kernel(n_sp, n_tp, *refs):
     (stream, weights, x, dt, rate, extra, first, b, c, gate, scale) = refs[:11]
     (w_gate, w_up, w_down, routes, grads, own) = refs[11:17]
-    (y, normed, coming, decays) = refs[17:21]
-    expert_outs = refs[21:26]
-    packed, arrived = refs[26:28]
-    front_scratch = refs[28 : 28 + FRONT_SCRATCH]
-    expert_scratch = refs[28 + FRONT_SCRATCH :]
+    tail_outs = refs[17:23]
+    weight_grads = refs[23:26]
+    (packed, arrived, y, normed, coming, decays, mix, all_weight) = refs[26:34]
+    front_scratch = refs[34 : 34 + FRONT_SCRATCH]
+    expert_scratch = refs[34 + FRONT_SCRATCH : 34 + FRONT_SCRATCH + EXPERT_SCRATCH]
+    tail_scratch = refs[34 + FRONT_SCRATCH + EXPERT_SCRATCH :]
     steps = expert_part(
         n_sp,
         n_tp,
@@ -845,7 +1161,9 @@
         routes,
         grads,
         own,
-        *expert_outs,
+        mix,
+        all_weight,
+        *weight_grads,
         *expert_scratch,
     )
     front_part(
@@ -873,6 +1191,26 @@
     )
     for _ in steps:
         pass
+    tail_part(
+        n_sp,
+        n_tp,
+        mix,
+        all_weight,
+        y,
+        normed,
+        x,
+        dt,
+        rate,
+        extra,
+        coming,
+        decays,
+        b,
+        c,
+        gate,
+        scale,
+        *tail_outs,
+        *tail_scratch,
+    )
 
 
 def main(
@@ -939,15 +1277,39 @@
         dma((13,)),
         pltpu.VMEM((3, pairs, units), F32),
     ]
+    cols = own.shape[0] * own.shape[1]
+    tail_scratch = (
+        [
+            pltpu.VMEM((tokens, channels // 2), BF16),
+            pltpu.VMEM((tokens, width * n_tp), BF16),
+            pltpu.VMEM((4, 4, 2, 2, cols // 2, channels // 2), BF16),
+            pltpu.VMEM((2, 2, 3, 4, cols // 2, channels // 2), BF16),
+            pltpu.VMEM((2, 2, 4, cols // 2, channels // 2), BF16),
+            pltpu.VMEM((2, 2, 3, cols // 2, channels // 2), BF16),
+            pltpu.VMEM((2, 2, cols // 2, channels // 2), BF16),
+            pltpu.VMEM((2, 2, 4, cols // 2, channels // 2), BF16),
+            pltpu.VMEM((2 * cols, channels // 2), F32),
+            pltpu.VMEM((n_sp, rows, entries), BF16),
+            pltpu.VMEM((n_sp, rows, entries), BF16),
+            pltpu.VMEM((n_sp, rows, entries), BF16),
+            pltpu.VMEM((n_sp, rows, entries), BF16),
+            pltpu.VMEM((tokens, channels), F32),
+            dma,
+            dma((3,)),
+            dma((3,)),
+            dma((4, 4, 3)),
+        ]
+        + [dma((n_sp,))] * 4
+    )
     return pl.pallas_call(
         functools.partial(main_kernel, n_sp, n_tp),
         out_shape=(
-            jax.ShapeDtypeStruct((tokens, channels), F32),
+            jax.ShapeDtypeStruct((own.shape[0] * own.shape[1], channels), F32),
             jax.ShapeDtypeStruct((tokens, channels), BF16),
-            jax.ShapeDtypeStruct((n_sp, rows, entries), BF16),
-            jax.ShapeDtypeStruct((n_sp, 1, entries), F32),
-            jax.ShapeDtypeStruct((tokens, width * n_tp), BF16),
-            jax.ShapeDtypeStruct((2, 4, 4) + own.shape, BF16),
+            jax.ShapeDtypeStruct(dt.shape, F32),
+            jax.ShapeDtypeStruct(b.shape, BF16),
+            jax.ShapeDtypeStruct(c.shape, BF16),
+            jax.ShapeDtypeStruct((tokens, channels), BF16),
             jax.ShapeDtypeStruct(w_gate.shape, BF16),
             jax.ShapeDtypeStruct(w_up.shape, BF16),
             jax.ShapeDtypeStruct(w_down.shape, BF16),
@@ -958,13 +1320,20 @@
         + [any_spec()] * 3
         + [vmem_spec()] * 2
         + [any_spec()],
-        out_specs=(vmem_spec(),) * 5 + (any_spec(),) * 4,
+        out_specs=(vmem_spec(),) * 6 + (any_spec(),) * 3,
         scratch_shapes=[
             pltpu.VMEM((n_sp, 4 * CAP, half), BF16),
             pltpu.VMEM((n_tp, n_sp, 4 * CAP, half), BF16),
+            pltpu.VMEM((tokens, channels), F32),
+            pltpu.VMEM((tokens, channels), BF16),
+            pltpu.VMEM((n_sp, rows, entries), BF16),
+            pltpu.VMEM((n_sp, 1, entries), F32),
+            pltpu.VMEM((tokens, width * n_tp), BF16),
+            pltpu.VMEM((4, 4, 2) + own.shape, BF16),
         ]
         + front_scratch
-        + expert_scratch,
+        + expert_scratch
+        + tail_scratch,
         compiler_params=pltpu.CompilerParams(
             collective_id=0, has_side_effects=True, vmem_limit_bytes=VMEM_BYTES
         ),
@@ -972,384 +1341,6 @@
     )(
         stream, weights, x, dt, rate, extra, first, b, c, gate, scale, w_gate, w_up, w_down, routes, grads, own
     )
-
-
-def tail_kernel(
-    n_sp,
-    n_tp,
-    mix_ref,
-    weight_hbm,
-    y_ref,
-    normed_ref,
-    x_ref,
-    dt_ref,
-    rate_ref,
-    extra_ref,
-    coming_ref,
-    decays,
-    b_ref,
-    c_ref,
-    gate_ref,
-    scale_ref,
-    proj_ref,
-    dx_ref,
-    ddt_ref,
-    db_ref,
-    dc_ref,
-    dgate_ref,
-    weight,
-    normed2,
-    mix2,
-    parts,
-    big_in,
-    big_sum,
-    small_in,
-    small_sum,
-    reduced,
-    total,
-    state_mine,
-    states,
-    carries,
-    later,
-    d_scaled,
-    one,
-    load,
-    p_send,
-    p_recv,
-    ring_sems,
-    sends,
-    recvs,
-    b_sends,
-    b_recvs,
-):
-    me, tp = lax.axis_index("sp"), lax.axis_index("tp")
-    core = lax.rem(me, 2)
-    partner = me + 1 - 2 * core
-    chip = lax.div(me, 2)
-    chips = n_sp // 2
-    fetches = [
-        pltpu.make_async_copy(weight_hbm.at[c], weight.at[:, c], load.at[c]) for c in range(2)
-    ]
-    for fetch in fetches:
-        fetch.start()
-    met = greet(me, tp, n_sp, n_tp)
-    heads, tokens = dt_ref.shape
-    channels = x_ref.shape[1]
-    groups = b_ref.shape[1] // STATE
-    wide = channels // groups
-    half = channels // 2
-    cols = proj_ref.shape[0]
-    n_parts, rows, entries = state_mine.shape
-    per_group = n_parts // groups
-
-    def pair(k, src, dst):
-        return pltpu.make_async_remote_copy(
-            src, dst, p_send.at[k], p_recv.at[k], (partner, tp), MESH
-        )
-
-    def mine(c):
-        return pl.ds(pl.multiple_of(c * half, half), half)
-
-    owner = head_spread(heads, HDIM)
-    dt = turned(dt_ref[...])
-    cum = cumulative_decay(dt, rate_ref[...], turned(extra_ref[...]))
-    cum_rows = turned(cum)
-    last = cum[tokens - 1 : tokens, :]
-    since = spread(jnp.exp(cum), owner)
-
-    for fetch in fetches:
-        fetch.wait()
-    whole_weight = weight[...].reshape(mix_ref.shape[1], channels)
-    normed_grads = [
-        dot(mix_ref[...], whole_weight[:, g * wide : (g + 1) * wide]) for g in range(groups)
-    ]
-    mix_t = jnp.transpose(mix_ref[...])
-    met()
-    pair(0, normed_ref.at[:, mine(1 - core)], normed2).start()
-    pair(1, mix_ref, mix2).start()
-    d_y = []
-    for g in range(groups):
-        at = slice(g * wide, (g + 1) * wide)
-        normed_grad = normed_grads[g]
-        y = y_ref[:, at]
-        gate = gate_ref[:, at].astype(F32)
-        sigmoid_gate = jax.nn.sigmoid(gate)
-        activated = gate * sigmoid_gate
-        gated = y * activated
-        factor = lax.rsqrt(jnp.mean(gated * gated, axis=1, keepdims=True) + norm_eps)
-        scaled_grad = normed_grad * scale_ref[:, at]
-        along = jnp.mean(scaled_grad * gated, axis=1, keepdims=True) * factor * factor
-        gated_grad = factor * (scaled_grad - gated * along)
-        d_y.append(gated_grad * activated)
-        dgate_ref[:, at] = (
-            gated_grad * y * (sigmoid_gate * (1.0 + gate * (1.0 - sigmoid_gate)))
-        ).astype(BF16)
-    d_out = jnp.concatenate(d_y, axis=1)
-    since_grad = since * d_out
-    since_low = since_grad.astype(BF16)
-    for g in range(groups):
-        state = dot(
-            since_low[:, g * wide : (g + 1) * wide],
-            c_ref[:, g * STATE : (g + 1) * STATE],
-            ((0,), (0,)),
-        )
-        state_mine[g * per_group : (g + 1) * per_group] = state.astype(BF16).reshape(
-            per_group, rows, entries
-        )
-    whole = jnp.exp(last)
-
-    def state_copy(d):
-        to = lax.rem(me + d, n_sp)
-        return pltpu.make_async_remote_copy(
-            state_mine.at[to], states.at[me], sends.at[d], recvs.at[d], (to, tp), MESH
-        )
-
-    def back_copy(d):
-        to = lax.rem(me + d, n_sp)
-        return pltpu.make_async_remote_copy(
-            carries.at[to], later.at[me], b_sends.at[d], b_recvs.at[d], (to, tp), MESH
-        )
-
-    def start_states(d, carry):
-        state_copy(hop(d, n_sp)).start()
-        return carry
-
-    lax.fori_loop(1, n_sp, start_states, 0)
-    kept = pltpu.make_async_copy(state_mine.at[me], states.at[me], one)
-    kept.start()
-
-    pair(0, normed_ref.at[:, mine(1 - core)], normed2).wait()
-    pair(1, mix_ref, mix2).wait()
-    both_mix = jnp.concatenate([mix_t, jnp.transpose(mix2[...])], axis=1)
-    both_normed = jnp.concatenate([normed_ref[:, mine(core)], normed2[...]], axis=0)
-    piece_rows = cols // 2
-    for z in range(4):
-        at = slice(z * 8 * cols, (z + 1) * 8 * cols)
-        parts[z] = (
-            dot(both_mix[at, :], both_normed).astype(BF16).reshape(4, 2, 2, piece_rows, half)
-        )
-
-    lane_y, lane_z = lax.rem(chip, 4), lax.div(chip, 4)
-
-    def at_y(y):
-        return (lane_z * 8 + lax.rem(y, 4) * 2 + core, tp)
-
-    def at_z(z):
-        return (lax.rem(z, 4) * 8 + lane_y * 2 + core, tp)
-
-    y_ring = (lane_y, at_y(lane_y + 1), at_y(lane_y + 3))
-    z_ring = (lane_z, at_z(lane_z + 1), at_z(lane_z + 3))
-
-    def four(ref, k):
-        return [ref.at[k, i] for i in range(4)]
-
-    def bufs(landing, sums, k):
-        return [landing.at[k, 0], landing.at[k, 1], sums.at[k, 0], sums.at[k, 1]]
-
-    stages = [
-        ring_reduce(lambda b, w: parts.at[:, b, 0, w], *y_ring, *bufs(big_in, big_sum, 0), four(ring_sems, 0)),
-        ring_reduce(lambda b, w: parts.at[b, :, 1, w], *z_ring, *bufs(big_in, big_sum, 1), four(ring_sems, 1)),
-        ring_reduce(lambda b, w: reduced.at[0, w, b], *z_ring, *bufs(small_in, small_sum, 0), four(ring_sems, 2)),
-        ring_reduce(lambda b, w: reduced.at[1, w, b], *y_ring, *bufs(small_in, small_sum, 1), four(ring_sems, 3)),
-    ]
-    stages[0][0]()
-    stages[1][0]()
-
-
-    values = x_ref[...].astype(F32)
-    steps = spread(dt, owner)
-    scaled = values * steps
-    scaled_low = scaled.astype(BF16)
-    d_low = d_out.astype(BF16)
-    not_before = triangle(tokens, lambda t, s: s >= t)
-    below = (iota((tokens, tokens), 1) < iota((tokens, tokens), 0)).astype(F32)
-    head_lane = iota((1, heads), 1)
-    crossing = [jnp.zeros((tokens, heads), F32)]
-    d_affinity = []
-
-    def inside(g):
-        affinity = dot(
-            c_ref[:, g * STATE : (g + 1) * STATE],
-            b_ref[:, g * STATE : (g + 1) * STATE],
-            ((1,), (1,)),
-        )
-        sum_affinity = jnp.zeros((tokens, tokens), F32)
-        first = g * (heads // 2 // groups)
-        for q in range(first, first + heads // 2 // groups):
-            at = slice(q * 2 * HDIM, (q + 1) * 2 * HDIM)
-            d_halves = halves(d_low[:, at])
-            d_weights = dot(d_halves, scaled_low[:, at], ((1,), (1,)))
-            weights, moved = [], []
-            for j in range(2):
-                between = decay_between(cum, cum_rows, 2 * q + j)
-                weights.append((affinity * between).astype(BF16))
-                d_between = d_weights[j * tokens : (j + 1) * tokens] * between
-                sum_affinity = sum_affinity + d_between
-                moved.append((d_between * affinity).astype(BF16))
-            d_scaled[:, at] = dot(jnp.concatenate(weights, axis=0), d_halves, ((0,), (0,)))
-            reach = dot(not_before, jnp.concatenate(moved, axis=1))
-            for j in range(2):
-                over = jnp.sum(
-                    reach[:, j * tokens : (j + 1) * tokens] * below, axis=1, keepdims=True
-                )
-                crossing[0] = crossing[0] + jnp.where(head_lane == 2 * q + j, over, 0.0)
-        d_affinity.append(sum_affinity.astype(BF16))
-
-    inside(0)
-    kept.wait()
-
-    def finish_states(d, carry):
-        state_copy(d).wait()
-        return carry
-
-    lax.fori_loop(1, n_sp, finish_states, 0)
-    running = jnp.zeros((rows, entries), F32)
-    for step in range(n_sp):
-        i = n_sp - 1 - step
-        carries[i] = running.astype(BF16)
-        running = decays[i] * running + states[i].astype(F32)
-
-    def start_back(d, carry):
-        back_copy(hop(d, n_sp)).start()
-        return carry
-
-    lax.fori_loop(1, n_sp, start_back, 0)
-    kept_back = pltpu.make_async_copy(carries.at[me], later.at[me], one)
-    kept_back.start()
-
-    for g in range(1, groups):
-        inside(g)
-    stages[0][1]()
-    stages[1][1]()
-    read_out = []
-    for g in range(groups):
-        at = slice(g * wide, (g + 1) * wide)
-        by = slice(g * STATE, (g + 1) * STATE)
-        incoming = coming_ref[g * per_group : (g + 1) * per_group].reshape(wide, entries)
-        read_out.append(dot(c_ref[:, by], incoming, ((1,), (1,))))
-        dc_ref[:, by] = (
-            dot(d_affinity[g], b_ref[:, by]) + dot(since_low[:, at], incoming)
-        ).astype(BF16)
-    for k in range(2):
-        stages[k][2]()
-        for w in range(2):
-            reduced[k, w] = stages[k][3](w).astype(BF16)
-    stages[2][0]()
-    stages[3][0]()
-    reading = by_head(since_grad * jnp.concatenate(read_out, axis=1), owner)
-
-    kept_back.wait()
-
-    def finish_back(d, carry):
-        back_copy(d).wait()
-        return carry
-
-    lax.fori_loop(1, n_sp, finish_back, 0)
-    until = spread(jnp.exp(last - cum), owner)
-    ending = scaled * until
-    ending_low = ending.astype(BF16)
-    from_later = []
-    for g in range(groups):
-        at = slice(g * wide, (g + 1) * wide)
-        by = slice(g * STATE, (g + 1) * STATE)
-        after = later[g * per_group : (g + 1) * per_group].reshape(wide, entries)
-        from_later.append(dot(b_ref[:, by], after, ((1,), (1,))))
-        db_ref[:, by] = (
-            dot(d_affinity[g], c_ref[:, by], ((0,), (0,))) + dot(ending_low[:, at], after)
-        ).astype(BF16)
-    stages[2][1]()
-    stages[3][1]()
-    closing = jnp.concatenate(from_later, axis=1)
-    gradient = d_scaled[...] + until * closing
-    dx_ref[...] = (gradient * steps).astype(BF16)
-    direct = by_head(gradient * values, owner)
-    stored = by_head(ending * closing, owner)
-    kept_state = jnp.sum(
-        (
-            coming_ref[...].astype(F32).reshape(heads, HDIM, entries)
-            * later[...].astype(F32).reshape(heads, HDIM, entries)
-        ),
-        axis=1,
-    )
-    passing = dot_split(
-        kept_state, jnp.ones((8, entries), BF16), 3, ((1,), (1,)), left=False
-    )[0:1, :]
-    earlier = triangle(tokens, lambda t, s: s < t)
-    d_decay = (
-        crossing[0]
-        + dot_split(reading, not_before, 3, ((1,), (0,)), left=False)
-        + dot_split(stored, earlier, 3, ((1,), (0,)), left=False)
-        + passing * whole
-    )
-    ddt_ref[...] = turned(direct - d_decay * rate_ref[...])
-
-    for k in range(2):
-        stages[2 + k][2]()
-        for w in range(2):
-            first = (2 * k + w) * piece_rows
-            total[first : first + piece_rows, :] = stages[2 + k][3](w)
-
-    def lines(c):
-        return pl.ds(pl.multiple_of(c * cols, cols), cols)
-
-    given = pair(2, total.at[lines(1 - core), :], proj_ref.at[:, mine(core)])
-    given.start()
-    proj_ref[:, mine(core)] = total[lines(core), :]
-    given.wait_send()
-    pair(2, total.at[lines(core), :], proj_ref.at[:, mine(1 - core)]).wait_recv()
-
-
-def tail(
-    mix, weight, y, normed, x, dt, rate, extra, coming, decays, b, c, gate, scale, n_sp, n_tp
-):
-    dma = pltpu.SemaphoreType.DMA
-    tokens, channels = x.shape
-    heads = dt.shape[0]
-    _, rows, entries = coming.shape
-    width = mix.shape[1]
-    half = channels // 2
-    chips = n_sp // 2
-    cols = width // n_sp
-    return pl.pallas_call(
-        functools.partial(tail_kernel, n_sp, n_tp),
-        out_shape=(
-            jax.ShapeDtypeStruct((cols, channels), F32),
-            jax.ShapeDtypeStruct((tokens, channels), BF16),
-            jax.ShapeDtypeStruct((heads, tokens), F32),
-            jax.ShapeDtypeStruct(b.shape, BF16),
-            jax.ShapeDtypeStruct(c.shape, BF16),
-            jax.ShapeDtypeStruct((tokens, channels), BF16),
-        ),
-        in_specs=[vmem_spec(), any_spec()] + [vmem_spec()] * 12,
-        out_specs=(vmem_spec(),) * 6,
-        scratch_shapes=[
-            pltpu.VMEM((chips, 2, cols, channels), BF16),
-            pltpu.VMEM((tokens, half), BF16),
-            pltpu.VMEM((tokens, width), BF16),
-            pltpu.VMEM((4, 4, 2, 2, cols // 2, half), BF16),
-            pltpu.VMEM((2, 2, 3, 4, cols // 2, half), BF16),
-            pltpu.VMEM((2, 2, 4, cols // 2, half), BF16),
-            pltpu.VMEM((2, 2, 3, cols // 2, half), BF16),
-            pltpu.VMEM((2, 2, cols // 2, half), BF16),
-            pltpu.VMEM((2, 2, 4, cols // 2, half), BF16),
-            pltpu.VMEM((2 * cols, half), F32),
-            pltpu.VMEM((n_sp, rows, entries), BF16),
-            pltpu.VMEM((n_sp, rows, entries), BF16),
-            pltpu.VMEM((n_sp, rows, entries), BF16),
-            pltpu.VMEM((n_sp, rows, entries), BF16),
-            pltpu.VMEM((tokens, channels), F32),
-            dma,
-            dma((2,)),
-            dma((3,)),
-            dma((3,)),
-            dma((4, 4, 3)),
-        ]
-        + [dma((n_sp,))] * 4,
-        compiler_params=pltpu.CompilerParams(
-            collective_id=2, has_side_effects=True, vmem_limit_bytes=VMEM_BYTES
-        ),
-        name="tail",
-    )(mix, weight, y, normed, x, dt, rate, extra, coming, decays, b, c, gate, scale)
 
 
 def finish_kernel(count, *refs):
@@ -1422,7 +1413,7 @@
     entering = state_entering_span.reshape(n_sp, part_rows, STATE)
     rate = head_decay_rate[None, :]
     scale = group_norm_scale[None, :]
-    scan_out, normed_low, coming, decays, mix_grad, weight, grad_g, grad_u, grad_d = main(
+    proj_grad, input_grad, step_grad, b_grad, c_grad, gate_grad_in, grad_g, grad_u, grad_d = main(
         mixer_output_stream,
         expert_combine_weight.T,
         head_mixer_input,
@@ -1440,25 +1431,6 @@
         routes.T,
         layer_output_gradient,
         mixer_output_weight.T.reshape(2, -1, mixer_output_weight.shape[0]),
-        n_sp,
-        n_tp,
-    )
-    weight = weight.reshape(2, n_sp // 2, -1, mixer_output_weight.shape[0])
-    proj_grad, input_grad, step_grad, b_grad, c_grad, gate_grad_in = tail(
-        mix_grad,
-        weight,
-        scan_out,
-        normed_low,
-        head_mixer_input,
-        head_step_size.T,
-        rate,
-        extra_log_decay.T,
-        coming,
-        decays,
-        state_input_vectors,
-        state_readout_vectors,
-        gate_preactivation,
-        scale,
         n_sp,
         n_tp,
     )

time: 131 us -> 125 us (0.954)
  Pallas kernels: 129 us -> 123 us
    pallas_call x1 -> x0, Pallas kernels: 33.8 us -> none  [tail(): pl.pallas_call(functools.partial(tail_kernel, n_sp, n_tp), out_shape=(jax...]
    pallas_call x1, Pallas kernels: 85.6 us -> 113 us  [main(): pl.pallas_call(functools.partial(main_kernel, n_sp, n_tp), out_shape=(jax...]
where the time goes in v5:
time: 125 us; the launch traced here: 124 us
  Pallas kernels  123 us (98%)
    pallas_call x1, Pallas kernels, main(): pl.pallas_call(functools.partial(main_kernel, n_sp, n_tp), out_shape=(jax...  113 us
    pallas_call x1, Pallas kernels, finish(): pl.pallas_call(functools.partial(finish_kernel, count), out_shape=tuple((...  9.21 us

profile of v5, /device:TPU:0, one launch (start us, length us, event | category | flops | bytes accessed | tf_op | source)
XLA Modules:
  0.0 123.5 jit_solution(17623343785528792159)
XLA Ops:
  0.6 113.5 %main.1 = (f32[64,1024]{1,0:T(8,128)}, bf16[128,1024]{1,0:T(8,128)(2,1)}, f32[16,128]{1,0:T(8,128)}, bf16[128,256]{1,0:T(8,128)(2,1)}, bf16[128,256]{1,0:T(8,128...) custom-call(bf16[128,512]{1,0:T(8,128)(2,1)} %refs_0_.1, ...), custom_call_target="tpu_custom_call" | custom-call | tf_op jit(solution)/shard_map/main/pallas_call | solution.py:1304
  114.2 9.2 %finish.1 = (f32[64,1024]{1,0:T(8,128)}, bf16[128,1024]{1,0:T(8,128)(2,1)}, f32[16,128]{1,0:T(8,128)}, bf16[128,256]{1,0:T(8,128)(2,1)}, bf16[128,256]{1,0:T(8,1...) custom-call(f32[64,1024]{1,0:T(8,128)} %get-tuple-element.27.refs_0_, ...), custom_call_target="tpu_custom_call" | custom-call | tf_op jit(solution)/shard_map/finish/pallas_call | solution.py:1378

commit v6 on v5

--- a/solution.py
+++ b/solution.py
@@ -892,6 +892,9 @@
     def mine(c):
         return pl.ds(pl.multiple_of(c * half, half), half)
 
+    pair(0, normed_ref.at[:, mine(1 - core)], normed2).start()
+    pair(1, mix_ref, mix2).start()
+
     owner = head_spread(heads, HDIM)
     dt = turned(dt_ref[...])
     cum = cumulative_decay(dt, rate_ref[...], turned(extra_ref[...]))
@@ -904,8 +907,6 @@
         dot(mix_ref[...], whole_weight[:, g * wide : (g + 1) * wide]) for g in range(groups)
     ]
     mix_t = jnp.transpose(mix_ref[...])
-    pair(0, normed_ref.at[:, mine(1 - core)], normed2).start()
-    pair(1, mix_ref, mix2).start()
     d_y = []
     for g in range(groups):
         at = slice(g * wide, (g + 1) * wide)

time: 125 us -> 125 us (level)
  no operation moved by 1% of the time
where the time goes in v6:
time: 125 us; the launch traced here: 123 us
  Pallas kernels  123 us (98%)
    pallas_call x1, Pallas kernels, main(): pl.pallas_call(functools.partial(main_kernel, n_sp, n_tp), out_shape=(jax...  113 us
    pallas_call x1, Pallas kernels, finish(): pl.pallas_call(functools.partial(finish_kernel, count), out_shape=tuple((...  9.21 us

profile of v6, /device:TPU:0, one launch (start us, length us, event | category | flops | bytes accessed | tf_op | source)
XLA Modules:
  0.0 123.4 jit_solution(75505761267480899)
XLA Ops:
  0.6 113.4 %main.1 = (f32[64,1024]{1,0:T(8,128)}, bf16[128,1024]{1,0:T(8,128)(2,1)}, f32[16,128]{1,0:T(8,128)}, bf16[128,256]{1,0:T(8,128)(2,1)}, bf16[128,256]{1,0:T(8,128...) custom-call(bf16[128,512]{1,0:T(8,128)(2,1)} %refs_0_.1, ...), custom_call_target="tpu_custom_call" | custom-call | tf_op jit(solution)/shard_map/main/pallas_call | solution.py:1305
  114.0 9.2 %finish.1 = (f32[64,1024]{1,0:T(8,128)}, bf16[128,1024]{1,0:T(8,128)(2,1)}, f32[16,128]{1,0:T(8,128)}, bf16[128,256]{1,0:T(8,128)(2,1)}, bf16[128,256]{1,0:T(8,1...) custom-call(f32[64,1024]{1,0:T(8,128)} %get-tuple-element.27.refs_0_, ...), custom_call_target="tpu_custom_call" | custom-call | tf_op jit(solution)/shard_map/finish/pallas_call | solution.py:1379
